TPU v7x, 256 devices: a whole 4x4x8 slice. The times are simulated.
256 devices in a mesh: fs: 32 (over z, y), tp: 8 (over x, core).
Axes of the slice: x: 4, y: 4, z: 8, core: 2. Of those that a mesh axis runs over, the one named last changes fastest.
Arguments:
- x_next: bfloat16 [6144, 2048], P(('fs', 'tp')), may hold values from -6 to 6
- x_prev: bfloat16 [6144, 2048], P(('fs', 'tp')), may hold values from -6 to 6
- grad_out: bfloat16 [6144, 2048], P(('fs', 'tp')), may hold values from -24 to 24
- gate_w: bfloat16 [2048, 2816], P('fs', 'tp'), may hold values from -0.125 to 0.125
- up_w: bfloat16 [2048, 2816], P('fs', 'tp'), may hold values from -0.125 to 0.125
- down_w: bfloat16 [2816, 2048], P('tp', 'fs'), may hold values from -0.109375 to 0.109375
- acc_gate: float32 [2048, 2816], P('fs', 'tp'), may hold values from -2.5 to 2.5
- acc_up: float32 [2048, 2816], P('fs', 'tp'), may hold values from -2.5 to 2.5
- acc_down: float32 [2816, 2048], P('tp', 'fs'), may hold values from -2.5 to 2.5
Outputs:
- out_next: bfloat16 [6144, 2048], P(('fs', 'tp'))
- saved_hidden: bfloat16 [6144, 2816], P('fs', 'tp')
- grad_input: bfloat16 [6144, 2048], P(('fs', 'tp'))
- new_gate: float32 [2048, 2816], P('fs', 'tp')
- new_up: float32 [2048, 2816], P('fs', 'tp')
- new_down: float32 [2816, 2048], P('tp', 'fs')
All inputs are finite; a program needn't handle non-finite values.
Results may differ from a plain program's by a relative error of at most 0.014.
Values may be sent and summed in bfloat16 or wider, within the bound.
No kernel may reach another device: no remote copies, remote signals or barrier semaphores. Data moves between devices by JAX's collectives and lax.ppermute only.
A program may use at most 64 MiB of HBM per device.

v0:
```python
import math

import jax
import jax.numpy as jnp
from jax import lax
from jax.sharding import Mesh
from jax.sharding import PartitionSpec as P


BF16 = jnp.bfloat16
F32 = jnp.float32
FS = ("z", "y")
TP = ("x", "c")
ALL = ("z", "y", "x", "c")


def spread(blocks, axis):
    return lax.all_to_all(blocks, axis, 0, 0, tiled=True)


def gathered(array, axis):
    return spread(jnp.broadcast_to(array[None], (lax.axis_size(axis), *array.shape)), axis)


def swapped(array):
    return lax.ppermute(array, "c", [(0, 1), (1, 0)])


def moved(array, axis, step):
    length = lax.axis_size(axis)
    return lax.ppermute(array, axis, [(i, (i + step) % length) for i in range(length)])


def around(array, axis):
    return [array] + [moved(array, axis, -step) for step in range(1, lax.axis_size(axis))]


def sum_for_owner(blocks, axis):
    total = blocks[0].astype(F32)
    for step in range(1, len(blocks)):
        total = total + moved(blocks[step], axis, step).astype(F32)
    return total.astype(BF16)


def dot(left, right, dims):
    return lax.dot_general(left, right, (dims, ((), ())), preferred_element_type=F32)


def layer(x_next, x_prev, grad_out, gate_w, up_w, down_w, acc_gate, acc_up, acc_down):
    rows, width = x_prev.shape
    nz, ny, nx, nc = (lax.axis_size(name) for name in ALL)
    plane = ny * nx
    total_rows = rows * nz * ny * nx * nc
    factor = 1.0 / math.sqrt(total_rows)
    units = gate_w.shape[1]
    part = units // ny
    shard = gate_w.shape[0]
    deep = shard * ny
    core = lax.axis_index("c")

    half = width // 2
    first = jnp.concatenate((x_prev, x_next[:, :half]), axis=1)
    second = jnp.concatenate((grad_out, x_next[:, half:]), axis=1)
    first = around(first, "x")
    second = around(second, "y")
    first, second = jnp.stack(first), jnp.stack(second)
    first = around(first, "y")
    second = around(second, "x")
    first = jnp.stack(first).reshape(plane * rows, width + half)
    second = jnp.stack(second, axis=1).reshape(plane * rows, width + half)
    prev, cotangent = first[:, :width], second[:, :width]
    later = jnp.concatenate((first[:, width:], second[:, width:]), axis=1)

    mine = jnp.stack((gate_w.T, up_w.T, down_w)).reshape(3, ny, part, shard)
    mine = jnp.moveaxis(mine, 1, 0)
    mine = spread(mine, "y")
    mine = jnp.moveaxis(mine, 0, 2).reshape(3, part, deep)
    own = gathered(mine, "z")
    other = swapped(own)
    weights = jnp.stack((own, other))
    weights = weights.transpose(2, 0, 3, 1, 4).reshape(3, 2 * part, width)
    gate_up = weights[:2].reshape(4 * part, width)
    down = weights[2]

    pre = dot(prev, gate_up, ((1,), (1,)))
    gate_prev, up_prev = pre[:, : 2 * part], pre[:, 2 * part :]
    grad_hidden = dot(cotangent, down, ((1,), (1,)))
    sig = jax.nn.sigmoid(gate_prev)
    silu = gate_prev * sig
    grad_gate = (grad_hidden * up_prev * sig * (1.0 + gate_prev * (1.0 - sig))).astype(BF16)
    grad_up = (grad_hidden * silu).astype(BF16)
    hidden_prev = (silu * up_prev).astype(BF16)
    grads = jnp.concatenate((grad_gate, grad_up), axis=1)
    term = dot(grads, prev, ((0,), (0,))).reshape(2, 2, part, width)
    term_down = dot(hidden_prev, cotangent, ((0,), (0,))).reshape(1, 2, part, width)
    kept = jnp.concatenate((term[:, 0], term_down[:, 0]))
    sent = jnp.concatenate((term[:, 1], term_down[:, 1])).astype(BF16)
    sent = swapped(sent)
    paired = (kept + sent.astype(F32)).astype(BF16)
    paired = jnp.moveaxis(paired.reshape(3, part, nz, deep), 2, 0)
    summed = spread(paired, "z")
    summed = jnp.sum(summed.astype(F32), axis=0).astype(BF16)
    summed = jnp.moveaxis(summed.reshape(3, part, ny, shard), 2, 0)
    summed = spread(summed, "y")
    summed = jnp.moveaxis(summed, 0, 1).reshape(3, units, shard).astype(F32)
    new_gate = acc_gate + factor * summed[0].T
    new_up = acc_up + factor * summed[1].T
    new_down = acc_down + factor * summed[2]

    input_part = dot(grads, gate_up, ((1,), (0,))).astype(BF16).reshape(ny, nx, rows, width)
    by_x = sum_for_owner([input_part[:, k] for k in range(nx)], "x")
    grad_input = sum_for_owner([by_x[k] for k in range(ny)], "y")

    pre_next = dot(later, gate_up, ((1,), (1,)))
    hidden = (jax.nn.silu(pre_next[:, : 2 * part]) * pre_next[:, 2 * part :]).astype(BF16)
    out_part = dot(hidden, down, ((1,), (0,))).astype(BF16).reshape(ny, nx, rows, width)
    by_y = sum_for_owner([out_part[k] for k in range(ny)], "y")
    out_next = sum_for_owner([by_y[k] for k in range(nx)], "x")

    partner = swapped(hidden[:, part:])
    pair = jnp.stack((hidden[:, :part], partner)).reshape(nc, ny, nx, rows, part)
    back = [pair[:, 0]] + [moved(pair[:, step], "y", step) for step in range(1, ny)]
    saved = jnp.stack([back[-step % ny] for step in range(ny)])
    saved = jnp.roll(saved, (lax.axis_index("y"), lax.axis_index("x")), (0, 2))
    saved = jnp.where(core == 0, saved, saved[:, ::-1])
    saved = saved.transpose(2, 1, 3, 0, 4).reshape(nx * nc * rows, units)
    return out_next, saved, grad_input, new_gate, new_up, new_down


def solution(mesh):
    split = Mesh(mesh.devices.reshape(8, 4, 4, 2), ALL)
    tokens = P(ALL, None)
    wide, tall = P(FS, TP), P(TP, FS)
    in_specs = (tokens, tokens, tokens, wide, wide, tall, wide, wide, tall)
    out_specs = (tokens, wide, tokens, wide, wide, tall)
    return jax.shard_map(layer, mesh=split, in_specs=in_specs, out_specs=out_specs, check_vma=False)
```

profile of v0, /device:TPU:64, one launch (start us, length us, event | category | flops | bytes accessed | tf_op | source)
XLA Modules:
  0.0 197.8 jit_solution(15919083127479670981)
XLA Ops:
  3.6 10.6 %all_to_all.20 = bf16[4,3,88,64]{2,3,1,0:T(8,128)(2,1)S(1)} all-to-all(bf16[4,3,88,64]{2,3,1,0:T(8,128)(2,1)S(1)} %copy.91), channel_id=1, replica_groups=mesh['z'=8,'y'=4,'x'=4,'c'=2] {'y'}, dimensions={0} | all-to-all | bytes 270336 | tf_op jit(solution)/shard_map/all_to_all | solution.py:18
  14.3 1.1 broadcast_in_dim.10
  15.5 8.1 %all-to-all-start.1 = ((bf16[8,3,88,256]{3,2,1,0:T(8,128)(2,1)}), bf16[8,3,88,256]{3,2,1,0:T(8,128)(2,1)S(1)}, u32[]{:S(2)}, u32[]{:S(2)}) async-start(bf16[8,3,88,256]{3,2,1,0:T(8,128)(2,1)} %broadcast_in_dim.10), calls=%async_computation.1 | async-start | bytes 2162688 | tf_op jit(solution)/shard_map/all_to_all | solution.py:18
  23.6 1.1 collective-permute-start.7
  24.7 2.2 %collective-permute-start.6 = (bf16[24,3072]{1,0:T(8,128)(2,1)S(1)}, bf16[24,3072]{1,0:T(8,128)(2,1)S(1)}, u32[]{:S(2)}, u32[]{:S(2)}) collective-permute-start(bf16[24,3072]{1,0:T(8,128)(2,1)S(1)} %get-tuple-element.34), channel_id=1, source_target_pairs={{0,24},{8,0},{16,8},{24,16},{1,25},{9,1},{17,9},{25,17},{2,26},{10... | collective-permute-start | bytes 442376 | tf_op jit(solution)/shard_map/ppermute | solution.py:31
  27.0 3.5 %collective-permute-done.7 = bf16[24,3072]{1,0:T(8,128)(2,1)S(1)} collective-permute-done((bf16[24,3072]{1,0:T(8,128)(2,1)S(1)}, bf16[24,3072]{1,0:T(8,128)(2,1)S(1)}, u32[]{:S(2)}, u32[]{:S(2)}) %collective-permute-start.7) | collective-permute-done | bytes 147488 | tf_op jit(solution)/shard_map/ppermute | solution.py:31
  30.5 2.8 %collective-permute-done.8 = bf16[24,3072]{1,0:T(8,128)(2,1)S(1)} collective-permute-done((bf16[24,3072]{1,0:T(8,128)(2,1)S(1)}, bf16[24,3072]{1,0:T(8,128)(2,1)S(1)}, u32[]{:S(2)}, u32[]{:S(2)}) %collective-permute-start.8) | collective-permute-done | bytes 147488 | tf_op jit(solution)/shard_map/ppermute | solution.py:31
  34.2 3.0 %collective-permute-start.10 = (bf16[4,24,3072]{2,1,0:T(8,128)(2,1)}, bf16[4,24,3072]{2,1,0:T(8,128)(2,1)}, u32[]{:S(2)}, u32[]{:S(2)}) collective-permute-start(bf16[4,24,3072]{2,1,0:T(8,128)(2,1)} %get-tuple-element.18), channel_id=1, source_target_pairs={{0,4},{2,6},{4,0},{6,2},{1,5},{3,7},{5,1},{7,3},{8,12},{10,14},{12... | collective-permute-start | bytes 1769480 | tf_op jit(solution)/shard_map/ppermute | solution.py:31
  37.2 1.1 collective-permute-start.9
  38.4 1.6 collective-permute-start.1
  40.0 2.0 %collective-permute-start = (bf16[24,3072]{1,0:T(8,128)(2,1)S(1)}, bf16[24,3072]{1,0:T(8,128)(2,1)S(1)}, u32[]{:S(2)}, u32[]{:S(2)}) collective-permute-start(bf16[24,3072]{1,0:T(8,128)(2,1)S(1)} %get-tuple-element.32), channel_id=1, source_target_pairs={{0,6},{2,0},{4,2},{6,4},{1,7},{3,1},{5,3},{7,5},{8,14},{10,8},{12,... | collective-permute-start | bytes 442376 | tf_op jit(solution)/shard_map/ppermute | solution.py:31
  42.1 12.0 %collective-permute-done.1 = bf16[24,3072]{1,0:T(8,128)(2,1)S(1)} collective-permute-done((bf16[24,3072]{1,0:T(8,128)(2,1)S(1)}, bf16[24,3072]{1,0:T(8,128)(2,1)S(1)}, u32[]{:S(2)}, u32[]{:S(2)}) %collective-permute-start.1) | collective-permute-done | bytes 147488 | tf_op jit(solution)/shard_map/ppermute | solution.py:31
  54.1 14.2 %collective-permute-start.11 = (bf16[4,24,3072]{2,1,0:T(8,128)(2,1)}, bf16[4,24,3072]{2,1,0:T(8,128)(2,1)}, u32[]{:S(2)}, u32[]{:S(2)}) collective-permute-start(bf16[4,24,3072]{2,1,0:T(8,128)(2,1)} %get-tuple-element.18), channel_id=1, source_target_pairs={{0,2},{2,4},{4,6},{6,0},{1,3},{3,5},{5,7},{7,1},{8,10},{10,12},{12... | collective-permute-start | bytes 1769480 | tf_op jit(solution)/shard_map/ppermute | solution.py:31
  69.1 2.0 %fusion.46 = (bf16[1,4,24,3072]{3,2,1,0:T(8,128)(2,1)S(1)}, bf16[4,24,3072]{2,1,0:T(8,128)(2,1)}) fusion(bf16[1,24,3072]{2,1,0:T(8,128)(2,1)} %bitcast.202, bf16[1,24,3072]{2,1,0:T(8,128)(2,1)} %bitcast.200, bf16[1,24,3072]{2,1,0:T(8,128)(2,1)} %bitcast.201, bf16[1,24,3072]{2,1,0:T(8,128)(2,1)S(1)} %get-tuple-element.31), kind=kLoop, calls=%fused_computation.109 | loop fusion | flops 884736 | bytes 1769472 | tf_op jit(solution)/shard_map/stack | solution.py:69
  71.8 1.3 collective-permute-start.5
  73.1 5.5 %collective-permute-done.11 = bf16[4,24,3072]{2,1,0:T(8,128)(2,1)} collective-permute-done((bf16[4,24,3072]{2,1,0:T(8,128)(2,1)}, bf16[4,24,3072]{2,1,0:T(8,128)(2,1)}, u32[]{:S(2)}, u32[]{:S(2)}) %collective-permute-start.11) | collective-permute-done | bytes 589856 | tf_op jit(solution)/shard_map/ppermute | solution.py:31
  78.7 1.7 pad_maximum_fusion.1
  80.5 8.7 %collective-permute-done.4 = bf16[4,24,3072]{2,1,0:T(8,128)(2,1)} collective-permute-done((bf16[4,24,3072]{2,1,0:T(8,128)(2,1)}, bf16[4,24,3072]{2,1,0:T(8,128)(2,1)}, u32[]{:S(2)}, u32[]{:S(2)}) %collective-permute-start.4) | collective-permute-done | bytes 589856 | tf_op jit(solution)/shard_map/ppermute | solution.py:31
  89.2 9.0 %collective-permute-done.3 = bf16[4,24,3072]{2,1,0:T(8,128)(2,1)} collective-permute-done((bf16[4,24,3072]{2,1,0:T(8,128)(2,1)}, bf16[4,24,3072]{2,1,0:T(8,128)(2,1)}, u32[]{:S(2)}, u32[]{:S(2)}) %collective-permute-start.3) | collective-permute-done | bytes 589856 | tf_op jit(solution)/shard_map/ppermute | solution.py:31
  98.2 3.1 %collective-permute-done.5 = bf16[4,24,3072]{2,1,0:T(8,128)(2,1)} collective-permute-done((bf16[4,24,3072]{2,1,0:T(8,128)(2,1)}, bf16[4,24,3072]{2,1,0:T(8,128)(2,1)}, u32[]{:S(2)}, u32[]{:S(2)}) %collective-permute-start.5) | collective-permute-done | bytes 589856 | tf_op jit(solution)/shard_map/ppermute | solution.py:31
  101.3 1.7 pad_maximum_fusion
  103.4 1.3 copy-done
  106.6 0.9 fusion.7
  108.8 1.0 convolution_convert_fusion.1
  109.8 0.9 fusion.5
  110.7 0.9 fusion.1
  113.4 1.1 fusion.47
  115.1 1.4 collective-permute-start.13
  116.8 1.1 pad_maximum_fusion.2
  118.9 1.0 copy.97
  120.0 2.5 %collective-permute-start.20 = (bf16[2,4,24,88]{3,2,1,0:T(8,128)(2,1)S(1)}, bf16[2,4,24,88]{3,2,1,0:T(8,128)(2,1)S(1)}, u32[]{:S(2)}, u32[]{:S(2)}) collective-permute-start(bf16[2,4,24,88]{3,2,1,0:T(8,128)(2,1)S(1)} %get-tuple-element.29), channel_id=1, source_target_pairs={{0,24},{8,0},{16,8},{24,16},{1,25},{9,1},{17,9},{25,17},{2,26},{10... | collective-permute-start | bytes 101384 | tf_op jit(solution)/shard_map/ppermute | solution.py:31
  122.5 13.2 %collective-permute-done.20 = bf16[2,4,24,88]{3,2,1,0:T(8,128)(2,1)S(1)} collective-permute-done((bf16[2,4,24,88]{3,2,1,0:T(8,128)(2,1)S(1)}, bf16[2,4,24,88]{3,2,1,0:T(8,128)(2,1)S(1)}, u32[]{:S(2)}, u32[]{:S(2)}) %collective-permute-start.20) | collective-permute-done | bytes 33824 | tf_op jit(solution)/shard_map/ppermute | solution.py:31
  136.0 5.5 %collective-permute-done.21 = bf16[2,4,24,88]{3,2,1,0:T(8,128)(2,1)S(1)} collective-permute-done((bf16[2,4,24,88]{3,2,1,0:T(8,128)(2,1)S(1)}, bf16[2,4,24,88]{3,2,1,0:T(8,128)(2,1)S(1)}, u32[]{:S(2)}, u32[]{:S(2)}) %collective-permute-start.21) | collective-permute-done | bytes 33824 | tf_op jit(solution)/shard_map/ppermute | solution.py:31
  141.5 5.3 %collective-permute-done.22 = bf16[2,4,24,88]{3,2,1,0:T(8,128)(2,1)S(1)} collective-permute-done((bf16[2,4,24,88]{3,2,1,0:T(8,128)(2,1)S(1)}, bf16[2,4,24,88]{3,2,1,0:T(8,128)(2,1)S(1)}, u32[]{:S(2)}, u32[]{:S(2)}) %collective-permute-start.22) | collective-permute-done | bytes 33824 | tf_op jit(solution)/shard_map/ppermute | solution.py:31
  146.8 1.4 collective-permute-start.23
  149.5 2.7 %collective-permute-start.24 = (bf16[4,24,2048]{2,1,0:T(8,128)(2,1)S(1)}, bf16[4,24,2048]{2,1,0:T(8,128)(2,1)}, u32[]{:S(2)}, u32[]{:S(2)}) collective-permute-start(bf16[4,24,2048]{2,1,0:T(8,128)(2,1)S(1)} %get-tuple-element.7), channel_id=1, source_target_pairs={{0,4},{2,6},{4,0},{6,2},{1,5},{3,7},{5,1},{7,3},{8,12},{10,14},{12... | collective-permute-start | bytes 1179656 | tf_op jit(solution)/shard_map/ppermute | solution.py:31
  152.1 1.5 fusion
  154.1 1.2 copy.108
  155.3 7.2 %all-to-all-start.2 = ((bf16[8,3,88,256]{3,2,1,0:T(8,128)(2,1)}), bf16[8,3,88,256]{3,2,1,0:T(8,128)(2,1)S(1)}, u32[]{:S(2)}, u32[]{:S(2)}) async-start(bf16[8,3,88,256]{3,2,1,0:T(8,128)(2,1)} %copy.108), calls=%async_computation.2 | async-start | bytes 2162688 | tf_op jit(solution)/shard_map/all_to_all | solution.py:18
  162.5 1.3 collective-permute-start.25
  163.8 1.5 fusion.18
  166.1 2.5 %collective-permute-start.18 = (bf16[24,2048]{1,0:T(8,128)(2,1)S(1)}, bf16[24,2048]{1,0:T(8,128)(2,1)S(1)}, u32[]{:S(2)}, u32[]{:S(2)}) collective-permute-start(bf16[24,2048]{1,0:T(8,128)(2,1)S(1)} %get-tuple-element.26), channel_id=1, source_target_pairs={{0,6},{2,0},{4,2},{6,4},{1,7},{3,1},{5,3},{7,5},{8,14},{10,8},{12,... | collective-permute-start | bytes 294920 | tf_op jit(solution)/shard_map/ppermute | solution.py:31
  168.6 3.1 %collective-permute-done.25 = bf16[4,24,2048]{2,1,0:T(8,128)(2,1)S(1)} collective-permute-done((bf16[4,24,2048]{2,1,0:T(8,128)(2,1)S(1)}, bf16[4,24,2048]{2,1,0:T(8,128)(2,1)S(1)}, u32[]{:S(2)}, u32[]{:S(2)}) %collective-permute-start.25) | collective-permute-done | bytes 393248 | tf_op jit(solution)/shard_map/ppermute | solution.py:31
  171.7 1.5 fusion.15
  173.3 3.2 %collective-permute-start.28 = (bf16[24,2048]{1,0:T(8,128)(2,1)S(1)}, bf16[24,2048]{1,0:T(8,128)(2,1)S(1)}, u32[]{:S(2)}, u32[]{:S(2)}) collective-permute-start(bf16[24,2048]{1,0:T(8,128)(2,1)S(1)} %get-tuple-element.23), channel_id=1, source_target_pairs={{0,24},{8,0},{16,8},{24,16},{1,25},{9,1},{17,9},{25,17},{2,26},{10... | collective-permute-start | bytes 294920 | tf_op jit(solution)/shard_map/ppermute | solution.py:31
  177.2 7.7 %all-to-all-done.2 = bf16[8,3,88,256]{3,2,1,0:T(8,128)(2,1)S(1)} async-done(((bf16[8,3,88,256]{3,2,1,0:T(8,128)(2,1)}), bf16[8,3,88,256]{3,2,1,0:T(8,128)(2,1)S(1)}, u32[]{:S(2)}, u32[]{:S(2)}) %all-to-all-start.2) | async-done | bytes 1081376 | tf_op jit(solution)/shard_map/all_to_all | solution.py:18
  186.0 3.4 %all-to-all-start.3 = ((bf16[4,3,88,64]{2,3,1,0:T(8,128)(2,1)}), bf16[4,3,88,64]{2,3,1,0:T(8,128)(2,1)S(1)}, u32[]{:S(2)}, u32[]{:S(2)}) async-start(bf16[4,3,88,64]{2,3,1,0:T(8,128)(2,1)} %copy.111), calls=%async_computation.3 | async-start | bytes 393216 | tf_op jit(solution)/shard_map/all_to_all | solution.py:18
  190.1 5.5 %all-to-all-done.3 = bf16[4,3,88,64]{2,3,1,0:T(8,128)(2,1)S(1)} async-done(((bf16[4,3,88,64]{2,3,1,0:T(8,128)(2,1)}), bf16[4,3,88,64]{2,3,1,0:T(8,128)(2,1)S(1)}, u32[]{:S(2)}, u32[]{:S(2)}) %all-to-all-start.3) | async-done | bytes 135200 | tf_op jit(solution)/shard_map/all_to_all | solution.py:18
  (121 shorter events, 20.1 us)
Async XLA Ops:
  14.3 9.3 %copy-start.9 = (bf16[24,2048]{1,0:T(8,128)(2,1)S(1)}, bf16[24,2048]{1,0:T(8,128)(2,1)}, u32[]{:S(2)}) copy-start(bf16[24,2048]{1,0:T(8,128)(2,1)} %param.9) | copy-start | bytes 294916
  14.3 9.3 %copy-start.5 = (bf16[24,2048]{1,0:T(8,128)(2,1)S(1)}, bf16[24,2048]{1,0:T(8,128)(2,1)}, u32[]{:S(2)}) copy-start(bf16[24,2048]{1,0:T(8,128)(2,1)} %param.11) | copy-start | bytes 294916
  15.5 53.0 %all-to-all-start.1 = ((bf16[8,3,88,256]{3,2,1,0:T(8,128)(2,1)}), bf16[8,3,88,256]{3,2,1,0:T(8,128)(2,1)S(1)}, u32[]{:S(2)}, u32[]{:S(2)}) async-start(bf16[8,3,88,256]{3,2,1,0:T(8,128)(2,1)} %broadcast_in_dim.10), calls=%async_computation.1 | async-start | bytes 2162688 | tf_op jit(solution)/shard_map/all_to_all | solution.py:18
  23.6 14.8 %copy-start.6 = (bf16[24,2048]{1,0:T(8,128)(2,1)S(1)}, bf16[24,2048]{1,0:T(8,128)(2,1)}, u32[]{:S(2)}) copy-start(bf16[24,2048]{1,0:T(8,128)(2,1)} %param.10) | copy-start | bytes 294916
  23.6 6.9 %collective-permute-start.7 = (bf16[24,3072]{1,0:T(8,128)(2,1)S(1)}, bf16[24,3072]{1,0:T(8,128)(2,1)S(1)}, u32[]{:S(2)}, u32[]{:S(2)}) collective-permute-start(bf16[24,3072]{1,0:T(8,128)(2,1)S(1)} %get-tuple-element.34), channel_id=1, source_target_pairs={{0,16},{8,24},{16,0},{24,8},{1,17},{9,25},{17,1},{25,9},{2,18},{10... | collective-permute-start | bytes 442376 | tf_op jit(solution)/shard_map/ppermute | solution.py:31
  24.7 5.8 %collective-permute-start.6 = (bf16[24,3072]{1,0:T(8,128)(2,1)S(1)}, bf16[24,3072]{1,0:T(8,128)(2,1)S(1)}, u32[]{:S(2)}, u32[]{:S(2)}) collective-permute-start(bf16[24,3072]{1,0:T(8,128)(2,1)S(1)} %get-tuple-element.34), channel_id=1, source_target_pairs={{0,24},{8,0},{16,8},{24,16},{1,25},{9,1},{17,9},{25,17},{2,26},{10... | collective-permute-start | bytes 442376 | tf_op jit(solution)/shard_map/ppermute | solution.py:31
  27.0 6.4 %collective-permute-start.8 = (bf16[24,3072]{1,0:T(8,128)(2,1)S(1)}, bf16[24,3072]{1,0:T(8,128)(2,1)S(1)}, u32[]{:S(2)}, u32[]{:S(2)}) collective-permute-start(bf16[24,3072]{1,0:T(8,128)(2,1)S(1)} %get-tuple-element.34), channel_id=1, source_target_pairs={{0,8},{8,16},{16,24},{24,0},{1,9},{9,17},{17,25},{25,1},{2,10},{10... | collective-permute-start | bytes 442376 | tf_op jit(solution)/shard_map/ppermute | solution.py:31
  34.2 36.9 %collective-permute-start.10 = (bf16[4,24,3072]{2,1,0:T(8,128)(2,1)}, bf16[4,24,3072]{2,1,0:T(8,128)(2,1)}, u32[]{:S(2)}, u32[]{:S(2)}) collective-permute-start(bf16[4,24,3072]{2,1,0:T(8,128)(2,1)} %get-tuple-element.18), channel_id=1, source_target_pairs={{0,4},{2,6},{4,0},{6,2},{1,5},{3,7},{5,1},{7,3},{8,12},{10,14},{12... | collective-permute-start | bytes 1769480 | tf_op jit(solution)/shard_map/ppermute | solution.py:31
  37.2 34.6 %collective-permute-start.9 = (bf16[4,24,3072]{2,1,0:T(8,128)(2,1)}, bf16[4,24,3072]{2,1,0:T(8,128)(2,1)}, u32[]{:S(2)}, u32[]{:S(2)}) collective-permute-start(bf16[4,24,3072]{2,1,0:T(8,128)(2,1)} %get-tuple-element.18), channel_id=1, source_target_pairs={{0,6},{2,0},{4,2},{6,4},{1,7},{3,1},{5,3},{7,5},{8,14},{10,8},{12,... | collective-permute-start | bytes 1769480 | tf_op jit(solution)/shard_map/ppermute | solution.py:31
  38.4 15.7 %collective-permute-start.1 = (bf16[24,3072]{1,0:T(8,128)(2,1)S(1)}, bf16[24,3072]{1,0:T(8,128)(2,1)S(1)}, u32[]{:S(2)}, u32[]{:S(2)}) collective-permute-start(bf16[24,3072]{1,0:T(8,128)(2,1)S(1)} %get-tuple-element.32), channel_id=1, source_target_pairs={{0,4},{2,6},{4,0},{6,2},{1,5},{3,7},{5,1},{7,3},{8,12},{10,14},{12... | collective-permute-start | bytes 442376 | tf_op jit(solution)/shard_map/ppermute | solution.py:31
  40.0 28.4 %collective-permute-start = (bf16[24,3072]{1,0:T(8,128)(2,1)S(1)}, bf16[24,3072]{1,0:T(8,128)(2,1)S(1)}, u32[]{:S(2)}, u32[]{:S(2)}) collective-permute-start(bf16[24,3072]{1,0:T(8,128)(2,1)S(1)} %get-tuple-element.32), channel_id=1, source_target_pairs={{0,6},{2,0},{4,2},{6,4},{1,7},{3,1},{5,3},{7,5},{8,14},{10,8},{12,... | collective-permute-start | bytes 442376 | tf_op jit(solution)/shard_map/ppermute | solution.py:31
  42.1 26.4 %collective-permute-start.2 = (bf16[24,3072]{1,0:T(8,128)(2,1)S(1)}, bf16[24,3072]{1,0:T(8,128)(2,1)S(1)}, u32[]{:S(2)}, u32[]{:S(2)}) collective-permute-start(bf16[24,3072]{1,0:T(8,128)(2,1)S(1)} %get-tuple-element.32), channel_id=1, source_target_pairs={{0,2},{2,4},{4,6},{6,0},{1,3},{3,5},{5,7},{7,1},{8,10},{10,12},{12... | collective-permute-start | bytes 442376 | tf_op jit(solution)/shard_map/ppermute | solution.py:31
  54.1 14.4 %copy-start.2 = (bf16[24,3072]{1,0:T(8,128)(2,1)}, bf16[24,3072]{1,0:T(8,128)(2,1)S(1)}, u32[]{:S(2)}) copy-start(bf16[24,3072]{1,0:T(8,128)(2,1)S(1)} %collective-permute-done.1) | copy-start | bytes 442372
  54.1 24.6 %collective-permute-start.11 = (bf16[4,24,3072]{2,1,0:T(8,128)(2,1)}, bf16[4,24,3072]{2,1,0:T(8,128)(2,1)}, u32[]{:S(2)}, u32[]{:S(2)}) collective-permute-start(bf16[4,24,3072]{2,1,0:T(8,128)(2,1)} %get-tuple-element.18), channel_id=1, source_target_pairs={{0,2},{2,4},{4,6},{6,0},{1,3},{3,5},{5,7},{7,1},{8,10},{10,12},{12... | collective-permute-start | bytes 1769480 | tf_op jit(solution)/shard_map/ppermute | solution.py:31
  68.4 0.7 copy-start.3
  68.4 34.6 %collective-permute-start.12 = (bf16[8,3,88,256]{3,2,1,0:T(8,128)(2,1)S(1)}, bf16[8,3,88,256]{3,2,1,0:T(8,128)(2,1)S(1)}, u32[]{:S(2)}, u32[]{:S(2)}) collective-permute-start(bf16[8,3,88,256]{3,2,1,0:T(8,128)(2,1)S(1)} %all-to-all-done.1), channel_id=1, source_target_pairs={{0,1},{1,0},{2,3},{3,2},{4,5},{5,4},{6,7},{7,6},{8,9},{9,8},{10,11... | collective-permute-start | bytes 3244040 | tf_op jit(solution)/shard_map/ppermute | solution.py:26
  68.4 0.7 copy-start.4
  71.1 18.1 %collective-permute-start.4 = (bf16[4,24,3072]{2,1,0:T(8,128)(2,1)}, bf16[4,24,3072]{2,1,0:T(8,128)(2,1)}, u32[]{:S(2)}, u32[]{:S(2)}) collective-permute-start(bf16[4,24,3072]{2,1,0:T(8,128)(2,1)} %get-tuple-element.16), channel_id=1, source_target_pairs={{0,16},{8,24},{16,0},{24,8},{1,17},{9,25},{17,1},{25,9},{2,18},{10... | collective-permute-start | bytes 1769480 | tf_op jit(solution)/shard_map/ppermute | solution.py:31
  71.1 27.1 %collective-permute-start.3 = (bf16[4,24,3072]{2,1,0:T(8,128)(2,1)}, bf16[4,24,3072]{2,1,0:T(8,128)(2,1)}, u32[]{:S(2)}, u32[]{:S(2)}) collective-permute-start(bf16[4,24,3072]{2,1,0:T(8,128)(2,1)} %get-tuple-element.16), channel_id=1, source_target_pairs={{0,24},{8,0},{16,8},{24,16},{1,25},{9,1},{17,9},{25,17},{2,26},{10... | collective-permute-start | bytes 1769480 | tf_op jit(solution)/shard_map/ppermute | solution.py:31
  71.8 29.5 %collective-permute-start.5 = (bf16[4,24,3072]{2,1,0:T(8,128)(2,1)}, bf16[4,24,3072]{2,1,0:T(8,128)(2,1)}, u32[]{:S(2)}, u32[]{:S(2)}) collective-permute-start(bf16[4,24,3072]{2,1,0:T(8,128)(2,1)} %get-tuple-element.16), channel_id=1, source_target_pairs={{0,8},{8,16},{16,24},{24,0},{1,9},{9,17},{17,25},{25,1},{2,10},{10... | collective-permute-start | bytes 1769480 | tf_op jit(solution)/shard_map/ppermute | solution.py:31
  103.3 1.4 copy-start
  105.2 1.1 slice-start
  109.8 8.1 %copy-start.1 = (bf16[384,2048]{1,0:T(8,128)(2,1)}, bf16[384,2048]{1,0:T(8,128)(2,1)S(1)}, u32[]{:S(2)}) copy-start(bf16[384,2048]{1,0:T(8,128)(2,1)S(1)} %convolution_convert_fusion.1) | copy-start | bytes 4718596
  113.2 5.7 %collective-permute-start.19 = (bf16[384,88]{0,1:T(8,128)(2,1)}, bf16[384,88]{0,1:T(8,128)(2,1)}, u32[]{:S(2)}, u32[]{:S(2)}) collective-permute-start(bf16[384,88]{0,1:T(8,128)(2,1)} %get-tuple-element.36), channel_id=1, source_target_pairs={{0,1},{1,0},{2,3},{3,2},{4,5},{5,4},{6,7},{7,6},{8,9},{9,8},{10,11... | collective-permute-start | bytes 202760 | tf_op jit(solution)/shard_map/ppermute | solution.py:26
  114.5 48.0 %collective-permute-start.15 = (bf16[4,24,2048]{2,1,0:T(8,128)(2,1)}, bf16[4,24,2048]{2,1,0:T(8,128)(2,1)}, u32[]{:S(2)}, u32[]{:S(2)}) collective-permute-start(bf16[4,24,2048]{2,1,0:T(8,128)(2,1)} %bitcast.32), channel_id=1, source_target_pairs={{0,24},{8,0},{16,8},{24,16},{1,25},{9,1},{17,9},{25,17},{2,26},{10... | collective-permute-start | bytes 1179656 | tf_op jit(solution)/shard_map/ppermute | solution.py:31
  115.1 48.8 %collective-permute-start.13 = (bf16[4,24,2048]{2,1,0:T(8,128)(2,1)}, bf16[4,24,2048]{2,1,0:T(8,128)(2,1)}, u32[]{:S(2)}, u32[]{:S(2)}) collective-permute-start(bf16[4,24,2048]{2,1,0:T(8,128)(2,1)} %bitcast.30), channel_id=1, source_target_pairs={{0,8},{8,16},{16,24},{24,0},{1,9},{9,17},{17,25},{25,1},{2,10},{10... | collective-permute-start | bytes 1179656 | tf_op jit(solution)/shard_map/ppermute | solution.py:31
  116.5 47.3 %collective-permute-start.14 = (bf16[4,24,2048]{2,1,0:T(8,128)(2,1)}, bf16[4,24,2048]{2,1,0:T(8,128)(2,1)}, u32[]{:S(2)}, u32[]{:S(2)}) collective-permute-start(bf16[4,24,2048]{2,1,0:T(8,128)(2,1)} %bitcast.31), channel_id=1, source_target_pairs={{0,16},{8,24},{16,0},{24,8},{1,17},{9,25},{17,1},{25,9},{2,18},{10... | collective-permute-start | bytes 1179656 | tf_op jit(solution)/shard_map/ppermute | solution.py:31
  117.9 31.6 %collective-permute-start.29 = (bf16[3,88,2048]{2,1,0:T(8,128)(2,1)}, bf16[3,88,2048]{2,1,0:T(8,128)(2,1)}, u32[]{:S(2)}, u32[]{:S(2)}) collective-permute-start(bf16[3,88,2048]{2,1,0:T(8,128)(2,1)} %pad_maximum_fusion.2), channel_id=1, source_target_pairs={{0,1},{1,0},{2,3},{3,2},{4,5},{5,4},{6,7},{7,6},{8,9},{9,8},{10,11... | collective-permute-start | bytes 3244040 | tf_op jit(solution)/shard_map/ppermute | solution.py:26
  120.0 15.7 %collective-permute-start.20 = (bf16[2,4,24,88]{3,2,1,0:T(8,128)(2,1)S(1)}, bf16[2,4,24,88]{3,2,1,0:T(8,128)(2,1)S(1)}, u32[]{:S(2)}, u32[]{:S(2)}) collective-permute-start(bf16[2,4,24,88]{3,2,1,0:T(8,128)(2,1)S(1)} %get-tuple-element.29), channel_id=1, source_target_pairs={{0,24},{8,0},{16,8},{24,16},{1,25},{9,1},{17,9},{25,17},{2,26},{10... | collective-permute-start | bytes 101384 | tf_op jit(solution)/shard_map/ppermute | solution.py:31
  135.7 5.8 %collective-permute-start.21 = (bf16[2,4,24,88]{3,2,1,0:T(8,128)(2,1)S(1)}, bf16[2,4,24,88]{3,2,1,0:T(8,128)(2,1)S(1)}, u32[]{:S(2)}, u32[]{:S(2)}) collective-permute-start(bf16[2,4,24,88]{3,2,1,0:T(8,128)(2,1)S(1)} %get-tuple-element.30), channel_id=1, source_target_pairs={{0,16},{8,24},{16,0},{24,8},{1,17},{9,25},{17,1},{25,9},{2,18},{10... | collective-permute-start | bytes 101384 | tf_op jit(solution)/shard_map/ppermute | solution.py:31
  141.5 5.3 %collective-permute-start.22 = (bf16[2,4,24,88]{3,2,1,0:T(8,128)(2,1)S(1)}, bf16[2,4,24,88]{3,2,1,0:T(8,128)(2,1)S(1)}, u32[]{:S(2)}, u32[]{:S(2)}) collective-permute-start(bf16[2,4,24,88]{3,2,1,0:T(8,128)(2,1)S(1)} %get-tuple-element.28), channel_id=1, source_target_pairs={{0,8},{8,16},{16,24},{24,0},{1,9},{9,17},{17,25},{25,1},{2,10},{10... | collective-permute-start | bytes 101384 | tf_op jit(solution)/shard_map/ppermute | solution.py:31
  146.8 21.8 %collective-permute-start.23 = (bf16[4,24,2048]{2,1,0:T(8,128)(2,1)}, bf16[4,24,2048]{2,1,0:T(8,128)(2,1)}, u32[]{:S(2)}, u32[]{:S(2)}) collective-permute-start(bf16[4,24,2048]{2,1,0:T(8,128)(2,1)} %get-tuple-element.6), channel_id=1, source_target_pairs={{0,2},{2,4},{4,6},{6,0},{1,3},{3,5},{5,7},{7,1},{8,10},{10,12},{12... | collective-permute-start | bytes 1179656 | tf_op jit(solution)/shard_map/ppermute | solution.py:31
  149.5 19.2 %collective-permute-start.24 = (bf16[4,24,2048]{2,1,0:T(8,128)(2,1)S(1)}, bf16[4,24,2048]{2,1,0:T(8,128)(2,1)}, u32[]{:S(2)}, u32[]{:S(2)}) collective-permute-start(bf16[4,24,2048]{2,1,0:T(8,128)(2,1)S(1)} %get-tuple-element.7), channel_id=1, source_target_pairs={{0,4},{2,6},{4,0},{6,2},{1,5},{3,7},{5,1},{7,3},{8,12},{10,14},{12... | collective-permute-start | bytes 1179656 | tf_op jit(solution)/shard_map/ppermute | solution.py:31
  155.3 29.7 %all-to-all-start.2 = ((bf16[8,3,88,256]{3,2,1,0:T(8,128)(2,1)}), bf16[8,3,88,256]{3,2,1,0:T(8,128)(2,1)S(1)}, u32[]{:S(2)}, u32[]{:S(2)}) async-start(bf16[8,3,88,256]{3,2,1,0:T(8,128)(2,1)} %copy.108), calls=%async_computation.2 | async-start | bytes 2162688 | tf_op jit(solution)/shard_map/all_to_all | solution.py:18
  162.5 9.2 %collective-permute-start.25 = (bf16[4,24,2048]{2,1,0:T(8,128)(2,1)S(1)}, bf16[4,24,2048]{2,1,0:T(8,128)(2,1)S(1)}, u32[]{:S(2)}, u32[]{:S(2)}) collective-permute-start(bf16[4,24,2048]{2,1,0:T(8,128)(2,1)S(1)} %get-tuple-element.8), channel_id=1, source_target_pairs={{0,6},{2,0},{4,2},{6,4},{1,7},{3,1},{5,3},{7,5},{8,14},{10,8},{12,... | collective-permute-start | bytes 1179656 | tf_op jit(solution)/shard_map/ppermute | solution.py:31
  165.3 11.2 %collective-permute-start.16 = (bf16[24,2048]{1,0:T(8,128)(2,1)S(1)}, bf16[24,2048]{1,0:T(8,128)(2,1)S(1)}, u32[]{:S(2)}, u32[]{:S(2)}) collective-permute-start(bf16[24,2048]{1,0:T(8,128)(2,1)S(1)} %get-tuple-element.25), channel_id=1, source_target_pairs={{0,2},{2,4},{4,6},{6,0},{1,3},{3,5},{5,7},{7,1},{8,10},{10,12},{12... | collective-permute-start | bytes 294920 | tf_op jit(solution)/shard_map/ppermute | solution.py:31
  166.1 10.4 %collective-permute-start.18 = (bf16[24,2048]{1,0:T(8,128)(2,1)S(1)}, bf16[24,2048]{1,0:T(8,128)(2,1)S(1)}, u32[]{:S(2)}, u32[]{:S(2)}) collective-permute-start(bf16[24,2048]{1,0:T(8,128)(2,1)S(1)} %get-tuple-element.26), channel_id=1, source_target_pairs={{0,6},{2,0},{4,2},{6,4},{1,7},{3,1},{5,3},{7,5},{8,14},{10,8},{12,... | collective-permute-start | bytes 294920 | tf_op jit(solution)/shard_map/ppermute | solution.py:31
  168.6 7.9 %collective-permute-start.17 = (bf16[24,2048]{1,0:T(8,128)(2,1)S(1)}, bf16[24,2048]{1,0:T(8,128)(2,1)S(1)}, u32[]{:S(2)}, u32[]{:S(2)}) collective-permute-start(bf16[24,2048]{1,0:T(8,128)(2,1)S(1)} %get-tuple-element.27), channel_id=1, source_target_pairs={{0,4},{2,6},{4,0},{6,2},{1,5},{3,7},{5,1},{7,3},{8,12},{10,14},{12... | collective-permute-start | bytes 294920 | tf_op jit(solution)/shard_map/ppermute | solution.py:31
  173.2 16.2 %collective-permute-start.26 = (bf16[24,2048]{1,0:T(8,128)(2,1)S(1)}, bf16[24,2048]{1,0:T(8,128)(2,1)S(1)}, u32[]{:S(2)}, u32[]{:S(2)}) collective-permute-start(bf16[24,2048]{1,0:T(8,128)(2,1)S(1)} %get-tuple-element.22), channel_id=1, source_target_pairs={{0,8},{8,16},{16,24},{24,0},{1,9},{9,17},{17,25},{25,1},{2,10},{10... | collective-permute-start | bytes 294920 | tf_op jit(solution)/shard_map/ppermute | solution.py:31
  173.3 16.1 %collective-permute-start.28 = (bf16[24,2048]{1,0:T(8,128)(2,1)S(1)}, bf16[24,2048]{1,0:T(8,128)(2,1)S(1)}, u32[]{:S(2)}, u32[]{:S(2)}) collective-permute-start(bf16[24,2048]{1,0:T(8,128)(2,1)S(1)} %get-tuple-element.23), channel_id=1, source_target_pairs={{0,24},{8,0},{16,8},{24,16},{1,25},{9,1},{17,9},{25,17},{2,26},{10... | collective-permute-start | bytes 294920 | tf_op jit(solution)/shard_map/ppermute | solution.py:31
  176.5 12.9 %collective-permute-start.27 = (bf16[24,2048]{1,0:T(8,128)(2,1)S(1)}, bf16[24,2048]{1,0:T(8,128)(2,1)S(1)}, u32[]{:S(2)}, u32[]{:S(2)}) collective-permute-start(bf16[24,2048]{1,0:T(8,128)(2,1)S(1)} %get-tuple-element.24), channel_id=1, source_target_pairs={{0,16},{8,24},{16,0},{24,8},{1,17},{9,25},{17,1},{25,9},{2,18},{10... | collective-permute-start | bytes 294920 | tf_op jit(solution)/shard_map/ppermute | solution.py:31
  186.0 9.7 %all-to-all-start.3 = ((bf16[4,3,88,64]{2,3,1,0:T(8,128)(2,1)}), bf16[4,3,88,64]{2,3,1,0:T(8,128)(2,1)S(1)}, u32[]{:S(2)}, u32[]{:S(2)}) async-start(bf16[4,3,88,64]{2,3,1,0:T(8,128)(2,1)} %copy.111), calls=%async_computation.3 | async-start | bytes 393216 | tf_op jit(solution)/shard_map/all_to_all | solution.py:18
  189.4 7.0 %copy-start.10 = (f32[352,64]{0,1:T(8,128)S(1)}, f32[352,64]{0,1:T(8,128)}, u32[]{:S(2)}) copy-start(f32[352,64]{0,1:T(8,128)} %param.17) | copy-start | bytes 270340
  190.1 7.0 %copy-start.7 = (f32[64,352]{1,0:T(8,128)S(1)}, f32[64,352]{1,0:T(8,128)}, u32[]{:S(2)}) copy-start(f32[64,352]{1,0:T(8,128)} %param.16) | copy-start | bytes 270340
  190.1 7.0 %copy-start.8 = (f32[64,352]{1,0:T(8,128)S(1)}, f32[64,352]{1,0:T(8,128)}, u32[]{:S(2)}) copy-start(f32[64,352]{1,0:T(8,128)} %param.15) | copy-start | bytes 270340
where the time goes:
time: 202 us; the launch traced here: 198 us
  waiting for transfers between devices  85.2 us (42%)
  starting transfers between devices  63.3 us (31%)
  local copies, waits for them, and re-layouts  16.3 us (8%)
  other arithmetic  15.6 us (8%)
  blocking collectives  10.6 us (5%)
  matrix products  5.63 us (3%)
    ppermute x27, waiting for transfers between devices, moved(): lax.ppermute(array, axis, [(i, (i + step) % length) for i in range(length)])  71.9 us
    ppermute x27, starting transfers between devices, moved(): lax.ppermute(array, axis, [(i, (i + step) % length) for i in range(length)])  44.5 us
    all_to_all x3, starting transfers between devices, spread(): return lax.all_to_all(blocks, axis, 0, 0, tiled=True)  18.7 us
    all_to_all x3, waiting for transfers between devices, spread(): return lax.all_to_all(blocks, axis, 0, 0, tiled=True)  13.3 us
    all_to_all x1, blocking collectives, spread(): return lax.all_to_all(blocks, axis, 0, 0, tiled=True)  10.6 us
    dot_general x7, matrix products, dot(): lax.dot_general(left, right, (dims, ((), ())), preferred_element_type=F32)  5.63 us
    convert_element_type x4, other arithmetic, sum_for_owner(): return total.astype(BF16)  4.32 us
  transfers between devices with their start and end apart: 33, of which 14 were waited for; matrix products, arithmetic and copies ran while one was open for 10% of the time, Pallas kernels for 0%

commit v1 on v0

v1 whole, which is shorter than its diff:
```python
import functools
import math

import jax
import jax.numpy as jnp
from jax import lax
from jax.experimental import pallas as pl
from jax.experimental.pallas import tpu as pltpu
from jax.sharding import Mesh
from jax.sharding import PartitionSpec as P


BF16 = jnp.bfloat16
F32 = jnp.float32
FS = ("z", "y")
TP = ("x", "c")
ALL = ("z", "y", "x", "c")


def spread(blocks, axis):
    return lax.all_to_all(blocks, axis, 0, 0, tiled=True)


def swapped(array):
    return lax.ppermute(array, "c", [(0, 1), (1, 0)])


def moved(array, axis, step):
    length = lax.axis_size(axis)
    return lax.ppermute(array, axis, [(i, (i + step) % length) for i in range(length)])


def around(array, axis):
    return [array] + [moved(array, axis, -step) for step in range(1, lax.axis_size(axis))]


def sum_for_owner(blocks, axis):
    total = blocks[0].astype(F32)
    for step in range(1, len(blocks)):
        total = total + moved(blocks[step], axis, step).astype(F32)
    return total.astype(BF16)


def dot(left, right, dims):
    return lax.dot_general(left, right, (dims, ((), ())), preferred_element_type=F32)


LANES = 128


def whole(kernel, out_shape, scratch=(), flops=0, moved_bytes=0):
    return pl.pallas_call(
        kernel,
        out_shape=out_shape,
        scratch_shapes=scratch,
        cost_estimate=pl.CostEstimate(flops=flops, bytes_accessed=moved_bytes, transcendentals=0),
    )


def like(shape, kind):
    return jax.ShapeDtypeStruct(shape, kind)


def exchange_lanes(left, right):
    half = LANES // 2
    lane = lax.broadcasted_iota(jnp.int32, left.shape, 1)
    low = jnp.where(lane < half, left, pltpu.roll(right, half, 1))
    high = jnp.where(lane < half, pltpu.roll(left, half, 1), right)
    return low, high


def pack_kernel(copies, part, pad, gate, up, down, out):
    both = jnp.concatenate((gate[...], up[...]), axis=0).astype(F32).T
    tall = down[...].astype(F32)
    half = pad // 2
    shard = tall.shape[1]
    for y in range(tall.shape[0] // part):
        top = both[y * part : (y + 1) * part]
        piece = tall[y * part : (y + 1) * part]
        first, second = piece[:half], piece[half:]
        second = jnp.concatenate((second, jnp.zeros((pad - part, shard), F32)))
        low = jnp.concatenate((first, second), axis=1)
        block = jnp.concatenate((top, jnp.zeros((pad - part, LANES), F32), low)).astype(BF16)
        for z in range(copies):
            out[z * (tall.shape[0] // part) + y] = block


def turned(array, outer, inner, rows):
    return jnp.concatenate(
        [
            array[(o * inner + i) * rows : (o * inner + i + 1) * rows]
            for i in range(inner)
            for o in range(outer)
        ]
    )


def backward_kernel(ny, nx, rows, pad, own, other, *refs):
    firsts, seconds = refs[:ny], refs[ny : ny + nx]
    kept, sent, gate_up, down, grads, prev, cotangent = refs[ny + nx :]
    width = prev.shape[1]
    half = pad // 2
    for base, packed in ((0, own), (pad, other)):
        for tile in range(packed.shape[0] // 2):
            at = pl.ds(tile * LANES, LANES)
            low, high = exchange_lanes(packed[2 * tile].astype(F32), packed[2 * tile + 1].astype(F32))
            gate_up[pl.ds(base, pad), at] = low[:pad].astype(BF16)
            gate_up[pl.ds(2 * pad + base, pad), at] = high[:pad].astype(BF16)
            down[pl.ds(base, half), at] = low[pad:].astype(BF16)
            down[pl.ds(base + half, half), at] = high[pad:].astype(BF16)
    for k in range(ny):
        prev[pl.ds(k * nx * rows, nx * rows)] = firsts[k][:, :width]
    for k in range(nx):
        cotangent[pl.ds(k * ny * rows, ny * rows)] = seconds[k][:, :width]
    pre = dot(prev[...], gate_up[...], ((1,), (1,)))
    gate_prev, up_prev = pre[:, : 2 * pad], pre[:, 2 * pad :]
    grad_hidden = turned(dot(cotangent[...], down[...], ((1,), (1,))), nx, ny, rows)
    sig = jax.nn.sigmoid(gate_prev)
    silu = gate_prev * sig
    grad_gate = grad_hidden * up_prev * sig * (1.0 + gate_prev * (1.0 - sig))
    grad_up = grad_hidden * silu
    hidden_prev = turned(silu * up_prev, ny, nx, rows)
    grads[:, : 2 * pad] = grad_gate.astype(BF16)
    grads[:, 2 * pad :] = grad_up.astype(BF16)
    for k, (value, tokens) in enumerate(((grad_gate, prev), (grad_up, prev), (hidden_prev, cotangent))):
        term = dot(value.astype(BF16).T, tokens[...], ((1,), (0,)))
        kept[pl.ds(k * pad, pad)] = term[:pad]
        sent[pl.ds(k * pad, pad)] = term[pad:].astype(BF16)


def pair_kernel(pad, kept, received, out):
    half = pad // 2
    for tile in range(out.shape[0] // 2):
        at = pl.ds(tile * LANES, LANES)
        total = kept[:, at] + received[:, at].astype(F32)
        left = jnp.concatenate((total[:pad], total[2 * pad : 2 * pad + half]))
        right = jnp.concatenate((total[pad : 2 * pad], total[2 * pad + half :]))
        even, odd = exchange_lanes(left, right)
        out[2 * tile] = even.astype(BF16)
        out[2 * tile + 1] = odd.astype(BF16)


def update_kernel(ny, part, pad, factor, arrived, gate, up, down, new_gate, new_up, new_down):
    half = pad // 2
    shard = down.shape[1]
    tops = []
    for y in range(ny):
        total = arrived[y].astype(F32)
        for z in range(1, arrived.shape[0] // ny):
            total = total + arrived[z * ny + y].astype(F32)
        tops.append(total[:part])
        low = total[pad:]
        high = pltpu.roll(low, LANES // 2, 1)
        at = y * part
        new_down[at : at + half] = down[at : at + half] + factor * low[:, :shard]
        rest = part - half
        new_down[at + half : at + part] = down[at + half : at + part] + factor * high[:rest, :shard]
    both = jnp.concatenate(tops).T
    new_gate[...] = gate[...] + factor * both[:shard]
    new_up[...] = up[...] + factor * both[shard:]


def forward_kernel(ny, nx, rows, pad, gate_up, down, *refs):
    firsts, seconds = refs[:ny], refs[ny : ny + nx]
    hidden, outs, tokens = refs[ny + nx], refs[ny + nx + 1 : -1], refs[-1]
    half = tokens.shape[1]
    width = gate_up.shape[1]
    for k in range(ny):
        tokens[pl.ds(k * nx * rows, nx * rows)] = firsts[k][:, width:]
    pre = dot(tokens[...], gate_up[:, :half], ((1,), (1,)))
    for k in range(nx):
        tokens[pl.ds(k * ny * rows, ny * rows)] = seconds[k][:, width:]
    pre = pre + turned(dot(tokens[...], gate_up[:, half:], ((1,), (1,))), nx, ny, rows)
    value = (jax.nn.silu(pre[:, : 2 * pad]) * pre[:, 2 * pad :]).astype(BF16)
    hidden[...] = value
    total = dot(value, down[...], ((1,), (0,)))
    for k in range(ny):
        outs[k][...] = total[k * nx * rows : (k + 1) * nx * rows].astype(BF16)


def layer(x_next, x_prev, grad_out, gate_w, up_w, down_w, acc_gate, acc_up, acc_down):
    rows, width = x_prev.shape
    nz, ny, nx, nc = (lax.axis_size(name) for name in ALL)
    group = ny * nx * rows
    factor = 1.0 / math.sqrt(rows * nz * ny * nx * nc)
    _, units = gate_w.shape
    part = units // ny
    pad = -(-part // 32) * 32
    tall = pad + pad // 2
    core = lax.axis_index("c")

    half = width // 2
    first = jnp.concatenate((x_prev, x_next[:, :half]), axis=1)
    second = jnp.concatenate((grad_out, x_next[:, half:]), axis=1)
    first = around(first, "x")
    second = around(second, "y")
    first = jnp.stack(first).reshape(nx * rows, width + half)
    second = jnp.stack(second).reshape(ny * rows, width + half)
    firsts = around(first, "y")
    seconds = around(second, "x")

    packed = whole(
        functools.partial(pack_kernel, nz, part, pad), like((nz * ny, tall, LANES), BF16)
    )(gate_w, up_w, down_w)
    own = spread(packed, FS)
    other = swapped(own)

    token_ops = 2 * group * 2 * pad * width
    kept, sent, gate_up, down, grads = whole(
        functools.partial(backward_kernel, ny, nx, rows, pad),
        (
            like((3 * pad, width), F32),
            like((3 * pad, width), BF16),
            like((4 * pad, width), BF16),
            like((2 * pad, width), BF16),
            like((group, 4 * pad), BF16),
        ),
        (pltpu.VMEM((group, width), BF16), pltpu.VMEM((group, width), BF16)),
        flops=6 * token_ops,
        moved_bytes=12 * group * width,
    )(own, other, *firsts, *seconds)
    received = swapped(sent)
    paired = whole(
        functools.partial(pair_kernel, pad), like((nz * ny, tall, LANES), BF16)
    )(kept, received)
    arrived = spread(paired, FS)
    new_gate, new_up, new_down = whole(
        functools.partial(update_kernel, ny, part, pad, factor),
        (like(acc_gate.shape, F32), like(acc_up.shape, F32), like(acc_down.shape, F32)),
    )(arrived, acc_gate, acc_up, acc_down)

    input_part = dot(grads, gate_up, ((1,), (0,))).astype(BF16).reshape(ny, nx, rows, width)
    by_x = sum_for_owner([input_part[:, k] for k in range(nx)], "x")
    grad_input = sum_for_owner([by_x[k] for k in range(ny)], "y")

    hidden, *out_part = whole(
        functools.partial(forward_kernel, ny, nx, rows, pad),
        (like((group, 2 * pad), BF16), *(like((nx * rows, width), BF16) for _ in range(ny))),
        (pltpu.VMEM((group, half), BF16),),
        flops=3 * token_ops,
        moved_bytes=6 * group * width,
    )(gate_up, down, *firsts, *seconds)
    by_y = sum_for_owner(out_part, "y").reshape(nx, rows, width)
    out_next = sum_for_owner([by_y[k] for k in range(nx)], "x")

    partner = swapped(hidden[:, pad : pad + part])
    pair = jnp.stack((hidden[:, :part], partner)).reshape(nc, ny, nx, rows, part)
    back = [pair[:, 0]] + [moved(pair[:, step], "y", step) for step in range(1, ny)]
    saved = jnp.stack([back[-step % ny] for step in range(ny)])
    saved = jnp.roll(saved, (lax.axis_index("y"), lax.axis_index("x")), (0, 2))
    saved = jnp.where(core == 0, saved, saved[:, ::-1])
    saved = saved.transpose(2, 1, 3, 0, 4).reshape(nx * nc * rows, units)
    return out_next, saved, grad_input, new_gate, new_up, new_down


def solution(mesh):
    split = Mesh(mesh.devices.reshape(8, 4, 4, 2), ALL)
    tokens = P(ALL, None)
    wide, tall = P(FS, TP), P(TP, FS)
    in_specs = (tokens, tokens, tokens, wide, wide, tall, wide, wide, tall)
    out_specs = (tokens, wide, tokens, wide, wide, tall)
    return jax.shard_map(layer, mesh=split, in_specs=in_specs, out_specs=out_specs, check_vma=False)
```

time: 202 us -> 191 us (0.946); the launches traced: 198 us -> 189 us
  Pallas kernels: 0 us -> 22.9 us
  blocking collectives: 10.6 us -> 0 us
  other arithmetic: 15.6 us -> 6.38 us
  local copies, waits for them, and re-layouts: 16.3 us -> 10.3 us
  waiting for transfers between devices: 85.2 us -> 80.8 us
  matrix products: 5.63 us -> 2.49 us
    pallas_call x0 -> x5, Pallas kernels: none -> 22.9 us  [the longest x1 9.18 us: layer(): whole(functools.partial(backward_kernel, ny, nx, rows, pad), (like((3 * p...]
    all_to_all x1 -> x0, blocking collectives: 10.6 us -> none  [spread(): return lax.all_to_all(blocks, axis, 0, 0, tiled=True)]
    ppermute x27, waiting for transfers between devices: 71.9 us -> 63 us  [moved(): lax.ppermute(array, axis, [(i, (i + step) % length) for i in range(length)])]
    another operation x6 -> x4, other arithmetic: 6.36 us -> 1.84 us  [the longest x2 1.74 us: layer(): first = jnp.stack(first).reshape(nx * rows, width + half)]
    all_to_all x3 -> x2, waiting for transfers between devices: 13.3 us -> 17.8 us  [spread(): return lax.all_to_all(blocks, axis, 0, 0, tiled=True)]
    unnamed x30 -> x32, local copies, waits for them, and re-layouts: 2.95 us -> 7.13 us
    dot_general x7 -> x1, matrix products: 5.63 us -> 2.49 us  [dot(): lax.dot_general(left, right, (dims, ((), ())), preferred_element_type=F32)]
    another operation x3 -> x0, local copies, waits for them, and re-layouts: 2.67 us -> none  [layer(): mine = jnp.stack((gate_w.T, up_w.T, down_w)).reshape(3, ny, part, shard)]
  transfers between devices with their start and end apart: 33 -> 32, of which waited for: 14 -> 17; matrix products, arithmetic and copies ran while one was open for 10% -> 7% of each run, Pallas kernels for 0% -> 5%
where the time goes in v1:
time: 191 us; the launch traced here: 189 us
  waiting for transfers between devices  80.8 us (42%)
  starting transfers between devices  65.2 us (34%)
  Pallas kernels  22.9 us (12%)
  local copies, waits for them, and re-layouts  10.3 us (5%)
  other arithmetic  6.38 us (3%)
  matrix products  2.49 us (1%)
    ppermute x27, waiting for transfers between devices, moved(): lax.ppermute(array, axis, [(i, (i + step) % length) for i in range(length)])  63 us
    ppermute x27, starting transfers between devices, moved(): lax.ppermute(array, axis, [(i, (i + step) % length) for i in range(length)])  44.8 us
    all_to_all x2, starting transfers between devices, spread(): return lax.all_to_all(blocks, axis, 0, 0, tiled=True)  19.8 us
    all_to_all x2, waiting for transfers between devices, spread(): return lax.all_to_all(blocks, axis, 0, 0, tiled=True)  17.8 us
    pallas_call x1, Pallas kernels, layer(): whole(functools.partial(backward_kernel, ny, nx, rows, pad), (like((3 * p...  9.18 us
    unnamed x32, local copies, waits for them, and re-layouts  7.13 us
    pallas_call x1, Pallas kernels, layer(): whole(functools.partial(forward_kernel, ny, nx, rows, pad), (like((group,...  5.63 us
    convert_element_type x4, other arithmetic, sum_for_owner(): return total.astype(BF16)  4.31 us
  transfers between devices with their start and end apart: 32, of which 17 were waited for; matrix products, arithmetic and copies ran while one was open for 7% of the time, Pallas kernels for 5%

profile of v1, /device:TPU:64, one launch (start us, length us, event | category | flops | bytes accessed | tf_op | source)
XLA Modules:
  0.0 189.0 jit_solution(3947982046797348650)
XLA Ops:
  0.6 1.5 copy.15.down
  2.2 2.2 %shard_map.136 = bf16[32,144,128]{2,1,0:T(8,128)(2,1)} custom-call(bf16[64,352]{1,0:T(8,128)(2,1)} %gate.2, bf16[64,352]{1,0:T(8,128)(2,1)} %up.2, bf16[352,64]{1,0:T(8,128)(2,1)} %copy.15.down), custom_call_target="tpu_custom_call" | custom-call | tf_op jit(solution)/shard_map/pallas_call | solution.py:202
  4.4 11.0 %all-to-all-start = ((bf16[32,144,128]{2,1,0:T(8,128)(2,1)}), bf16[32,144,128]{2,1,0:T(8,128)(2,1)S(1)}, u32[]{:S(2)}, u32[]{:S(2)}) async-start(bf16[32,144,128]{2,1,0:T(8,128)(2,1)} %shard_map.136), calls=%async_computation | async-start | bytes 2359296 | tf_op jit(solution)/shard_map/all_to_all | solution.py:21
  15.5 2.8 %collective-permute-start.7 = (bf16[24,3072]{1,0:T(8,128)(2,1)S(1)}, bf16[24,3072]{1,0:T(8,128)(2,1)S(1)}, u32[]{:S(2)}, u32[]{:S(2)}) collective-permute-start(bf16[24,3072]{1,0:T(8,128)(2,1)S(1)} %get-tuple-element.53), channel_id=1, source_target_pairs={{0,24},{8,0},{16,8},{24,16},{1,25},{9,1},{17,9},{25,17},{2,26},{10... | collective-permute-start | bytes 442376 | tf_op jit(solution)/shard_map/ppermute | solution.py:30
  20.7 2.8 %collective-permute-start.1 = (bf16[24,3072]{1,0:T(8,128)(2,1)S(1)}, bf16[24,3072]{1,0:T(8,128)(2,1)S(1)}, u32[]{:S(2)}, u32[]{:S(2)}) collective-permute-start(bf16[24,3072]{1,0:T(8,128)(2,1)S(1)} %get-tuple-element.55), channel_id=1, source_target_pairs={{0,6},{2,0},{4,2},{6,4},{1,7},{3,1},{5,3},{7,5},{8,14},{10,8},{12,... | collective-permute-start | bytes 442376 | tf_op jit(solution)/shard_map/ppermute | solution.py:30
  23.4 6.2 %collective-permute-done.7 = bf16[24,3072]{1,0:T(8,128)(2,1)S(1)} collective-permute-done((bf16[24,3072]{1,0:T(8,128)(2,1)S(1)}, bf16[24,3072]{1,0:T(8,128)(2,1)S(1)}, u32[]{:S(2)}, u32[]{:S(2)}) %collective-permute-start.7) | collective-permute-done | bytes 147488 | tf_op jit(solution)/shard_map/ppermute | solution.py:30
  29.6 5.2 %collective-permute-done.9 = bf16[24,3072]{1,0:T(8,128)(2,1)S(1)} collective-permute-done((bf16[24,3072]{1,0:T(8,128)(2,1)S(1)}, bf16[24,3072]{1,0:T(8,128)(2,1)S(1)}, u32[]{:S(2)}, u32[]{:S(2)}) %collective-permute-start.9) | collective-permute-done | bytes 147488 | tf_op jit(solution)/shard_map/ppermute | solution.py:30
  34.9 2.8 %collective-permute-start.10 = (bf16[96,3072]{1,0:T(8,128)(2,1)S(1)}, bf16[96,3072]{1,0:T(8,128)(2,1)S(1)}, u32[]{:S(2)}, u32[]{:S(2)}) collective-permute-start(bf16[96,3072]{1,0:T(8,128)(2,1)S(1)} %bitcast.78), channel_id=1, source_target_pairs={{0,6},{2,0},{4,2},{6,4},{1,7},{3,1},{5,3},{7,5},{8,14},{10,8},{12,... | collective-permute-start | bytes 1769480 | tf_op jit(solution)/shard_map/ppermute | solution.py:30
  38.5 7.8 %all-to-all-done.own = bf16[32,144,128]{2,1,0:T(8,128)(2,1)S(1)} async-done(((bf16[32,144,128]{2,1,0:T(8,128)(2,1)}), bf16[32,144,128]{2,1,0:T(8,128)(2,1)S(1)}, u32[]{:S(2)}, u32[]{:S(2)}) %all-to-all-start) | async-done | bytes 1179680 | tf_op jit(solution)/shard_map/all_to_all | solution.py:21
  46.3 3.0 %collective-permute-start.2 = (bf16[24,3072]{1,0:T(8,128)(2,1)S(1)}, bf16[24,3072]{1,0:T(8,128)(2,1)S(1)}, u32[]{:S(2)}, u32[]{:S(2)}) collective-permute-start(bf16[24,3072]{1,0:T(8,128)(2,1)S(1)} %get-tuple-element.55), channel_id=1, source_target_pairs={{0,4},{2,6},{4,0},{6,2},{1,5},{3,7},{5,1},{7,3},{8,12},{10,14},{12... | collective-permute-start | bytes 442376 | tf_op jit(solution)/shard_map/ppermute | solution.py:30
  49.9 8.7 %collective-permute-done.2 = bf16[24,3072]{1,0:T(8,128)(2,1)S(1)} collective-permute-done((bf16[24,3072]{1,0:T(8,128)(2,1)S(1)}, bf16[24,3072]{1,0:T(8,128)(2,1)S(1)}, u32[]{:S(2)}, u32[]{:S(2)}) %collective-permute-start.2) | collective-permute-done | bytes 147488 | tf_op jit(solution)/shard_map/ppermute | solution.py:30
  58.6 9.7 %collective-permute-start.12 = (bf16[96,3072]{1,0:T(8,128)(2,1)S(1)}, bf16[96,3072]{1,0:T(8,128)(2,1)}, u32[]{:S(2)}, u32[]{:S(2)}) collective-permute-start(bf16[96,3072]{1,0:T(8,128)(2,1)S(1)} %bitcast.80), channel_id=1, source_target_pairs={{0,2},{2,4},{4,6},{6,0},{1,3},{3,5},{5,7},{7,1},{8,10},{10,12},{12... | collective-permute-start | bytes 1769480 | tf_op jit(solution)/shard_map/ppermute | solution.py:30
  68.4 1.1 pad_maximum_fusion
  69.7 2.2 %collective-permute-start.6 = (bf16[96,3072]{1,0:T(8,128)(2,1)S(1)}, bf16[96,3072]{1,0:T(8,128)(2,1)}, u32[]{:S(2)}, u32[]{:S(2)}) collective-permute-start(bf16[96,3072]{1,0:T(8,128)(2,1)S(1)} %bitcast.85), channel_id=1, source_target_pairs={{0,8},{8,16},{16,24},{24,0},{1,9},{9,17},{17,25},{25,1},{2,10},{10... | collective-permute-start | bytes 1769480 | tf_op jit(solution)/shard_map/ppermute | solution.py:30
  71.8 1.7 copy.24.down
  73.5 7.8 %collective-permute-done.12.refs_7_ = bf16[96,3072]{1,0:T(8,128)(2,1)} collective-permute-done((bf16[96,3072]{1,0:T(8,128)(2,1)S(1)}, bf16[96,3072]{1,0:T(8,128)(2,1)}, u32[]{:S(2)}, u32[]{:S(2)}) %collective-permute-start.12) | collective-permute-done | bytes 589856 | tf_op jit(solution)/shard_map/ppermute | solution.py:30
  81.4 4.5 %collective-permute-done.4.refs_1_ = bf16[96,3072]{1,0:T(8,128)(2,1)} collective-permute-done((bf16[96,3072]{1,0:T(8,128)(2,1)S(1)}, bf16[96,3072]{1,0:T(8,128)(2,1)}, u32[]{:S(2)}, u32[]{:S(2)}) %collective-permute-start.4) | collective-permute-done | bytes 589856 | tf_op jit(solution)/shard_map/ppermute | solution.py:30
  85.8 1.7 collective-permute-done.5.refs_2_
  87.5 10.5 %collective-permute-done.6.refs_3_ = bf16[96,3072]{1,0:T(8,128)(2,1)} collective-permute-done((bf16[96,3072]{1,0:T(8,128)(2,1)S(1)}, bf16[96,3072]{1,0:T(8,128)(2,1)}, u32[]{:S(2)}, u32[]{:S(2)}) %collective-permute-start.6) | collective-permute-done | bytes 589856 | tf_op jit(solution)/shard_map/ppermute | solution.py:30
  98.0 9.2 %shard_map.137 = (f32[288,2048]{1,0:T(8,128)}, bf16[288,2048]{1,0:T(8,128)(2,1)}, bf16[384,2048]{1,0:T(8,128)(2,1)}, bf16[192,2048]{1,0:T(8,128)(2,1)}, bf16[384,384]{1,0:T(8,128)(2,1)}) custom-call(bf16[32,144,128]{2,1,0:T(8,128)(2,1)} %copy-done.2, bf16[32,144,128]{2,1,0:T(8,128)(2,1)} %collective-permute-done.other, bf16[96,3072]{1,0:T(8,128)(2,1)} %bitcast.86, ...), custom_call_target="tpu_custom_call" | custom-call | flops 1811939328 | bytes 9437184 | tf_op jit(solution)/shard_map/pallas_call | solution.py:209
  107.2 2.5 %convolution_convert_fusion = bf16[384,2048]{1,0:T(8,128)(2,1)S(1)} fusion(bf16[384,384]{1,0:T(8,128)(2,1)} %get-tuple-element.26, bf16[384,2048]{1,0:T(8,128)(2,1)} %get-tuple-element.19.gate_up), kind=kOutput, calls=%fused_computation | convolution fusion | flops 604766208 | bytes 3440640 | tf_op jit(solution)/shard_map/dot_general | solution.py:45
  109.7 5.6 %shard_map.138 = (bf16[384,192]{1,0:T(8,128)(2,1)}, bf16[96,2048]{1,0:T(8,128)(2,1)}, bf16[96,2048]{1,0:T(8,128)(2,1)}, bf16[96,2048]{1,0:T(8,128)(2,1)}, bf16[96,2048]{1,0:T(8,128)(2,1)}) custom-call(bf16[384,2048]{1,0:T(8,128)(2,1)} %get-tuple-element.19.gate_up, bf16[192,2048]{1,0:T(8,128)(2,1)} %get-tuple-element.20.down, bf16[96,3072]{1,0:T(8,128)(2,1)} %bitcast.87, ...), custom_call_target="tpu_custom_call" | custom-call | flops 905969664 | bytes 4718592 | tf_op jit(solution)/shard_map/pallas_call | solution.py:236
  115.3 1.1 fusion.18
  117.0 1.0 slice_bitcast_fusion.2
  118.3 1.8 collective-permute-start.24
  120.1 2.3 %collective-permute-start.25 = (bf16[4,24,2048]{2,1,0:T(8,128)(2,1)S(1)}, bf16[4,24,2048]{2,1,0:T(8,128)(2,1)}, u32[]{:S(2)}, u32[]{:S(2)}) collective-permute-start(bf16[4,24,2048]{2,1,0:T(8,128)(2,1)S(1)} %get-tuple-element.40), channel_id=1, source_target_pairs={{0,6},{2,0},{4,2},{6,4},{1,7},{3,1},{5,3},{7,5},{8,14},{10,8},{12,... | collective-permute-start | bytes 1179656 | tf_op jit(solution)/shard_map/ppermute | solution.py:30
  122.5 1.1 collective-permute-start.20
  123.6 3.0 %collective-permute-done.20 = bf16[2,4,24,88]{3,2,1,0:T(8,128)(2,1)S(1)} collective-permute-done((bf16[2,4,24,88]{3,2,1,0:T(8,128)(2,1)S(1)}, bf16[2,4,24,88]{3,2,1,0:T(8,128)(2,1)S(1)}, u32[]{:S(2)}, u32[]{:S(2)}) %collective-permute-start.20) | collective-permute-done | bytes 33824 | tf_op jit(solution)/shard_map/ppermute | solution.py:30
  127.1 5.1 %collective-permute-done.21 = bf16[2,4,24,88]{3,2,1,0:T(8,128)(2,1)S(1)} collective-permute-done((bf16[2,4,24,88]{3,2,1,0:T(8,128)(2,1)S(1)}, bf16[2,4,24,88]{3,2,1,0:T(8,128)(2,1)S(1)}, u32[]{:S(2)}, u32[]{:S(2)}) %collective-permute-start.21) | collective-permute-done | bytes 33824 | tf_op jit(solution)/shard_map/ppermute | solution.py:30
  132.2 5.3 %collective-permute-done.22 = bf16[2,4,24,88]{3,2,1,0:T(8,128)(2,1)S(1)} collective-permute-done((bf16[2,4,24,88]{3,2,1,0:T(8,128)(2,1)S(1)}, bf16[2,4,24,88]{3,2,1,0:T(8,128)(2,1)S(1)}, u32[]{:S(2)}, u32[]{:S(2)}) %collective-permute-start.22) | collective-permute-done | bytes 33824 | tf_op jit(solution)/shard_map/ppermute | solution.py:30
  139.0 2.6 %collective-permute-start.14 = (bf16[96,2048]{1,0:T(8,128)(2,1)}, bf16[96,2048]{1,0:T(8,128)(2,1)}, u32[]{:S(2)}, u32[]{:S(2)}) collective-permute-start(bf16[96,2048]{1,0:T(8,128)(2,1)} %get-tuple-element.23), channel_id=1, source_target_pairs={{0,16},{8,24},{16,0},{24,8},{1,17},{9,25},{17,1},{25,9},{2,18},{10... | collective-permute-start | bytes 1179656 | tf_op jit(solution)/shard_map/ppermute | solution.py:30
  142.2 1.5 fusion.2
  143.6 1.0 copy-done.6
  144.7 3.5 %shard_map.139 = bf16[32,144,128]{2,1,0:T(8,128)(2,1)} custom-call(f32[288,2048]{1,0:T(8,128)} %get-tuple-element.27.kept, bf16[288,2048]{1,0:T(8,128)(2,1)} %copy-done.6), custom_call_target="tpu_custom_call" | custom-call | tf_op jit(solution)/shard_map/pallas_call | solution.py:223
  148.2 8.8 %all-to-all-start.1 = ((bf16[32,144,128]{2,1,0:T(8,128)(2,1)}), bf16[32,144,128]{2,1,0:T(8,128)(2,1)S(1)}, u32[]{:S(2)}, u32[]{:S(2)}) async-start(bf16[32,144,128]{2,1,0:T(8,128)(2,1)} %shard_map.139), calls=%async_computation.1 | async-start | bytes 2359296 | tf_op jit(solution)/shard_map/all_to_all | solution.py:21
  157.0 1.5 collective-permute-start.26
  158.6 2.7 %collective-permute-start.27 = (bf16[24,2048]{1,0:T(8,128)(2,1)S(1)}, bf16[24,2048]{1,0:T(8,128)(2,1)S(1)}, u32[]{:S(2)}, u32[]{:S(2)}) collective-permute-start(bf16[24,2048]{1,0:T(8,128)(2,1)S(1)} %get-tuple-element.43), channel_id=1, source_target_pairs={{0,16},{8,24},{16,0},{24,8},{1,17},{9,25},{17,1},{25,9},{2,18},{10... | collective-permute-start | bytes 294920 | tf_op jit(solution)/shard_map/ppermute | solution.py:30
  161.3 1.5 collective-permute-start.28
  162.7 1.1 collective-permute-done.15
  163.8 1.5 add_convert_fusion
  166.2 2.5 %collective-permute-start.18 = (bf16[24,2048]{1,0:T(8,128)(2,1)S(1)}, bf16[24,2048]{1,0:T(8,128)(2,1)S(1)}, u32[]{:S(2)}, u32[]{:S(2)}) collective-permute-start(bf16[24,2048]{1,0:T(8,128)(2,1)S(1)} %get-tuple-element.45), channel_id=1, source_target_pairs={{0,6},{2,0},{4,2},{6,4},{1,7},{3,1},{5,3},{7,5},{8,14},{10,8},{12,... | collective-permute-start | bytes 294920 | tf_op jit(solution)/shard_map/ppermute | solution.py:30
  168.7 0.9 collective-permute-done.28
  170.3 2.0 %collective-permute-done.16 = bf16[24,2048]{1,0:T(8,128)(2,1)S(1)} collective-permute-done((bf16[24,2048]{1,0:T(8,128)(2,1)S(1)}, bf16[24,2048]{1,0:T(8,128)(2,1)S(1)}, u32[]{:S(2)}, u32[]{:S(2)}) %collective-permute-start.16) | collective-permute-done | bytes 98336 | tf_op jit(solution)/shard_map/ppermute | solution.py:30
  172.3 0.9 collective-permute-done.18
  173.9 10.0 %all-to-all-done.1.arrived = bf16[32,144,128]{2,1,0:T(8,128)(2,1)S(1)} async-done(((bf16[32,144,128]{2,1,0:T(8,128)(2,1)}), bf16[32,144,128]{2,1,0:T(8,128)(2,1)S(1)}, u32[]{:S(2)}, u32[]{:S(2)}) %all-to-all-start.1) | async-done | bytes 1179680 | tf_op jit(solution)/shard_map/all_to_all | solution.py:21
  183.9 1.1 copy-done.3
  185.0 2.3 %shard_map.140 = (f32[64,352]{1,0:T(8,128)}, f32[64,352]{1,0:T(8,128)}, f32[352,64]{1,0:T(8,128)}) custom-call(bf16[32,144,128]{2,1,0:T(8,128)(2,1)} %copy-done.3, f32[64,352]{1,0:T(8,128)} %gate.3, f32[64,352]{1,0:T(8,128)} %up.3, f32[352,64]{1,0:T(8,128)} %copy.24.down), custom_call_target="tpu_custom_call" | custom-call | tf_op jit(solution)/shard_map/pallas_call | solution.py:227
  187.3 1.7 copy.25
  (76 shorter events, 9.9 us)
Async XLA Ops:
  2.2 13.3 %copy-start.11 = (bf16[24,2048]{1,0:T(8,128)(2,1)S(1)}, bf16[24,2048]{1,0:T(8,128)(2,1)}, u32[]{:S(2)}) copy-start(bf16[24,2048]{1,0:T(8,128)(2,1)} %param.9) | copy-start | bytes 294916
  4.4 11.1 %copy-start.9 = (bf16[24,2048]{1,0:T(8,128)(2,1)S(1)}, bf16[24,2048]{1,0:T(8,128)(2,1)}, u32[]{:S(2)}) copy-start(bf16[24,2048]{1,0:T(8,128)(2,1)} %param.11) | copy-start | bytes 294916
  4.4 15.6 %copy-start.10 = (bf16[24,2048]{1,0:T(8,128)(2,1)S(1)}, bf16[24,2048]{1,0:T(8,128)(2,1)}, u32[]{:S(2)}) copy-start(bf16[24,2048]{1,0:T(8,128)(2,1)} %param.10) | copy-start | bytes 294916
  4.4 41.9 %all-to-all-start = ((bf16[32,144,128]{2,1,0:T(8,128)(2,1)}), bf16[32,144,128]{2,1,0:T(8,128)(2,1)S(1)}, u32[]{:S(2)}, u32[]{:S(2)}) async-start(bf16[32,144,128]{2,1,0:T(8,128)(2,1)} %shard_map.136), calls=%async_computation | async-start | bytes 2359296 | tf_op jit(solution)/shard_map/all_to_all | solution.py:21
  15.5 14.1 %collective-permute-start.7 = (bf16[24,3072]{1,0:T(8,128)(2,1)S(1)}, bf16[24,3072]{1,0:T(8,128)(2,1)S(1)}, u32[]{:S(2)}, u32[]{:S(2)}) collective-permute-start(bf16[24,3072]{1,0:T(8,128)(2,1)S(1)} %get-tuple-element.53), channel_id=1, source_target_pairs={{0,24},{8,0},{16,8},{24,16},{1,25},{9,1},{17,9},{25,17},{2,26},{10... | collective-permute-start | bytes 442376 | tf_op jit(solution)/shard_map/ppermute | solution.py:30
  18.3 11.3 %collective-permute-start.8 = (bf16[24,3072]{1,0:T(8,128)(2,1)S(1)}, bf16[24,3072]{1,0:T(8,128)(2,1)S(1)}, u32[]{:S(2)}, u32[]{:S(2)}) collective-permute-start(bf16[24,3072]{1,0:T(8,128)(2,1)S(1)} %get-tuple-element.53), channel_id=1, source_target_pairs={{0,16},{8,24},{16,0},{24,8},{1,17},{9,25},{17,1},{25,9},{2,18},{10... | collective-permute-start | bytes 442376 | tf_op jit(solution)/shard_map/ppermute | solution.py:30
  19.1 15.7 %collective-permute-start.9 = (bf16[24,3072]{1,0:T(8,128)(2,1)S(1)}, bf16[24,3072]{1,0:T(8,128)(2,1)S(1)}, u32[]{:S(2)}, u32[]{:S(2)}) collective-permute-start(bf16[24,3072]{1,0:T(8,128)(2,1)S(1)} %get-tuple-element.53), channel_id=1, source_target_pairs={{0,8},{8,16},{16,24},{24,0},{1,9},{9,17},{17,25},{25,1},{2,10},{10... | collective-permute-start | bytes 442376 | tf_op jit(solution)/shard_map/ppermute | solution.py:30
  20.7 28.6 %collective-permute-start.1 = (bf16[24,3072]{1,0:T(8,128)(2,1)S(1)}, bf16[24,3072]{1,0:T(8,128)(2,1)S(1)}, u32[]{:S(2)}, u32[]{:S(2)}) collective-permute-start(bf16[24,3072]{1,0:T(8,128)(2,1)S(1)} %get-tuple-element.55), channel_id=1, source_target_pairs={{0,6},{2,0},{4,2},{6,4},{1,7},{3,1},{5,3},{7,5},{8,14},{10,8},{12,... | collective-permute-start | bytes 442376 | tf_op jit(solution)/shard_map/ppermute | solution.py:30
  34.9 63.1 %copy-start = (bf16[4,24,3072]{2,1,0:T(8,128)(2,1)}, bf16[4,24,3072]{2,1,0:T(8,128)(2,1)S(1)}, u32[]{:S(2)}) copy-start(bf16[4,24,3072]{2,1,0:T(8,128)(2,1)S(1)} %pad_maximum_fusion.1) | copy-start | bytes 1769476
  34.9 34.7 %collective-permute-start.10 = (bf16[96,3072]{1,0:T(8,128)(2,1)S(1)}, bf16[96,3072]{1,0:T(8,128)(2,1)S(1)}, u32[]{:S(2)}, u32[]{:S(2)}) collective-permute-start(bf16[96,3072]{1,0:T(8,128)(2,1)S(1)} %bitcast.78), channel_id=1, source_target_pairs={{0,6},{2,0},{4,2},{6,4},{1,7},{3,1},{5,3},{7,5},{8,14},{10,8},{12,... | collective-permute-start | bytes 1769480 | tf_op jit(solution)/shard_map/ppermute | solution.py:30
  37.7 31.9 %collective-permute-start.11 = (bf16[96,3072]{1,0:T(8,128)(2,1)S(1)}, bf16[96,3072]{1,0:T(8,128)(2,1)S(1)}, u32[]{:S(2)}, u32[]{:S(2)}) collective-permute-start(bf16[96,3072]{1,0:T(8,128)(2,1)S(1)} %bitcast.79), channel_id=1, source_target_pairs={{0,4},{2,6},{4,0},{6,2},{1,5},{3,7},{5,1},{7,3},{8,12},{10,14},{12... | collective-permute-start | bytes 1769480 | tf_op jit(solution)/shard_map/ppermute | solution.py:30
  46.3 51.7 %copy-start.2 = (bf16[32,144,128]{2,1,0:T(8,128)(2,1)}, bf16[32,144,128]{2,1,0:T(8,128)(2,1)S(1)}, u32[]{:S(2)}) copy-start(bf16[32,144,128]{2,1,0:T(8,128)(2,1)S(1)} %all-to-all-done.own) | copy-start | bytes 3538948
  46.3 51.7 %collective-permute-start = (bf16[32,144,128]{2,1,0:T(8,128)(2,1)S(1)}, bf16[32,144,128]{2,1,0:T(8,128)(2,1)}, u32[]{:S(2)}, u32[]{:S(2)}) collective-permute-start(bf16[32,144,128]{2,1,0:T(8,128)(2,1)S(1)} %all-to-all-done.own), channel_id=1, source_target_pairs={{0,1},{1,0},{2,3},{3,2},{4,5},{5,4},{6,7},{7,6},{8,9},{9,8},{10,11... | collective-permute-start | bytes 3538952 | tf_op jit(solution)/shard_map/ppermute | solution.py:25
  46.3 12.3 %collective-permute-start.2 = (bf16[24,3072]{1,0:T(8,128)(2,1)S(1)}, bf16[24,3072]{1,0:T(8,128)(2,1)S(1)}, u32[]{:S(2)}, u32[]{:S(2)}) collective-permute-start(bf16[24,3072]{1,0:T(8,128)(2,1)S(1)} %get-tuple-element.55), channel_id=1, source_target_pairs={{0,4},{2,6},{4,0},{6,2},{1,5},{3,7},{5,1},{7,3},{8,12},{10,14},{12... | collective-permute-start | bytes 442376 | tf_op jit(solution)/shard_map/ppermute | solution.py:30
  49.3 19.1 %copy-start.8 = (bf16[24,3072]{1,0:T(8,128)(2,1)}, bf16[24,3072]{1,0:T(8,128)(2,1)S(1)}, u32[]{:S(2)}) copy-start(bf16[24,3072]{1,0:T(8,128)(2,1)S(1)} %collective-permute-done.1) | copy-start | bytes 442372
  49.3 19.1 %collective-permute-start.3 = (bf16[24,3072]{1,0:T(8,128)(2,1)S(1)}, bf16[24,3072]{1,0:T(8,128)(2,1)S(1)}, u32[]{:S(2)}, u32[]{:S(2)}) collective-permute-start(bf16[24,3072]{1,0:T(8,128)(2,1)S(1)} %get-tuple-element.55), channel_id=1, source_target_pairs={{0,2},{2,4},{4,6},{6,0},{1,3},{3,5},{5,7},{7,1},{8,10},{10,12},{12... | collective-permute-start | bytes 442376 | tf_op jit(solution)/shard_map/ppermute | solution.py:30
  58.6 22.7 %collective-permute-start.12 = (bf16[96,3072]{1,0:T(8,128)(2,1)S(1)}, bf16[96,3072]{1,0:T(8,128)(2,1)}, u32[]{:S(2)}, u32[]{:S(2)}) collective-permute-start(bf16[96,3072]{1,0:T(8,128)(2,1)S(1)} %bitcast.80), channel_id=1, source_target_pairs={{0,2},{2,4},{4,6},{6,0},{1,3},{3,5},{5,7},{7,1},{8,10},{10,12},{12... | collective-permute-start | bytes 1769480 | tf_op jit(solution)/shard_map/ppermute | solution.py:30
  69.4 28.5 %copy-start.1 = (bf16[4,24,3072]{2,1,0:T(8,128)(2,1)}, bf16[4,24,3072]{2,1,0:T(8,128)(2,1)S(1)}, u32[]{:S(2)}) copy-start(bf16[4,24,3072]{2,1,0:T(8,128)(2,1)S(1)} %pad_maximum_fusion) | copy-start | bytes 1769476
  69.5 16.4 %collective-permute-start.4 = (bf16[96,3072]{1,0:T(8,128)(2,1)S(1)}, bf16[96,3072]{1,0:T(8,128)(2,1)}, u32[]{:S(2)}, u32[]{:S(2)}) collective-permute-start(bf16[96,3072]{1,0:T(8,128)(2,1)S(1)} %bitcast.83), channel_id=1, source_target_pairs={{0,24},{8,0},{16,8},{24,16},{1,25},{9,1},{17,9},{25,17},{2,26},{10... | collective-permute-start | bytes 1769480 | tf_op jit(solution)/shard_map/ppermute | solution.py:30
  69.6 28.4 %copy-start.4 = (bf16[96,3072]{1,0:T(8,128)(2,1)}, bf16[96,3072]{1,0:T(8,128)(2,1)S(1)}, u32[]{:S(2)}) copy-start(bf16[96,3072]{1,0:T(8,128)(2,1)S(1)} %collective-permute-done.10.refs_5_) | copy-start | bytes 1769476
  69.6 17.9 %collective-permute-start.5 = (bf16[96,3072]{1,0:T(8,128)(2,1)S(1)}, bf16[96,3072]{1,0:T(8,128)(2,1)}, u32[]{:S(2)}, u32[]{:S(2)}) collective-permute-start(bf16[96,3072]{1,0:T(8,128)(2,1)S(1)} %bitcast.84), channel_id=1, source_target_pairs={{0,16},{8,24},{16,0},{24,8},{1,17},{9,25},{17,1},{25,9},{2,18},{10... | collective-permute-start | bytes 1769480 | tf_op jit(solution)/shard_map/ppermute | solution.py:30
  69.7 28.3 %copy-start.5 = (bf16[96,3072]{1,0:T(8,128)(2,1)}, bf16[96,3072]{1,0:T(8,128)(2,1)S(1)}, u32[]{:S(2)}) copy-start(bf16[96,3072]{1,0:T(8,128)(2,1)S(1)} %collective-permute-done.11.refs_6_) | copy-start | bytes 1769476
  69.7 28.3 %collective-permute-start.6 = (bf16[96,3072]{1,0:T(8,128)(2,1)S(1)}, bf16[96,3072]{1,0:T(8,128)(2,1)}, u32[]{:S(2)}, u32[]{:S(2)}) collective-permute-start(bf16[96,3072]{1,0:T(8,128)(2,1)S(1)} %bitcast.85), channel_id=1, source_target_pairs={{0,8},{8,16},{16,24},{24,0},{1,9},{9,17},{17,25},{25,1},{2,10},{10... | collective-permute-start | bytes 1769480 | tf_op jit(solution)/shard_map/ppermute | solution.py:30
  107.2 36.4 %collective-permute-start.29 = (bf16[288,2048]{1,0:T(8,128)(2,1)}, bf16[288,2048]{1,0:T(8,128)(2,1)S(1)}, u32[]{:S(2)}, u32[]{:S(2)}) collective-permute-start(bf16[288,2048]{1,0:T(8,128)(2,1)} %get-tuple-element.28), channel_id=1, source_target_pairs={{0,1},{1,0},{2,3},{3,2},{4,5},{5,4},{6,7},{7,6},{8,9},{9,8},{10,11... | collective-permute-start | bytes 3538952 | tf_op jit(solution)/shard_map/ppermute | solution.py:25
  116.4 6.0 %collective-permute-start.19 = (bf16[384,88]{1,0:T(8,128)(2,1)S(1)}, bf16[384,88]{1,0:T(8,128)(2,1)S(1)}, u32[]{:S(2)}, u32[]{:S(2)}) collective-permute-start(bf16[384,88]{1,0:T(8,128)(2,1)S(1)} %get-tuple-element.51), channel_id=1, source_target_pairs={{0,1},{1,0},{2,3},{3,2},{4,5},{5,4},{6,7},{7,6},{8,9},{9,8},{10,11... | collective-permute-start | bytes 202760 | tf_op jit(solution)/shard_map/ppermute | solution.py:25
  118.0 21.0 %collective-permute-start.23 = (bf16[4,24,2048]{2,1,0:T(8,128)(2,1)}, bf16[4,24,2048]{2,1,0:T(8,128)(2,1)}, u32[]{:S(2)}, u32[]{:S(2)}) collective-permute-start(bf16[4,24,2048]{2,1,0:T(8,128)(2,1)} %get-tuple-element.38), channel_id=1, source_target_pairs={{0,2},{2,4},{4,6},{6,0},{1,3},{3,5},{5,7},{7,1},{8,10},{10,12},{12... | collective-permute-start | bytes 1179656 | tf_op jit(solution)/shard_map/ppermute | solution.py:30
  118.3 23.3 %collective-permute-start.24 = (bf16[4,24,2048]{2,1,0:T(8,128)(2,1)}, bf16[4,24,2048]{2,1,0:T(8,128)(2,1)}, u32[]{:S(2)}, u32[]{:S(2)}) collective-permute-start(bf16[4,24,2048]{2,1,0:T(8,128)(2,1)} %get-tuple-element.39), channel_id=1, source_target_pairs={{0,4},{2,6},{4,0},{6,2},{1,5},{3,7},{5,1},{7,3},{8,12},{10,14},{12... | collective-permute-start | bytes 1179656 | tf_op jit(solution)/shard_map/ppermute | solution.py:30
  120.1 22.1 %collective-permute-start.25 = (bf16[4,24,2048]{2,1,0:T(8,128)(2,1)S(1)}, bf16[4,24,2048]{2,1,0:T(8,128)(2,1)}, u32[]{:S(2)}, u32[]{:S(2)}) collective-permute-start(bf16[4,24,2048]{2,1,0:T(8,128)(2,1)S(1)} %get-tuple-element.40), channel_id=1, source_target_pairs={{0,6},{2,0},{4,2},{6,4},{1,7},{3,1},{5,3},{7,5},{8,14},{10,8},{12,... | collective-permute-start | bytes 1179656 | tf_op jit(solution)/shard_map/ppermute | solution.py:30
  122.5 4.2 %collective-permute-start.20 = (bf16[2,4,24,88]{3,2,1,0:T(8,128)(2,1)S(1)}, bf16[2,4,24,88]{3,2,1,0:T(8,128)(2,1)S(1)}, u32[]{:S(2)}, u32[]{:S(2)}) collective-permute-start(bf16[2,4,24,88]{3,2,1,0:T(8,128)(2,1)S(1)} %get-tuple-element.48), channel_id=1, source_target_pairs={{0,24},{8,0},{16,8},{24,16},{1,25},{9,1},{17,9},{25,17},{2,26},{10... | collective-permute-start | bytes 101384 | tf_op jit(solution)/shard_map/ppermute | solution.py:30
  126.6 5.6 %collective-permute-start.21 = (bf16[2,4,24,88]{3,2,1,0:T(8,128)(2,1)S(1)}, bf16[2,4,24,88]{3,2,1,0:T(8,128)(2,1)S(1)}, u32[]{:S(2)}, u32[]{:S(2)}) collective-permute-start(bf16[2,4,24,88]{3,2,1,0:T(8,128)(2,1)S(1)} %get-tuple-element.49), channel_id=1, source_target_pairs={{0,16},{8,24},{16,0},{24,8},{1,17},{9,25},{17,1},{25,9},{2,18},{10... | collective-permute-start | bytes 101384 | tf_op jit(solution)/shard_map/ppermute | solution.py:30
  132.2 5.3 %collective-permute-start.22 = (bf16[2,4,24,88]{3,2,1,0:T(8,128)(2,1)S(1)}, bf16[2,4,24,88]{3,2,1,0:T(8,128)(2,1)S(1)}, u32[]{:S(2)}, u32[]{:S(2)}) collective-permute-start(bf16[2,4,24,88]{3,2,1,0:T(8,128)(2,1)S(1)} %get-tuple-element.47), channel_id=1, source_target_pairs={{0,8},{8,16},{16,24},{24,0},{1,9},{9,17},{17,25},{25,1},{2,10},{10... | collective-permute-start | bytes 101384 | tf_op jit(solution)/shard_map/ppermute | solution.py:30
  137.5 23.7 %collective-permute-start.13 = (bf16[96,2048]{1,0:T(8,128)(2,1)}, bf16[96,2048]{1,0:T(8,128)(2,1)}, u32[]{:S(2)}, u32[]{:S(2)}) collective-permute-start(bf16[96,2048]{1,0:T(8,128)(2,1)} %get-tuple-element.22), channel_id=1, source_target_pairs={{0,8},{8,16},{16,24},{24,0},{1,9},{9,17},{17,25},{25,1},{2,10},{10... | collective-permute-start | bytes 1179656 | tf_op jit(solution)/shard_map/ppermute | solution.py:30
  139.0 23.7 %collective-permute-start.14 = (bf16[96,2048]{1,0:T(8,128)(2,1)}, bf16[96,2048]{1,0:T(8,128)(2,1)}, u32[]{:S(2)}, u32[]{:S(2)}) collective-permute-start(bf16[96,2048]{1,0:T(8,128)(2,1)} %get-tuple-element.23), channel_id=1, source_target_pairs={{0,16},{8,24},{16,0},{24,8},{1,17},{9,25},{17,1},{25,9},{2,18},{10... | collective-permute-start | bytes 1179656 | tf_op jit(solution)/shard_map/ppermute | solution.py:30
  141.6 22.2 %collective-permute-start.15 = (bf16[96,2048]{1,0:T(8,128)(2,1)}, bf16[96,2048]{1,0:T(8,128)(2,1)}, u32[]{:S(2)}, u32[]{:S(2)}) collective-permute-start(bf16[96,2048]{1,0:T(8,128)(2,1)} %get-tuple-element.24), channel_id=1, source_target_pairs={{0,24},{8,0},{16,8},{24,16},{1,25},{9,1},{17,9},{25,17},{2,26},{10... | collective-permute-start | bytes 1179656 | tf_op jit(solution)/shard_map/ppermute | solution.py:30
  143.6 1.1 copy-start.6
  148.2 15.6 %copy-start.7 = (bf16[96,2048]{1,0:T(8,128)(2,1)S(1)}, bf16[96,2048]{1,0:T(8,128)(2,1)}, u32[]{:S(2)}) copy-start(bf16[96,2048]{1,0:T(8,128)(2,1)} %get-tuple-element.21) | copy-start | bytes 1179652
  148.2 35.7 %all-to-all-start.1 = ((bf16[32,144,128]{2,1,0:T(8,128)(2,1)}), bf16[32,144,128]{2,1,0:T(8,128)(2,1)S(1)}, u32[]{:S(2)}, u32[]{:S(2)}) async-start(bf16[32,144,128]{2,1,0:T(8,128)(2,1)} %shard_map.139), calls=%async_computation.1 | async-start | bytes 2359296 | tf_op jit(solution)/shard_map/all_to_all | solution.py:21
  157.0 9.1 %collective-permute-start.26 = (bf16[24,2048]{1,0:T(8,128)(2,1)S(1)}, bf16[24,2048]{1,0:T(8,128)(2,1)S(1)}, u32[]{:S(2)}, u32[]{:S(2)}) collective-permute-start(bf16[24,2048]{1,0:T(8,128)(2,1)S(1)} %get-tuple-element.41), channel_id=1, source_target_pairs={{0,8},{8,16},{16,24},{24,0},{1,9},{9,17},{17,25},{25,1},{2,10},{10... | collective-permute-start | bytes 294920 | tf_op jit(solution)/shard_map/ppermute | solution.py:30
  158.6 10.1 %collective-permute-start.27 = (bf16[24,2048]{1,0:T(8,128)(2,1)S(1)}, bf16[24,2048]{1,0:T(8,128)(2,1)S(1)}, u32[]{:S(2)}, u32[]{:S(2)}) collective-permute-start(bf16[24,2048]{1,0:T(8,128)(2,1)S(1)} %get-tuple-element.43), channel_id=1, source_target_pairs={{0,16},{8,24},{16,0},{24,8},{1,17},{9,25},{17,1},{25,9},{2,18},{10... | collective-permute-start | bytes 294920 | tf_op jit(solution)/shard_map/ppermute | solution.py:30
  161.3 8.4 %collective-permute-start.28 = (bf16[24,2048]{1,0:T(8,128)(2,1)S(1)}, bf16[24,2048]{1,0:T(8,128)(2,1)S(1)}, u32[]{:S(2)}, u32[]{:S(2)}) collective-permute-start(bf16[24,2048]{1,0:T(8,128)(2,1)S(1)} %get-tuple-element.42), channel_id=1, source_target_pairs={{0,24},{8,0},{16,8},{24,16},{1,25},{9,1},{17,9},{25,17},{2,26},{10... | collective-permute-start | bytes 294920 | tf_op jit(solution)/shard_map/ppermute | solution.py:30
  165.3 7.0 %collective-permute-start.16 = (bf16[24,2048]{1,0:T(8,128)(2,1)S(1)}, bf16[24,2048]{1,0:T(8,128)(2,1)S(1)}, u32[]{:S(2)}, u32[]{:S(2)}) collective-permute-start(bf16[24,2048]{1,0:T(8,128)(2,1)S(1)} %get-tuple-element.44), channel_id=1, source_target_pairs={{0,2},{2,4},{4,6},{6,0},{1,3},{3,5},{5,7},{7,1},{8,10},{10,12},{12... | collective-permute-start | bytes 294920 | tf_op jit(solution)/shard_map/ppermute | solution.py:30
  165.4 6.9 %collective-permute-start.17 = (bf16[24,2048]{1,0:T(8,128)(2,1)S(1)}, bf16[24,2048]{1,0:T(8,128)(2,1)S(1)}, u32[]{:S(2)}, u32[]{:S(2)}) collective-permute-start(bf16[24,2048]{1,0:T(8,128)(2,1)S(1)} %get-tuple-element.46), channel_id=1, source_target_pairs={{0,4},{2,6},{4,0},{6,2},{1,5},{3,7},{5,1},{7,3},{8,12},{10,14},{12... | collective-permute-start | bytes 294920 | tf_op jit(solution)/shard_map/ppermute | solution.py:30
  166.2 7.0 %collective-permute-start.18 = (bf16[24,2048]{1,0:T(8,128)(2,1)S(1)}, bf16[24,2048]{1,0:T(8,128)(2,1)S(1)}, u32[]{:S(2)}, u32[]{:S(2)}) collective-permute-start(bf16[24,2048]{1,0:T(8,128)(2,1)S(1)} %get-tuple-element.45), channel_id=1, source_target_pairs={{0,6},{2,0},{4,2},{6,4},{1,7},{3,1},{5,3},{7,5},{8,14},{10,8},{12,... | collective-permute-start | bytes 294920 | tf_op jit(solution)/shard_map/ppermute | solution.py:30
  183.9 1.1 copy-start.3

commit v2 on v1

v2 whole, which is shorter than its diff:
```python
import functools
import math

import jax
import jax.numpy as jnp
from jax import lax
from jax.experimental import pallas as pl
from jax.experimental.pallas import tpu as pltpu
from jax.sharding import Mesh
from jax.sharding import PartitionSpec as P


BF16 = jnp.bfloat16
F32 = jnp.float32
FS = ("z", "y")
TP = ("x", "c")
ALL = ("z", "y", "x", "c")


def spread(blocks, axis):
    return lax.all_to_all(blocks, axis, 0, 0, tiled=True)


def swapped(array):
    return lax.ppermute(array, "c", [(0, 1), (1, 0)])


def moved(array, axis, step):
    length = lax.axis_size(axis)
    return lax.ppermute(array, axis, [(i, (i + step) % length) for i in range(length)])


def around(array, axis):
    return [array] + [moved(array, axis, -step) for step in range(1, lax.axis_size(axis))]


def for_owner(blocks, axis):
    return [blocks[0]] + [moved(blocks[step], axis, step) for step in range(1, len(blocks))]


def added(parts):
    total = parts[0].astype(F32)
    for part in parts[1:]:
        total = total + part.astype(F32)
    return total.astype(BF16)


def dot(left, right, dims):
    return lax.dot_general(left, right, (dims, ((), ())), preferred_element_type=F32)


LANES = 128


def whole(kernel, out_shape, inputs, scratch=(), flops=0, grant=12, scalars=0):
    spec = pl.BlockSpec(memory_space=pltpu.VMEM)
    count = len(inputs) - scalars
    single = not isinstance(out_shape, tuple)
    return pl.pallas_call(
        kernel,
        out_shape=out_shape,
        in_specs=[pl.BlockSpec(memory_space=pltpu.SMEM)] * scalars + [spec] * count,
        out_specs=spec if single else tuple(spec for _ in out_shape),
        scratch_shapes=scratch,
        compiler_params=pltpu.CompilerParams(vmem_limit_bytes=grant * 2**20),
        cost_estimate=pl.CostEstimate(flops=flops, bytes_accessed=0, transcendentals=0),
    )(*inputs)


def like(shape, kind):
    return jax.ShapeDtypeStruct(shape, kind)


def exchange_lanes(left, right):
    half = LANES // 2
    lane = lax.broadcasted_iota(jnp.int32, left.shape, 1)
    low = jnp.where(lane < half, left, pltpu.roll(right, half, 1))
    high = jnp.where(lane < half, pltpu.roll(left, half, 1), right)
    return low, high


def front_kernel(copies, part, pad, x_next, x_prev, grad_out, gate, up, down_t, first, second, out):
    width = x_prev.shape[1]
    mid = width // 2
    first[:, :width] = x_prev[...]
    first[:, width:] = x_next[:, :mid]
    second[:, :width] = grad_out[...]
    second[:, width:] = x_next[:, mid:]
    shard, units = gate.shape
    both = jnp.concatenate((gate[...], up[...]), axis=0).astype(F32).T
    tall = jnp.concatenate((down_t[...], jnp.zeros_like(down_t))).astype(F32).T[:, :shard]
    half = pad // 2
    count = units // part
    for y in range(count):
        top = both[y * part : (y + 1) * part]
        piece = tall[y * part : (y + 1) * part]
        ahead, behind = piece[:half], piece[half:]
        behind = jnp.concatenate((behind, jnp.zeros((pad - part, shard), F32)))
        low = jnp.concatenate((ahead, behind), axis=1)
        block = jnp.concatenate((top, jnp.zeros((pad - part, LANES), F32), low)).astype(BF16)
        for z in range(copies):
            out[z * count + y] = block


def turned(array, outer, inner, rows):
    return jnp.concatenate(
        [
            array[(o * inner + i) * rows : (o * inner + i + 1) * rows]
            for i in range(inner)
            for o in range(outer)
        ]
    )


def backward_kernel(ny, nx, rows, pad, own, other, *refs):
    firsts, seconds = refs[:ny], refs[ny : ny + nx]
    kept, sent, gate_up, down, grads, prev, cotangent = refs[ny + nx :]
    half = pad // 2
    for base, packed in ((0, own), (pad, other)):
        for tile in range(packed.shape[0] // 2):
            at = pl.ds(tile * LANES, LANES)
            low, high = exchange_lanes(packed[2 * tile].astype(F32), packed[2 * tile + 1].astype(F32))
            gate_up[pl.ds(base, pad), at] = low[:pad].astype(BF16)
            gate_up[pl.ds(2 * pad + base, pad), at] = high[:pad].astype(BF16)
            down[pl.ds(base, half), at] = low[pad:].astype(BF16)
            down[pl.ds(base + half, half), at] = high[pad:].astype(BF16)
    for k in range(ny):
        prev[pl.ds(k * nx * rows, nx * rows)] = firsts[k][...]
    for k in range(nx):
        cotangent[pl.ds(k * ny * rows, ny * rows)] = seconds[k][...]
    pre = dot(prev[...], gate_up[...], ((1,), (1,)))
    gate_prev, up_prev = pre[:, : 2 * pad], pre[:, 2 * pad :]
    grad_hidden = turned(dot(cotangent[...], down[...], ((1,), (1,))), nx, ny, rows)
    sig = jax.nn.sigmoid(gate_prev)
    silu = gate_prev * sig
    grad_gate = grad_hidden * up_prev * sig * (1.0 + gate_prev * (1.0 - sig))
    grad_up = grad_hidden * silu
    hidden_prev = turned(silu * up_prev, ny, nx, rows)
    grads[:, : 2 * pad] = turned(grad_gate, ny, nx, rows).astype(BF16)
    grads[:, 2 * pad :] = turned(grad_up, ny, nx, rows).astype(BF16)
    for k, (value, tokens) in enumerate(((grad_gate, prev), (grad_up, prev), (hidden_prev, cotangent))):
        term = dot(value.astype(BF16).T, tokens[...], ((1,), (0,)))
        kept[pl.ds(k * pad, pad)] = term[:pad]
        sent[pl.ds(k * pad, pad)] = term[pad:].astype(BF16)


def input_kernel(grads, gate_up, *outs):
    rows = outs[0].shape[0]
    for k, out in enumerate(outs):
        at = pl.ds(k * rows, rows)
        out[...] = dot(grads[at, :], gate_up[...], ((1,), (0,))).astype(BF16)


def sum_kernel(count, *refs):
    parts, outs = refs[:count], refs[count:]
    rows = outs[0].shape[0]
    total = parts[0][...].astype(F32)
    for part in parts[1:]:
        total = total + part[...].astype(F32)
    for k, out in enumerate(outs):
        out[...] = total[k * rows : (k + 1) * rows].astype(BF16)


def pair_kernel(pad, kept, received, out):
    half = pad // 2
    for tile in range(out.shape[0] // 2):
        at = pl.ds(tile * LANES, LANES)
        total = kept[:, at] + received[:, at].astype(F32)
        left = jnp.concatenate((total[:pad], total[2 * pad : 2 * pad + half]))
        right = jnp.concatenate((total[pad : 2 * pad], total[2 * pad + half :]))
        even, odd = exchange_lanes(left, right)
        out[2 * tile] = even.astype(BF16)
        out[2 * tile + 1] = odd.astype(BF16)


def update_kernel(ny, part, pad, factor, arrived, gate, up, down_t, new_gate, new_up, new_down_t):
    half = pad // 2
    shard = down_t.shape[0]
    tops, lows = [], []
    for y in range(ny):
        total = arrived[y].astype(F32)
        for z in range(1, arrived.shape[0] // ny):
            total = total + arrived[z * ny + y].astype(F32)
        tops.append(total[:part])
        low = total[pad:]
        lows.append(low)
        lows.append(pltpu.roll(low, LANES // 2, 1)[: part - half])
    both = jnp.concatenate(tops).T
    new_gate[...] = gate[...] + factor * both[:shard]
    new_up[...] = up[...] + factor * both[shard:]
    new_down_t[...] = down_t[...] + factor * jnp.concatenate(lows).T[:shard]


def hidden_kernel(ny, nx, rows, pad, gate_up, *refs):
    firsts, seconds = refs[:ny], refs[ny : ny + nx]
    mine, theirs, hidden, tokens = refs[ny + nx :]
    half = tokens.shape[1]
    for k in range(ny):
        tokens[pl.ds(k * nx * rows, nx * rows)] = firsts[k][...]
    pre = dot(tokens[...], gate_up[:, :half], ((1,), (1,)))
    for k in range(nx):
        tokens[pl.ds(k * ny * rows, ny * rows)] = seconds[k][...]
    pre = pre + turned(dot(tokens[...], gate_up[:, half:], ((1,), (1,))), nx, ny, rows)
    value = jax.nn.silu(pre[:, : 2 * pad]) * pre[:, 2 * pad :]
    blank = jnp.zeros((value.shape[0], LANES - pad), F32)
    mine[...] = jnp.concatenate((value[:, :pad], blank), axis=1).astype(BF16)
    theirs[...] = jnp.concatenate((value[:, pad:], blank), axis=1).astype(BF16)
    hidden[...] = value.astype(BF16)


def output_kernel(hidden, down, mine, partner, *outs):
    rows = outs[0].shape[0]
    width = down.shape[1]
    for k, out in enumerate(outs):
        at = pl.ds(k * rows, rows)
        out[:, :width] = dot(hidden[at, :], down[...], ((1,), (0,))).astype(BF16)
        out[:, width : width + LANES] = mine[at, :]
        out[:, width + LANES :] = partner[at, :]


def arrival_kernel(nx, rows, part, place, *refs):
    ny = len(refs) - nx - 3
    parts, outs = refs[:ny], refs[ny : ny + nx]
    saved, by_y, by_x = refs[ny + nx :]
    width = outs[0].shape[1]
    total = parts[0][:, :width].astype(F32)
    for piece in parts[1:]:
        total = total + piece[:, :width].astype(F32)
    for k, out in enumerate(outs):
        out[...] = total[k * rows : (k + 1) * rows].astype(BF16)
    x, y, core = place[0], place[1], place[2]
    for k in range(ny):
        by_y[k] = parts[k][:, width:].astype(F32)
    pieces = [by_y[lax.rem(y - s + ny, ny)] for s in range(ny)]
    here = jnp.concatenate([piece[:, :part] for piece in pieces], axis=1)
    there = jnp.concatenate([piece[:, LANES : LANES + part] for piece in pieces], axis=1)
    low = jnp.where(core == 0, here, there)
    high = jnp.where(core == 0, there, here)
    for k in range(nx):
        by_x[k, :rows] = low[k * rows : (k + 1) * rows]
        by_x[k, rows:] = high[k * rows : (k + 1) * rows]
    ordered = [by_x[lax.rem(s - x + nx, nx)] for s in range(nx)]
    saved[...] = jnp.concatenate(ordered).astype(BF16)


def layer(x_next, x_prev, grad_out, gate_w, up_w, down_w, acc_gate, acc_up, acc_down):
    rows, width = x_prev.shape
    nz, ny, nx, nc = (lax.axis_size(name) for name in ALL)
    group = ny * nx * rows
    factor = 1.0 / math.sqrt(rows * nz * ny * nx * nc)
    units = gate_w.shape[1]
    part = units // ny
    pad = -(-part // 32) * 32
    block = (nz * ny, pad + pad // 2, LANES)
    mid = width // 2
    token_ops = 2 * group * 2 * pad * width

    first, second, packed = whole(
        functools.partial(front_kernel, nz, part, pad),
        (like((rows, width + mid), BF16), like((rows, width + mid), BF16), like(block, BF16)),
        (x_next, x_prev, grad_out, gate_w, up_w, down_w.T),
    )

    own = spread(packed, FS)
    other = swapped(own)

    first = jnp.stack(around(first, "x")).reshape(nx * rows, width + mid)
    second = jnp.stack(around(second, "y")).reshape(ny * rows, width + mid)
    prevs = around(first[:, :width], "y")
    cotangents = around(second[:, :width], "x")
    nexts = around(first[:, width:], "y")
    nexts = nexts + around(second[:, width:], "x")

    kept, sent, gate_up, down, grads = whole(
        functools.partial(backward_kernel, ny, nx, rows, pad),
        (
            like((3 * pad, width), F32),
            like((3 * pad, width), BF16),
            like((4 * pad, width), BF16),
            like((2 * pad, width), BF16),
            like((group, 4 * pad), BF16),
        ),
        (own, other, *prevs, *cotangents),
        (pltpu.VMEM((group, width), BF16), pltpu.VMEM((group, width), BF16)),
        flops=6 * token_ops,
        grant=20,
    )
    received = swapped(sent)
    input_parts = whole(
        input_kernel,
        tuple(like((ny * rows, width), BF16) for _ in range(nx)),
        (grads, gate_up),
        flops=2 * token_ops,
    )
    paired = whole(functools.partial(pair_kernel, pad), like(block, BF16), (kept, received))
    arrived = spread(paired, FS)
    new_gate, new_up, new_down_t = whole(
        functools.partial(update_kernel, ny, part, pad, factor),
        (like(acc_gate.shape, F32), like(acc_up.shape, F32), like(acc_down.shape[::-1], F32)),
        (arrived, acc_gate, acc_up, acc_down.T),
    )

    arrivals = for_owner(input_parts, "x")
    by_x = whole(
        functools.partial(sum_kernel, nx),
        tuple(like((rows, width), BF16) for _ in range(ny)),
        arrivals,
    )
    grad_input = added(for_owner(by_x, "y"))

    mine, theirs, hidden = whole(
        functools.partial(hidden_kernel, ny, nx, rows, pad),
        (like((group, LANES), BF16), like((group, LANES), BF16), like((group, 2 * pad), BF16)),
        (gate_up, *nexts),
        (pltpu.VMEM((group, mid), BF16),),
        flops=2 * token_ops,
    )
    partner = swapped(theirs)
    out_parts = whole(
        output_kernel,
        tuple(like((nx * rows, width + 2 * LANES), BF16) for _ in range(ny)),
        (hidden, down, mine, partner),
        flops=token_ops,
    )
    arrivals = for_owner(out_parts, "y")
    place = jnp.stack([lax.axis_index(name) for name in ("x", "y", "c")]).astype(jnp.int32)
    *by_y, saved = whole(
        functools.partial(arrival_kernel, nx, rows, part),
        (
            *(like((rows, width), BF16) for _ in range(nx)),
            like((nx * nc * rows, units), BF16),
        ),
        (place, *arrivals),
        (
            pltpu.VMEM((ny, nx * rows, 2 * LANES), F32),
            pltpu.VMEM((nx, nc * rows, units), F32),
        ),
        scalars=1,
    )
    out_next = added(for_owner(by_y, "x"))
    return out_next, saved, grad_input, new_gate, new_up, new_down_t.T


def solution(mesh):
    split = Mesh(mesh.devices.reshape(8, 4, 4, 2), ALL)
    tokens = P(ALL, None)
    wide, tall = P(FS, TP), P(TP, FS)
    in_specs = (tokens, tokens, tokens, wide, wide, tall, wide, wide, tall)
    out_specs = (tokens, wide, tokens, wide, wide, tall)
    return jax.shard_map(layer, mesh=split, in_specs=in_specs, out_specs=out_specs, check_vma=False)
```

time: 191 us -> 187 us (0.979)
  waiting for transfers between devices: 80.8 us -> 95.4 us
  Pallas kernels: 22.9 us -> 15.2 us
  starting transfers between devices: 65.2 us -> 59.2 us
  other arithmetic: 6.38 us -> 1.61 us
  matrix products: 2.49 us -> 0 us
    all_to_all x2, waiting for transfers between devices: 17.8 us -> 26.4 us  [spread(): return lax.all_to_all(blocks, axis, 0, 0, tiled=True)]
    pallas_call x5 -> x9, Pallas kernels: 22.9 us -> 15.2 us  [whole(): pl.pallas_call(kernel, out_shape=out_shape, in_specs=[pl.BlockSpec(memory...]
    ppermute x3, waiting for transfers between devices: 0.01 us -> 4.01 us  [swapped(): return lax.ppermute(array, 'c', [(0, 1), (1, 0)])]
    all_to_all x2, starting transfers between devices: 19.8 us -> 16.5 us  [spread(): return lax.all_to_all(blocks, axis, 0, 0, tiled=True)]
    unnamed x32 -> x34, local copies, waits for them, and re-layouts: 7.13 us -> 10.3 us
    convert_element_type x4 -> x2, other arithmetic: 4.31 us -> 1.39 us  [added(): return total.astype(BF16)]
    ppermute x27 -> x30, starting transfers between devices: 44.8 us -> 42.2 us  [moved(): lax.ppermute(array, axis, [(i, (i + step) % length) for i in range(length)])]
    dot_general x1 -> x0, matrix products: 2.49 us -> none  [dot(): lax.dot_general(left, right, (dims, ((), ())), preferred_element_type=F32)]
  transfers between devices with their start and end apart: 32 -> 35, of which waited for: 17 -> 17; matrix products, arithmetic and copies ran while one was open for 7% -> 2% of each run, Pallas kernels for 5% -> 4%
where the time goes in v2:
time: 187 us; the launch traced here: 184 us
  waiting for transfers between devices  95.4 us (51%)
  starting transfers between devices  59.2 us (32%)
  Pallas kernels  15.2 us (8%)
  local copies, waits for them, and re-layouts  12.2 us (7%)
    ppermute x30, waiting for transfers between devices, moved(): lax.ppermute(array, axis, [(i, (i + step) % length) for i in range(length)])  65 us
    ppermute x30, starting transfers between devices, moved(): lax.ppermute(array, axis, [(i, (i + step) % length) for i in range(length)])  42.2 us
    all_to_all x2, waiting for transfers between devices, spread(): return lax.all_to_all(blocks, axis, 0, 0, tiled=True)  26.4 us
    all_to_all x2, starting transfers between devices, spread(): return lax.all_to_all(blocks, axis, 0, 0, tiled=True)  16.5 us
    pallas_call x9, Pallas kernels, whole(): pl.pallas_call(kernel, out_shape=out_shape, in_specs=[pl.BlockSpec(memory...  15.2 us
    unnamed x34, local copies, waits for them, and re-layouts  10.3 us
    ppermute x3, waiting for transfers between devices, swapped(): return lax.ppermute(array, 'c', [(0, 1), (1, 0)])  4.01 us
  transfers between devices with their start and end apart: 35, of which 17 were waited for; matrix products, arithmetic and copies ran while one was open for 2% of the time, Pallas kernels for 4%

profile of v2, /device:TPU:64, one launch (start us, length us, event | category | flops | bytes accessed | tf_op | source)
XLA Modules:
  0.0 184.5 jit_solution(12003887566368764924)
XLA Ops:
  1.5 0.9 copy-done.5
  2.4 0.9 copy-done.6
  5.7 1.3 shard_map.136
  7.0 10.9 %all-to-all-start = ((bf16[32,144,128]{2,1,0:T(8,128)(2,1)}), bf16[32,144,128]{2,1,0:T(8,128)(2,1)S(1)}, u32[]{:S(2)}, u32[]{:S(2)}) async-start(bf16[32,144,128]{2,1,0:T(8,128)(2,1)} %get-tuple-element.37), calls=%async_computation | async-start | bytes 2359296 | tf_op jit(solution)/shard_map/all_to_all | solution.py:21
  17.9 2.8 %collective-permute-start.7 = (bf16[24,3072]{1,0:T(8,128)(2,1)S(1)}, bf16[24,3072]{1,0:T(8,128)(2,1)S(1)}, u32[]{:S(2)}, u32[]{:S(2)}) collective-permute-start(bf16[24,3072]{1,0:T(8,128)(2,1)S(1)} %get-tuple-element.39), channel_id=1, source_target_pairs={{0,24},{8,0},{16,8},{24,16},{1,25},{9,1},{17,9},{25,17},{2,26},{10... | collective-permute-start | bytes 442376 | tf_op jit(solution)/shard_map/ppermute | solution.py:30
  22.4 26.4 %all-to-all-done.own = bf16[32,144,128]{2,1,0:T(8,128)(2,1)S(1)} async-done(((bf16[32,144,128]{2,1,0:T(8,128)(2,1)}), bf16[32,144,128]{2,1,0:T(8,128)(2,1)S(1)}, u32[]{:S(2)}, u32[]{:S(2)}) %all-to-all-start) | async-done | bytes 1179680 | tf_op jit(solution)/shard_map/all_to_all | solution.py:21
  48.7 2.8 %collective-permute-start.1 = (bf16[24,3072]{1,0:T(8,128)(2,1)S(1)}, bf16[24,3072]{1,0:T(8,128)(2,1)S(1)}, u32[]{:S(2)}, u32[]{:S(2)}) collective-permute-start(bf16[24,3072]{1,0:T(8,128)(2,1)S(1)} %get-tuple-element.38), channel_id=1, source_target_pairs={{0,6},{2,0},{4,2},{6,4},{1,7},{3,1},{5,3},{7,5},{8,14},{10,8},{12,... | collective-permute-start | bytes 442376 | tf_op jit(solution)/shard_map/ppermute | solution.py:30
  53.3 2.4 %collective-permute-start.10 = (bf16[96,2048]{1,0:T(8,128)(2,1)S(1)}, bf16[96,2048]{1,0:T(8,128)(2,1)S(1)}, u32[]{:S(2)}, u32[]{:S(2)}) collective-permute-start(bf16[96,2048]{1,0:T(8,128)(2,1)S(1)} %slice.17.refs_4_), channel_id=1, source_target_pairs={{0,6},{2,0},{4,2},{6,4},{1,7},{3,1},{5,3},{7,5},{8,14},{10,8},{12,... | collective-permute-start | bytes 1179656 | tf_op jit(solution)/shard_map/ppermute | solution.py:30
  55.8 3.0 %collective-permute-done.1 = bf16[24,3072]{1,0:T(8,128)(2,1)S(1)} collective-permute-done((bf16[24,3072]{1,0:T(8,128)(2,1)S(1)}, bf16[24,3072]{1,0:T(8,128)(2,1)S(1)}, u32[]{:S(2)}, u32[]{:S(2)}) %collective-permute-start.1) | collective-permute-done | bytes 147488 | tf_op jit(solution)/shard_map/ppermute | solution.py:30
  58.8 1.0 collective-permute-done.2
  59.8 3.7 %collective-permute-start.12 = (bf16[96,2048]{1,0:T(8,128)(2,1)S(1)}, bf16[96,2048]{1,0:T(8,128)(2,1)S(1)}, u32[]{:S(2)}, u32[]{:S(2)}) collective-permute-start(bf16[96,2048]{1,0:T(8,128)(2,1)S(1)} %slice.17.refs_4_), channel_id=1, source_target_pairs={{0,2},{2,4},{4,6},{6,0},{1,3},{3,5},{5,7},{7,1},{8,10},{10,12},{12... | collective-permute-start | bytes 1179656 | tf_op jit(solution)/shard_map/ppermute | solution.py:30
  63.9 11.5 %collective-permute-done.10.refs_5_ = bf16[96,2048]{1,0:T(8,128)(2,1)S(1)} collective-permute-done((bf16[96,2048]{1,0:T(8,128)(2,1)S(1)}, bf16[96,2048]{1,0:T(8,128)(2,1)S(1)}, u32[]{:S(2)}, u32[]{:S(2)}) %collective-permute-start.10) | collective-permute-done | bytes 393248 | tf_op jit(solution)/shard_map/ppermute | solution.py:30
  76.4 2.7 %collective-permute-done.12.refs_7_ = bf16[96,2048]{1,0:T(8,128)(2,1)S(1)} collective-permute-done((bf16[96,2048]{1,0:T(8,128)(2,1)S(1)}, bf16[96,2048]{1,0:T(8,128)(2,1)S(1)}, u32[]{:S(2)}, u32[]{:S(2)}) %collective-permute-start.12) | collective-permute-done | bytes 393248 | tf_op jit(solution)/shard_map/ppermute | solution.py:30
  79.1 9.8 %collective-permute-done.5.refs_2_ = bf16[96,2048]{1,0:T(8,128)(2,1)S(1)} collective-permute-done((bf16[96,2048]{1,0:T(8,128)(2,1)S(1)}, bf16[96,2048]{1,0:T(8,128)(2,1)S(1)}, u32[]{:S(2)}, u32[]{:S(2)}) %collective-permute-start.5) | collective-permute-done | bytes 393248 | tf_op jit(solution)/shard_map/ppermute | solution.py:30
  88.8 6.9 %collective-permute-done.6.refs_3_ = bf16[96,2048]{1,0:T(8,128)(2,1)S(1)} collective-permute-done((bf16[96,2048]{1,0:T(8,128)(2,1)S(1)}, bf16[96,2048]{1,0:T(8,128)(2,1)S(1)}, u32[]{:S(2)}, u32[]{:S(2)}) %collective-permute-start.6) | collective-permute-done | bytes 393248 | tf_op jit(solution)/shard_map/ppermute | solution.py:30
  95.7 4.0 %shard_map.137 = (f32[288,2048]{1,0:T(8,128)S(1)}, bf16[288,2048]{1,0:T(8,128)(2,1)S(1)}, bf16[384,2048]{1,0:T(8,128)(2,1)S(1)}, bf16[192,2048]{1,0:T(8,128)(2,1)S(1)}, bf16[384,384]{1,0:T(8,128)(2,1)S(1)}) custom-call(bf16[32,144,128]{2,1,0:T(8,128)(2,1)S(1)} %all-to-all-done.own, bf16[32,144,128]{2,1,0:T(8,128)(2,1)S(1)} %collective-permute-done.other, ...), custom_call_target="tpu_custom_call" | custom-call | flops 1811939328 | tf_op jit(solution)/shard_map/pallas_call | solution.py:59
  100.4 2.8 %collective-permute-done.32.received = bf16[288,2048]{1,0:T(8,128)(2,1)S(1)} collective-permute-done((bf16[288,2048]{1,0:T(8,128)(2,1)S(1)}, bf16[288,2048]{1,0:T(8,128)(2,1)S(1)}, u32[]{:S(2)}, u32[]{:S(2)}) %collective-permute-start.32) | collective-permute-done | bytes 1179680 | tf_op jit(solution)/shard_map/ppermute | solution.py:25
  103.3 1.6 shard_map.143
  104.8 5.6 %all-to-all-start.1 = ((bf16[32,144,128]{2,1,0:T(8,128)(2,1)}), bf16[32,144,128]{2,1,0:T(8,128)(2,1)S(1)}, u32[]{:S(2)}, u32[]{:S(2)}) async-start(bf16[32,144,128]{2,1,0:T(8,128)(2,1)} %shard_map.143), calls=%async_computation.1 | async-start | bytes 2359296 | tf_op jit(solution)/shard_map/all_to_all | solution.py:21
  110.4 0.9 slice.19.refs_4_
  111.4 3.9 %collective-permute-start.16 = (bf16[96,1024]{1,0:T(8,128)(2,1)S(1)}, bf16[96,1024]{1,0:T(8,128)(2,1)S(1)}, u32[]{:S(2)}, u32[]{:S(2)}) collective-permute-start(bf16[96,1024]{1,0:T(8,128)(2,1)S(1)} %slice.19.refs_4_), channel_id=1, source_target_pairs={{0,6},{2,0},{4,2},{6,4},{1,7},{3,1},{5,3},{7,5},{8,14},{10,8},{12,... | collective-permute-start | bytes 589832 | tf_op jit(solution)/shard_map/ppermute | solution.py:30
  115.3 1.0 collective-permute-start.18
  116.3 0.9 slice.18.refs_0_
  117.2 2.8 %collective-permute-start.13 = (bf16[96,1024]{1,0:T(8,128)(2,1)S(1)}, bf16[96,1024]{1,0:T(8,128)(2,1)S(1)}, u32[]{:S(2)}, u32[]{:S(2)}) collective-permute-start(bf16[96,1024]{1,0:T(8,128)(2,1)S(1)} %slice.18.refs_0_), channel_id=1, source_target_pairs={{0,24},{8,0},{16,8},{24,16},{1,25},{9,1},{17,9},{25,17},{2,26},{10... | collective-permute-start | bytes 589832 | tf_op jit(solution)/shard_map/ppermute | solution.py:30
  120.8 2.6 %collective-permute-done.16.refs_5_ = bf16[96,1024]{1,0:T(8,128)(2,1)S(1)} collective-permute-done((bf16[96,1024]{1,0:T(8,128)(2,1)S(1)}, bf16[96,1024]{1,0:T(8,128)(2,1)S(1)}, u32[]{:S(2)}, u32[]{:S(2)}) %collective-permute-start.16) | collective-permute-done | bytes 196640 | tf_op jit(solution)/shard_map/ppermute | solution.py:30
  123.4 1.5 collective-permute-start.15
  124.9 1.0 copy-done.14
  125.8 2.1 %shard_map.141 = (bf16[96,2048]{1,0:T(8,128)(2,1)S(1)}, bf16[96,2048]{1,0:T(8,128)(2,1)S(1)}, bf16[96,2048]{1,0:T(8,128)(2,1)}, bf16[96,2048]{1,0:T(8,128)(2,1)}) custom-call(bf16[384,384]{1,0:T(8,128)(2,1)S(1)} %copy-done.14, bf16[384,2048]{1,0:T(8,128)(2,1)S(1)} %get-tuple-element.40.gate_up), custom_call_target="tpu_custom_call" | custom-call | flops 603979776 | tf_op jit(solution)/shard_map/pallas_call | solution.py:59
  128.7 5.3 %collective-permute-done.13.refs_1_ = bf16[96,1024]{1,0:T(8,128)(2,1)S(1)} collective-permute-done((bf16[96,1024]{1,0:T(8,128)(2,1)S(1)}, bf16[96,1024]{1,0:T(8,128)(2,1)S(1)}, u32[]{:S(2)}, u32[]{:S(2)}) %collective-permute-start.13) | collective-permute-done | bytes 196640 | tf_op jit(solution)/shard_map/ppermute | solution.py:30
  134.0 4.0 %collective-permute-done.15.refs_3_ = bf16[96,1024]{1,0:T(8,128)(2,1)S(1)} collective-permute-done((bf16[96,1024]{1,0:T(8,128)(2,1)S(1)}, bf16[96,1024]{1,0:T(8,128)(2,1)S(1)}, u32[]{:S(2)}, u32[]{:S(2)}) %collective-permute-start.15) | collective-permute-done | bytes 196640 | tf_op jit(solution)/shard_map/ppermute | solution.py:30
  138.0 1.2 shard_map.138
  139.6 1.2 collective-permute-done.19.partner
  140.8 1.6 shard_map.139
  142.4 2.5 %collective-permute-start.28 = (bf16[96,2048]{1,0:T(8,128)(2,1)}, bf16[96,2048]{1,0:T(8,128)(2,1)}, u32[]{:S(2)}, u32[]{:S(2)}) collective-permute-start(bf16[96,2048]{1,0:T(8,128)(2,1)} %get-tuple-element.58), channel_id=1, source_target_pairs={{0,6},{2,0},{4,2},{6,4},{1,7},{3,1},{5,3},{7,5},{8,14},{10,8},{12,... | collective-permute-start | bytes 1179656 | tf_op jit(solution)/shard_map/ppermute | solution.py:30
  144.9 3.5 %collective-permute-start.21 = (bf16[96,2304]{1,0:T(8,128)(2,1)}, bf16[96,2304]{1,0:T(8,128)(2,1)S(1)}, u32[]{:S(2)}, u32[]{:S(2)}) collective-permute-start(bf16[96,2304]{1,0:T(8,128)(2,1)} %get-tuple-element.47), channel_id=1, source_target_pairs={{0,16},{8,24},{16,0},{24,8},{1,17},{9,25},{17,1},{25,9},{2,18},{10... | collective-permute-start | bytes 1327112 | tf_op jit(solution)/shard_map/ppermute | solution.py:30
  149.3 5.9 %collective-permute-done.27.refs_2_ = bf16[96,2048]{1,0:T(8,128)(2,1)S(1)} collective-permute-done((bf16[96,2048]{1,0:T(8,128)(2,1)}, bf16[96,2048]{1,0:T(8,128)(2,1)S(1)}, u32[]{:S(2)}, u32[]{:S(2)}) %collective-permute-start.27) | collective-permute-done | bytes 393248 | tf_op jit(solution)/shard_map/ppermute | solution.py:30
  155.3 8.4 %collective-permute-done.28.refs_3_ = bf16[96,2048]{1,0:T(8,128)(2,1)} collective-permute-done((bf16[96,2048]{1,0:T(8,128)(2,1)}, bf16[96,2048]{1,0:T(8,128)(2,1)}, u32[]{:S(2)}, u32[]{:S(2)}) %collective-permute-start.28) | collective-permute-done | bytes 393248 | tf_op jit(solution)/shard_map/ppermute | solution.py:30
  163.7 1.0 copy-done.1
  164.7 1.0 copy-done.3
  165.7 1.2 shard_map.142
  167.7 3.7 %collective-permute-start.30 = (bf16[24,2048]{1,0:T(8,128)(2,1)S(1)}, bf16[24,2048]{1,0:T(8,128)(2,1)S(1)}, u32[]{:S(2)}, u32[]{:S(2)}) collective-permute-start(bf16[24,2048]{1,0:T(8,128)(2,1)S(1)} %get-tuple-element.61), channel_id=1, source_target_pairs={{0,16},{8,24},{16,0},{24,8},{1,17},{9,25},{17,1},{25,9},{2,18},{10... | collective-permute-start | bytes 294920 | tf_op jit(solution)/shard_map/ppermute | solution.py:30
  171.4 1.4 collective-permute-start.31
  172.9 1.5 shard_map.140
  174.7 3.6 %collective-permute-start.24 = (bf16[24,2048]{1,0:T(8,128)(2,1)S(1)}, bf16[24,2048]{1,0:T(8,128)(2,1)S(1)}, u32[]{:S(2)}, u32[]{:S(2)}) collective-permute-start(bf16[24,2048]{1,0:T(8,128)(2,1)S(1)} %get-tuple-element.51), channel_id=1, source_target_pairs={{0,4},{2,6},{4,0},{6,2},{1,5},{3,7},{5,1},{7,3},{8,12},{10,14},{12... | collective-permute-start | bytes 294920 | tf_op jit(solution)/shard_map/ppermute | solution.py:30
  178.9 1.9 %collective-permute-done.23 = bf16[24,2048]{1,0:T(8,128)(2,1)S(1)} collective-permute-done((bf16[24,2048]{1,0:T(8,128)(2,1)S(1)}, bf16[24,2048]{1,0:T(8,128)(2,1)S(1)}, u32[]{:S(2)}, u32[]{:S(2)}) %collective-permute-start.23) | collective-permute-done | bytes 98336 | tf_op jit(solution)/shard_map/ppermute | solution.py:30
  180.8 1.1 collective-permute-done.24
  181.9 1.0 collective-permute-done.25
  183.6 0.9 shard_map.144
  (74 shorter events, 14.5 us)
Async XLA Ops:
  0.6 0.9 copy-start.4
  1.5 0.9 copy-start.5
  2.4 0.9 copy-start.6
  3.3 0.8 copy-start.10
  4.1 0.8 copy-start.11
  7.0 41.7 %all-to-all-start = ((bf16[32,144,128]{2,1,0:T(8,128)(2,1)}), bf16[32,144,128]{2,1,0:T(8,128)(2,1)S(1)}, u32[]{:S(2)}, u32[]{:S(2)}) async-start(bf16[32,144,128]{2,1,0:T(8,128)(2,1)} %get-tuple-element.37), calls=%async_computation | async-start | bytes 2359296 | tf_op jit(solution)/shard_map/all_to_all | solution.py:21
  17.9 33.6 %collective-permute-start.7 = (bf16[24,3072]{1,0:T(8,128)(2,1)S(1)}, bf16[24,3072]{1,0:T(8,128)(2,1)S(1)}, u32[]{:S(2)}, u32[]{:S(2)}) collective-permute-start(bf16[24,3072]{1,0:T(8,128)(2,1)S(1)} %get-tuple-element.39), channel_id=1, source_target_pairs={{0,24},{8,0},{16,8},{24,16},{1,25},{9,1},{17,9},{25,17},{2,26},{10... | collective-permute-start | bytes 442376 | tf_op jit(solution)/shard_map/ppermute | solution.py:30
  20.7 31.6 %collective-permute-start.8 = (bf16[24,3072]{1,0:T(8,128)(2,1)S(1)}, bf16[24,3072]{1,0:T(8,128)(2,1)S(1)}, u32[]{:S(2)}, u32[]{:S(2)}) collective-permute-start(bf16[24,3072]{1,0:T(8,128)(2,1)S(1)} %get-tuple-element.39), channel_id=1, source_target_pairs={{0,16},{8,24},{16,0},{24,8},{1,17},{9,25},{17,1},{25,9},{2,18},{10... | collective-permute-start | bytes 442376 | tf_op jit(solution)/shard_map/ppermute | solution.py:30
  21.5 31.7 %collective-permute-start.9 = (bf16[24,3072]{1,0:T(8,128)(2,1)S(1)}, bf16[24,3072]{1,0:T(8,128)(2,1)S(1)}, u32[]{:S(2)}, u32[]{:S(2)}) collective-permute-start(bf16[24,3072]{1,0:T(8,128)(2,1)S(1)} %get-tuple-element.39), channel_id=1, source_target_pairs={{0,8},{8,16},{16,24},{24,0},{1,9},{9,17},{17,25},{25,1},{2,10},{10... | collective-permute-start | bytes 442376 | tf_op jit(solution)/shard_map/ppermute | solution.py:30
  48.7 47.0 %collective-permute-start = (bf16[32,144,128]{2,1,0:T(8,128)(2,1)S(1)}, bf16[32,144,128]{2,1,0:T(8,128)(2,1)S(1)}, u32[]{:S(2)}, u32[]{:S(2)}) collective-permute-start(bf16[32,144,128]{2,1,0:T(8,128)(2,1)S(1)} %all-to-all-done.own), channel_id=1, source_target_pairs={{0,1},{1,0},{2,3},{3,2},{4,5},{5,4},{6,7},{7,6},{8,9},{9,8},{10,11... | collective-permute-start | bytes 3538952 | tf_op jit(solution)/shard_map/ppermute | solution.py:25
  48.7 10.0 %collective-permute-start.1 = (bf16[24,3072]{1,0:T(8,128)(2,1)S(1)}, bf16[24,3072]{1,0:T(8,128)(2,1)S(1)}, u32[]{:S(2)}, u32[]{:S(2)}) collective-permute-start(bf16[24,3072]{1,0:T(8,128)(2,1)S(1)} %get-tuple-element.38), channel_id=1, source_target_pairs={{0,6},{2,0},{4,2},{6,4},{1,7},{3,1},{5,3},{7,5},{8,14},{10,8},{12,... | collective-permute-start | bytes 442376 | tf_op jit(solution)/shard_map/ppermute | solution.py:30
  51.5 8.3 %collective-permute-start.2 = (bf16[24,3072]{1,0:T(8,128)(2,1)S(1)}, bf16[24,3072]{1,0:T(8,128)(2,1)S(1)}, u32[]{:S(2)}, u32[]{:S(2)}) collective-permute-start(bf16[24,3072]{1,0:T(8,128)(2,1)S(1)} %get-tuple-element.38), channel_id=1, source_target_pairs={{0,4},{2,6},{4,0},{6,2},{1,5},{3,7},{5,1},{7,3},{8,12},{10,14},{12... | collective-permute-start | bytes 442376 | tf_op jit(solution)/shard_map/ppermute | solution.py:30
  52.3 11.1 %collective-permute-start.3 = (bf16[24,3072]{1,0:T(8,128)(2,1)S(1)}, bf16[24,3072]{1,0:T(8,128)(2,1)S(1)}, u32[]{:S(2)}, u32[]{:S(2)}) collective-permute-start(bf16[24,3072]{1,0:T(8,128)(2,1)S(1)} %get-tuple-element.38), channel_id=1, source_target_pairs={{0,2},{2,4},{4,6},{6,0},{1,3},{3,5},{5,7},{7,1},{8,10},{10,12},{12... | collective-permute-start | bytes 442376 | tf_op jit(solution)/shard_map/ppermute | solution.py:30
  53.3 42.4 %copy-start.15 = (bf16[4,24,3072]{2,1,0:T(8,128)(2,1)}, bf16[4,24,3072]{2,1,0:T(8,128)(2,1)S(1)}, u32[]{:S(2)}) copy-start(bf16[4,24,3072]{2,1,0:T(8,128)(2,1)S(1)} %pad_maximum_fusion.1) | copy-start | bytes 1769476
  53.3 22.0 %collective-permute-start.10 = (bf16[96,2048]{1,0:T(8,128)(2,1)S(1)}, bf16[96,2048]{1,0:T(8,128)(2,1)S(1)}, u32[]{:S(2)}, u32[]{:S(2)}) collective-permute-start(bf16[96,2048]{1,0:T(8,128)(2,1)S(1)} %slice.17.refs_4_), channel_id=1, source_target_pairs={{0,6},{2,0},{4,2},{6,4},{1,7},{3,1},{5,3},{7,5},{8,14},{10,8},{12,... | collective-permute-start | bytes 1179656 | tf_op jit(solution)/shard_map/ppermute | solution.py:30
  58.8 17.1 %collective-permute-start.11 = (bf16[96,2048]{1,0:T(8,128)(2,1)S(1)}, bf16[96,2048]{1,0:T(8,128)(2,1)S(1)}, u32[]{:S(2)}, u32[]{:S(2)}) collective-permute-start(bf16[96,2048]{1,0:T(8,128)(2,1)S(1)} %slice.17.refs_4_), channel_id=1, source_target_pairs={{0,4},{2,6},{4,0},{6,2},{1,5},{3,7},{5,1},{7,3},{8,12},{10,14},{12... | collective-permute-start | bytes 1179656 | tf_op jit(solution)/shard_map/ppermute | solution.py:30
  59.8 19.3 %collective-permute-start.12 = (bf16[96,2048]{1,0:T(8,128)(2,1)S(1)}, bf16[96,2048]{1,0:T(8,128)(2,1)S(1)}, u32[]{:S(2)}, u32[]{:S(2)}) collective-permute-start(bf16[96,2048]{1,0:T(8,128)(2,1)S(1)} %slice.17.refs_4_), channel_id=1, source_target_pairs={{0,2},{2,4},{4,6},{6,0},{1,3},{3,5},{5,7},{7,1},{8,10},{10,12},{12... | collective-permute-start | bytes 1179656 | tf_op jit(solution)/shard_map/ppermute | solution.py:30
  63.5 32.2 %copy-start.16 = (bf16[4,24,3072]{2,1,0:T(8,128)(2,1)}, bf16[4,24,3072]{2,1,0:T(8,128)(2,1)S(1)}, u32[]{:S(2)}) copy-start(bf16[4,24,3072]{2,1,0:T(8,128)(2,1)S(1)} %pad_maximum_fusion) | copy-start | bytes 1769476
  63.6 15.5 %collective-permute-start.4 = (bf16[96,2048]{1,0:T(8,128)(2,1)S(1)}, bf16[96,2048]{1,0:T(8,128)(2,1)S(1)}, u32[]{:S(2)}, u32[]{:S(2)}) collective-permute-start(bf16[96,2048]{1,0:T(8,128)(2,1)S(1)} %slice.16.refs_0_), channel_id=1, source_target_pairs={{0,24},{8,0},{16,8},{24,16},{1,25},{9,1},{17,9},{25,17},{2,26},{10... | collective-permute-start | bytes 1179656 | tf_op jit(solution)/shard_map/ppermute | solution.py:30
  75.3 13.5 %collective-permute-start.5 = (bf16[96,2048]{1,0:T(8,128)(2,1)S(1)}, bf16[96,2048]{1,0:T(8,128)(2,1)S(1)}, u32[]{:S(2)}, u32[]{:S(2)}) collective-permute-start(bf16[96,2048]{1,0:T(8,128)(2,1)S(1)} %slice.16.refs_0_), channel_id=1, source_target_pairs={{0,16},{8,24},{16,0},{24,8},{1,17},{9,25},{17,1},{25,9},{2,18},{10... | collective-permute-start | bytes 1179656 | tf_op jit(solution)/shard_map/ppermute | solution.py:30
  75.9 19.9 %collective-permute-start.6 = (bf16[96,2048]{1,0:T(8,128)(2,1)S(1)}, bf16[96,2048]{1,0:T(8,128)(2,1)S(1)}, u32[]{:S(2)}, u32[]{:S(2)}) collective-permute-start(bf16[96,2048]{1,0:T(8,128)(2,1)S(1)} %slice.16.refs_0_), channel_id=1, source_target_pairs={{0,8},{8,16},{16,24},{24,0},{1,9},{9,17},{17,25},{25,1},{2,10},{10... | collective-permute-start | bytes 1179656 | tf_op jit(solution)/shard_map/ppermute | solution.py:30
  100.4 2.8 %collective-permute-start.32 = (bf16[288,2048]{1,0:T(8,128)(2,1)S(1)}, bf16[288,2048]{1,0:T(8,128)(2,1)S(1)}, u32[]{:S(2)}, u32[]{:S(2)}) collective-permute-start(bf16[288,2048]{1,0:T(8,128)(2,1)S(1)} %get-tuple-element.64), channel_id=1, source_target_pairs={{0,1},{1,0},{2,3},{3,2},{4,5},{5,4},{6,7},{7,6},{8,9},{9,8},{10,11... | collective-permute-start | bytes 3538952 | tf_op jit(solution)/shard_map/ppermute | solution.py:25
  104.8 78.7 %all-to-all-start.1 = ((bf16[32,144,128]{2,1,0:T(8,128)(2,1)}), bf16[32,144,128]{2,1,0:T(8,128)(2,1)S(1)}, u32[]{:S(2)}, u32[]{:S(2)}) async-start(bf16[32,144,128]{2,1,0:T(8,128)(2,1)} %shard_map.143), calls=%async_computation.1 | async-start | bytes 2359296 | tf_op jit(solution)/shard_map/all_to_all | solution.py:21
  111.4 12.0 %collective-permute-start.16 = (bf16[96,1024]{1,0:T(8,128)(2,1)S(1)}, bf16[96,1024]{1,0:T(8,128)(2,1)S(1)}, u32[]{:S(2)}, u32[]{:S(2)}) collective-permute-start(bf16[96,1024]{1,0:T(8,128)(2,1)S(1)} %slice.19.refs_4_), channel_id=1, source_target_pairs={{0,6},{2,0},{4,2},{6,4},{1,7},{3,1},{5,3},{7,5},{8,14},{10,8},{12,... | collective-permute-start | bytes 589832 | tf_op jit(solution)/shard_map/ppermute | solution.py:30
  115.3 13.4 %collective-permute-start.17 = (bf16[96,1024]{1,0:T(8,128)(2,1)S(1)}, bf16[96,1024]{1,0:T(8,128)(2,1)S(1)}, u32[]{:S(2)}, u32[]{:S(2)}) collective-permute-start(bf16[96,1024]{1,0:T(8,128)(2,1)S(1)} %slice.19.refs_4_), channel_id=1, source_target_pairs={{0,4},{2,6},{4,0},{6,2},{1,5},{3,7},{5,1},{7,3},{8,12},{10,14},{12... | collective-permute-start | bytes 589832 | tf_op jit(solution)/shard_map/ppermute | solution.py:30
  115.3 13.4 %collective-permute-start.18 = (bf16[96,1024]{1,0:T(8,128)(2,1)S(1)}, bf16[96,1024]{1,0:T(8,128)(2,1)S(1)}, u32[]{:S(2)}, u32[]{:S(2)}) collective-permute-start(bf16[96,1024]{1,0:T(8,128)(2,1)S(1)} %slice.19.refs_4_), channel_id=1, source_target_pairs={{0,2},{2,4},{4,6},{6,0},{1,3},{3,5},{5,7},{7,1},{8,10},{10,12},{12... | collective-permute-start | bytes 589832 | tf_op jit(solution)/shard_map/ppermute | solution.py:30
  117.2 16.8 %collective-permute-start.13 = (bf16[96,1024]{1,0:T(8,128)(2,1)S(1)}, bf16[96,1024]{1,0:T(8,128)(2,1)S(1)}, u32[]{:S(2)}, u32[]{:S(2)}) collective-permute-start(bf16[96,1024]{1,0:T(8,128)(2,1)S(1)} %slice.18.refs_0_), channel_id=1, source_target_pairs={{0,24},{8,0},{16,8},{24,16},{1,25},{9,1},{17,9},{25,17},{2,26},{10... | collective-permute-start | bytes 589832 | tf_op jit(solution)/shard_map/ppermute | solution.py:30
  119.9 14.1 %collective-permute-start.14 = (bf16[96,1024]{1,0:T(8,128)(2,1)S(1)}, bf16[96,1024]{1,0:T(8,128)(2,1)S(1)}, u32[]{:S(2)}, u32[]{:S(2)}) collective-permute-start(bf16[96,1024]{1,0:T(8,128)(2,1)S(1)} %slice.18.refs_0_), channel_id=1, source_target_pairs={{0,16},{8,24},{16,0},{24,8},{1,17},{9,25},{17,1},{25,9},{2,18},{10... | collective-permute-start | bytes 589832 | tf_op jit(solution)/shard_map/ppermute | solution.py:30
  123.4 14.6 %collective-permute-start.15 = (bf16[96,1024]{1,0:T(8,128)(2,1)S(1)}, bf16[96,1024]{1,0:T(8,128)(2,1)S(1)}, u32[]{:S(2)}, u32[]{:S(2)}) collective-permute-start(bf16[96,1024]{1,0:T(8,128)(2,1)S(1)} %slice.18.refs_0_), channel_id=1, source_target_pairs={{0,8},{8,16},{16,24},{24,0},{1,9},{9,17},{17,25},{25,1},{2,10},{10... | collective-permute-start | bytes 589832 | tf_op jit(solution)/shard_map/ppermute | solution.py:30
  124.9 1.0 copy-start.14
  128.7 19.7 %collective-permute-start.26 = (bf16[96,2048]{1,0:T(8,128)(2,1)S(1)}, bf16[96,2048]{1,0:T(8,128)(2,1)S(1)}, u32[]{:S(2)}, u32[]{:S(2)}) collective-permute-start(bf16[96,2048]{1,0:T(8,128)(2,1)S(1)} %get-tuple-element.56), channel_id=1, source_target_pairs={{0,2},{2,4},{4,6},{6,0},{1,3},{3,5},{5,7},{7,1},{8,10},{10,12},{12... | collective-permute-start | bytes 1179656 | tf_op jit(solution)/shard_map/ppermute | solution.py:30
  139.2 1.6 collective-permute-start.19
  142.4 29.0 %collective-permute-start.20 = (bf16[96,2304]{1,0:T(8,128)(2,1)}, bf16[96,2304]{1,0:T(8,128)(2,1)S(1)}, u32[]{:S(2)}, u32[]{:S(2)}) collective-permute-start(bf16[96,2304]{1,0:T(8,128)(2,1)} %get-tuple-element.46), channel_id=1, source_target_pairs={{0,8},{8,16},{16,24},{24,0},{1,9},{9,17},{17,25},{25,1},{2,10},{10... | collective-permute-start | bytes 1327112 | tf_op jit(solution)/shard_map/ppermute | solution.py:30
  142.4 12.9 %collective-permute-start.27 = (bf16[96,2048]{1,0:T(8,128)(2,1)}, bf16[96,2048]{1,0:T(8,128)(2,1)S(1)}, u32[]{:S(2)}, u32[]{:S(2)}) collective-permute-start(bf16[96,2048]{1,0:T(8,128)(2,1)} %get-tuple-element.57), channel_id=1, source_target_pairs={{0,4},{2,6},{4,0},{6,2},{1,5},{3,7},{5,1},{7,3},{8,12},{10,14},{12... | collective-permute-start | bytes 1179656 | tf_op jit(solution)/shard_map/ppermute | solution.py:30
  142.4 21.3 %collective-permute-start.28 = (bf16[96,2048]{1,0:T(8,128)(2,1)}, bf16[96,2048]{1,0:T(8,128)(2,1)}, u32[]{:S(2)}, u32[]{:S(2)}) collective-permute-start(bf16[96,2048]{1,0:T(8,128)(2,1)} %get-tuple-element.58), channel_id=1, source_target_pairs={{0,6},{2,0},{4,2},{6,4},{1,7},{3,1},{5,3},{7,5},{8,14},{10,8},{12,... | collective-permute-start | bytes 1179656 | tf_op jit(solution)/shard_map/ppermute | solution.py:30
  144.9 28.0 %collective-permute-start.21 = (bf16[96,2304]{1,0:T(8,128)(2,1)}, bf16[96,2304]{1,0:T(8,128)(2,1)S(1)}, u32[]{:S(2)}, u32[]{:S(2)}) collective-permute-start(bf16[96,2304]{1,0:T(8,128)(2,1)} %get-tuple-element.47), channel_id=1, source_target_pairs={{0,16},{8,24},{16,0},{24,8},{1,17},{9,25},{17,1},{25,9},{2,18},{10... | collective-permute-start | bytes 1327112 | tf_op jit(solution)/shard_map/ppermute | solution.py:30
  149.1 23.7 %collective-permute-start.22 = (bf16[96,2304]{1,0:T(8,128)(2,1)}, bf16[96,2304]{1,0:T(8,128)(2,1)S(1)}, u32[]{:S(2)}, u32[]{:S(2)}) collective-permute-start(bf16[96,2304]{1,0:T(8,128)(2,1)} %get-tuple-element.48), channel_id=1, source_target_pairs={{0,24},{8,0},{16,8},{24,16},{1,25},{9,1},{17,9},{25,17},{2,26},{10... | collective-permute-start | bytes 1327112 | tf_op jit(solution)/shard_map/ppermute | solution.py:30
  163.7 1.0 copy-start.1
  164.7 1.0 copy-start.3
  166.9 11.4 %collective-permute-start.29 = (bf16[24,2048]{1,0:T(8,128)(2,1)S(1)}, bf16[24,2048]{1,0:T(8,128)(2,1)S(1)}, u32[]{:S(2)}, u32[]{:S(2)}) collective-permute-start(bf16[24,2048]{1,0:T(8,128)(2,1)S(1)} %get-tuple-element.60), channel_id=1, source_target_pairs={{0,8},{8,16},{16,24},{24,0},{1,9},{9,17},{17,25},{25,1},{2,10},{10... | collective-permute-start | bytes 294920 | tf_op jit(solution)/shard_map/ppermute | solution.py:30
  167.7 10.6 %collective-permute-start.30 = (bf16[24,2048]{1,0:T(8,128)(2,1)S(1)}, bf16[24,2048]{1,0:T(8,128)(2,1)S(1)}, u32[]{:S(2)}, u32[]{:S(2)}) collective-permute-start(bf16[24,2048]{1,0:T(8,128)(2,1)S(1)} %get-tuple-element.61), channel_id=1, source_target_pairs={{0,16},{8,24},{16,0},{24,8},{1,17},{9,25},{17,1},{25,9},{2,18},{10... | collective-permute-start | bytes 294920 | tf_op jit(solution)/shard_map/ppermute | solution.py:30
  171.4 6.9 %collective-permute-start.31 = (bf16[24,2048]{1,0:T(8,128)(2,1)S(1)}, bf16[24,2048]{1,0:T(8,128)(2,1)S(1)}, u32[]{:S(2)}, u32[]{:S(2)}) collective-permute-start(bf16[24,2048]{1,0:T(8,128)(2,1)S(1)} %get-tuple-element.62), channel_id=1, source_target_pairs={{0,24},{8,0},{16,8},{24,16},{1,25},{9,1},{17,9},{25,17},{2,26},{10... | collective-permute-start | bytes 294920 | tf_op jit(solution)/shard_map/ppermute | solution.py:30
  172.9 10.7 %copy-start.7 = (f32[64,352]{1,0:T(8,128)S(1)}, f32[64,352]{1,0:T(8,128)}, u32[]{:S(2)}) copy-start(f32[64,352]{1,0:T(8,128)} %gate.3) | copy-start | bytes 270340
  172.9 10.7 %copy-start.8 = (f32[64,352]{1,0:T(8,128)S(1)}, f32[64,352]{1,0:T(8,128)}, u32[]{:S(2)}) copy-start(f32[64,352]{1,0:T(8,128)} %up.3) | copy-start | bytes 270340
  172.9 10.7 %copy-start.9 = (f32[352,64]{0,1:T(8,128)S(1)}, f32[352,64]{0,1:T(8,128)}, u32[]{:S(2)}) copy-start(f32[352,64]{0,1:T(8,128)} %param.17) | copy-start | bytes 270340
  174.4 6.4 %collective-permute-start.23 = (bf16[24,2048]{1,0:T(8,128)(2,1)S(1)}, bf16[24,2048]{1,0:T(8,128)(2,1)S(1)}, u32[]{:S(2)}, u32[]{:S(2)}) collective-permute-start(bf16[24,2048]{1,0:T(8,128)(2,1)S(1)} %get-tuple-element.50), channel_id=1, source_target_pairs={{0,2},{2,4},{4,6},{6,0},{1,3},{3,5},{5,7},{7,1},{8,10},{10,12},{12... | collective-permute-start | bytes 294920 | tf_op jit(solution)/shard_map/ppermute | solution.py:30
  174.7 7.2 %collective-permute-start.24 = (bf16[24,2048]{1,0:T(8,128)(2,1)S(1)}, bf16[24,2048]{1,0:T(8,128)(2,1)S(1)}, u32[]{:S(2)}, u32[]{:S(2)}) collective-permute-start(bf16[24,2048]{1,0:T(8,128)(2,1)S(1)} %get-tuple-element.51), channel_id=1, source_target_pairs={{0,4},{2,6},{4,0},{6,2},{1,5},{3,7},{5,1},{7,3},{8,12},{10,14},{12... | collective-permute-start | bytes 294920 | tf_op jit(solution)/shard_map/ppermute | solution.py:30
  178.2 4.6 %collective-permute-start.25 = (bf16[24,2048]{1,0:T(8,128)(2,1)S(1)}, bf16[24,2048]{1,0:T(8,128)(2,1)S(1)}, u32[]{:S(2)}, u32[]{:S(2)}) collective-permute-start(bf16[24,2048]{1,0:T(8,128)(2,1)S(1)} %get-tuple-element.52), channel_id=1, source_target_pairs={{0,6},{2,0},{4,2},{6,4},{1,7},{3,1},{5,3},{7,5},{8,14},{10,8},{12,... | collective-permute-start | bytes 294920 | tf_op jit(solution)/shard_map/ppermute | solution.py:30
  (4 other events, 3.0 us)

commit v3 on v2

--- a/solution.py
+++ b/solution.py
@@ -52,19 +52,30 @@
 LANES = 128
 
 
-def whole(kernel, out_shape, inputs, scratch=(), flops=0, grant=12, scalars=0):
-    spec = pl.BlockSpec(memory_space=pltpu.VMEM)
-    count = len(inputs) - scalars
+def whole(kernel, out_shape, inputs, scratch=(), flops=0, grant=12, spaces=None, result=pltpu.VMEM):
+    spec = pl.BlockSpec(memory_space=result)
+    spaces = spaces or [pltpu.VMEM] * len(inputs)
     single = not isinstance(out_shape, tuple)
     return pl.pallas_call(
         kernel,
         out_shape=out_shape,
-        in_specs=[pl.BlockSpec(memory_space=pltpu.SMEM)] * scalars + [spec] * count,
+        in_specs=[pl.BlockSpec(memory_space=space) for space in spaces],
         out_specs=spec if single else tuple(spec for _ in out_shape),
         scratch_shapes=scratch,
-        compiler_params=pltpu.CompilerParams(vmem_limit_bytes=grant * 2**20),
+        compiler_params=pltpu.CompilerParams(vmem_limit_bytes=int(grant * 2**20)),
         cost_estimate=pl.CostEstimate(flops=flops, bytes_accessed=0, transcendentals=0),
     )(*inputs)
+
+
+def fetched(sources, target, sems, first=0):
+    rows = target.shape[0] // len(sources)
+    copies = [
+        pltpu.make_async_copy(source, target.at[pl.ds(k * rows, rows)], sems.at[first + k])
+        for k, source in enumerate(sources)
+    ]
+    for copy in copies:
+        copy.start()
+    return copies
 
 
 def like(shape, kind):
@@ -79,7 +90,15 @@
     return low, high
 
 
-def front_kernel(copies, part, pad, x_next, x_prev, grad_out, gate, up, down_t, first, second, out):
+def front_kernel(copies, part, pad, *refs):
+    sources, (first, second, out), refs = refs[:6], refs[6:9], refs[9:]
+    targets, sems = refs[:6], refs[6]
+    moves = [pltpu.make_async_copy(*pair, sems.at[k]) for k, pair in enumerate(zip(sources, targets))]
+    for move in moves:
+        move.start()
+    for move in moves:
+        move.wait()
+    x_next, x_prev, grad_out, gate, up, down_t = targets
     width = x_prev.shape[1]
     mid = width // 2
     first[:, :width] = x_prev[...]
@@ -112,9 +131,7 @@
     )
 
 
-def backward_kernel(ny, nx, rows, pad, own, other, *refs):
-    firsts, seconds = refs[:ny], refs[ny : ny + nx]
-    kept, sent, gate_up, down, grads, prev, cotangent = refs[ny + nx :]
+def unpack_kernel(pad, own, other, gate_up, down):
     half = pad // 2
     for base, packed in ((0, own), (pad, other)):
         for tile in range(packed.shape[0] // 2):
@@ -124,10 +141,9 @@
             gate_up[pl.ds(2 * pad + base, pad), at] = high[:pad].astype(BF16)
             down[pl.ds(base, half), at] = low[pad:].astype(BF16)
             down[pl.ds(base + half, half), at] = high[pad:].astype(BF16)
-    for k in range(ny):
-        prev[pl.ds(k * nx * rows, nx * rows)] = firsts[k][...]
-    for k in range(nx):
-        cotangent[pl.ds(k * ny * rows, ny * rows)] = seconds[k][...]
+
+
+def backward_kernel(ny, nx, rows, pad, gate_up, down, prev, cotangent, kept, sent, grads):
     pre = dot(prev[...], gate_up[...], ((1,), (1,)))
     gate_prev, up_prev = pre[:, : 2 * pad], pre[:, 2 * pad :]
     grad_hidden = turned(dot(cotangent[...], down[...], ((1,), (1,))), nx, ny, rows)
@@ -193,14 +209,13 @@
 
 def hidden_kernel(ny, nx, rows, pad, gate_up, *refs):
     firsts, seconds = refs[:ny], refs[ny : ny + nx]
-    mine, theirs, hidden, tokens = refs[ny + nx :]
-    half = tokens.shape[1]
-    for k in range(ny):
-        tokens[pl.ds(k * nx * rows, nx * rows)] = firsts[k][...]
-    pre = dot(tokens[...], gate_up[:, :half], ((1,), (1,)))
-    for k in range(nx):
-        tokens[pl.ds(k * ny * rows, ny * rows)] = seconds[k][...]
-    pre = pre + turned(dot(tokens[...], gate_up[:, half:], ((1,), (1,))), nx, ny, rows)
+    mine, theirs, hidden, left, right, sems = refs[ny + nx :]
+    half = left.shape[1]
+    moves = fetched(firsts, left, sems) + fetched(seconds, right, sems, ny)
+    for move in moves:
+        move.wait()
+    pre = dot(left[...], gate_up[:, :half], ((1,), (1,)))
+    pre = pre + turned(dot(right[...], gate_up[:, half:], ((1,), (1,))), nx, ny, rows)
     value = jax.nn.silu(pre[:, : 2 * pad]) * pre[:, 2 * pad :]
     blank = jnp.zeros((value.shape[0], LANES - pad), F32)
     mine[...] = jnp.concatenate((value[:, :pad], blank), axis=1).astype(BF16)
@@ -259,6 +274,14 @@
         functools.partial(front_kernel, nz, part, pad),
         (like((rows, width + mid), BF16), like((rows, width + mid), BF16), like(block, BF16)),
         (x_next, x_prev, grad_out, gate_w, up_w, down_w.T),
+        (
+            *(pltpu.VMEM((rows, width), BF16) for _ in range(3)),
+            *(pltpu.VMEM((width // (nz * ny), units), BF16) for _ in range(3)),
+            pltpu.SemaphoreType.DMA((6,)),
+        ),
+        grant=60,
+        spaces=[pltpu.HBM] * 6,
+        result=None,
     )
 
     own = spread(packed, FS)
@@ -271,19 +294,19 @@
     nexts = around(first[:, width:], "y")
     nexts = nexts + around(second[:, width:], "x")
 
-    kept, sent, gate_up, down, grads = whole(
+    gate_up, down = whole(
+        functools.partial(unpack_kernel, pad),
+        (like((4 * pad, width), BF16), like((2 * pad, width), BF16)),
+        (own, other),
+    )
+
+    prev = jnp.concatenate(prevs)
+    cotangent = jnp.concatenate(cotangents)
+    kept, sent, grads = whole(
         functools.partial(backward_kernel, ny, nx, rows, pad),
-        (
-            like((3 * pad, width), F32),
-            like((3 * pad, width), BF16),
-            like((4 * pad, width), BF16),
-            like((2 * pad, width), BF16),
-            like((group, 4 * pad), BF16),
-        ),
-        (own, other, *prevs, *cotangents),
-        (pltpu.VMEM((group, width), BF16), pltpu.VMEM((group, width), BF16)),
+        (like((3 * pad, width), F32), like((3 * pad, width), BF16), like((group, 4 * pad), BF16)),
+        (gate_up, down, prev, cotangent),
         flops=6 * token_ops,
-        grant=20,
     )
     received = swapped(sent)
     input_parts = whole(
@@ -312,8 +335,13 @@
         functools.partial(hidden_kernel, ny, nx, rows, pad),
         (like((group, LANES), BF16), like((group, LANES), BF16), like((group, 2 * pad), BF16)),
         (gate_up, *nexts),
-        (pltpu.VMEM((group, mid), BF16),),
+        (
+            pltpu.VMEM((group, mid), BF16),
+            pltpu.VMEM((group, mid), BF16),
+            pltpu.SemaphoreType.DMA((ny + nx,)),
+        ),
         flops=2 * token_ops,
+        spaces=[pltpu.VMEM] + [pltpu.HBM] * (ny + nx),
     )
     partner = swapped(theirs)
     out_parts = whole(
@@ -335,7 +363,7 @@
             pltpu.VMEM((ny, nx * rows, 2 * LANES), F32),
             pltpu.VMEM((nx, nc * rows, units), F32),
         ),
-        scalars=1,
+        spaces=[pltpu.SMEM] + [pltpu.VMEM] * ny,
     )
     out_next = added(for_owner(by_y, "x"))
     return out_next, saved, grad_input, new_gate, new_up, new_down_t.T

time: 187 us -> 179 us (0.957)
  the two profiles are of different devices: /device:TPU:64 before, /device:TPU:96 now
where the time goes in v3:
time: 179 us; the launch traced here: 178 us
  starting transfers between devices  81.2 us (45%)
  waiting for transfers between devices  68.1 us (38%)
  Pallas kernels  19.1 us (11%)
  local copies, waits for them, and re-layouts  7.13 us (4%)
  other arithmetic  1.94 us (1%)
    ppermute x30, starting transfers between devices, moved(): lax.ppermute(array, axis, [(i, (i + step) % length) for i in range(length)])  58.8 us
    ppermute x30, waiting for transfers between devices, moved(): lax.ppermute(array, axis, [(i, (i + step) % length) for i in range(length)])  45.8 us
    all_to_all x2, starting transfers between devices, spread(): return lax.all_to_all(blocks, axis, 0, 0, tiled=True)  22.3 us
    pallas_call x10, Pallas kernels, whole(): pl.pallas_call(kernel, out_shape=out_shape, in_specs=[pl.BlockSpec(memory...  19.1 us
    all_to_all x2, waiting for transfers between devices, spread(): return lax.all_to_all(blocks, axis, 0, 0, tiled=True)  18.1 us
    unnamed x26, local copies, waits for them, and re-layouts  5.19 us
    ppermute x3, waiting for transfers between devices, swapped(): return lax.ppermute(array, 'c', [(0, 1), (1, 0)])  4.14 us
  transfers between devices with their start and end apart: 35, of which 12 were waited for; matrix products, arithmetic and copies ran while one was open for 2% of the time, Pallas kernels for 5%

profile of v3, /device:TPU:96, one launch (start us, length us, event | category | flops | bytes accessed | tf_op | source)
XLA Modules:
  0.0 178.3 jit_solution(9946933141414236402)
XLA Ops:
  0.6 2.4 %shard_map.136 = (bf16[24,3072]{1,0:T(8,128)(2,1)}, bf16[24,3072]{1,0:T(8,128)(2,1)}, bf16[32,144,128]{2,1,0:T(8,128)(2,1)}) custom-call(bf16[24,2048]{1,0:T(8,128)(2,1)} %refs_0_.1, bf16[24,2048]{1,0:T(8,128)(2,1)} %refs_1_.1, bf16[24,2048]{1,0:T(8,128)(2,1)} %refs_2_.1, bf16[64,352]{1,0:T(8,128)(2,1)} %refs_3_.1, bf16[64,352]{1,0:T(8,128)(2,1)} %refs_4_.1, ...), custom_call_target="tpu_custom_call" | custom-call | tf_op jit(solution)/shard_map/pallas_call | solution.py:59
  3.0 10.6 %all-to-all-start = ((bf16[32,144,128]{2,1,0:T(8,128)(2,1)}), bf16[32,144,128]{2,1,0:T(8,128)(2,1)S(1)}, u32[]{:S(2)}, u32[]{:S(2)}) async-start(bf16[32,144,128]{2,1,0:T(8,128)(2,1)} %get-tuple-element.37), calls=%async_computation | async-start | bytes 2359296 | tf_op jit(solution)/shard_map/all_to_all | solution.py:21
  13.6 1.6 collective-permute-start.3
  15.2 2.7 %collective-permute-start.2 = (bf16[24,3072]{1,0:T(8,128)(2,1)S(1)}, bf16[24,3072]{1,0:T(8,128)(2,1)S(1)}, u32[]{:S(2)}, u32[]{:S(2)}) collective-permute-start(bf16[24,3072]{1,0:T(8,128)(2,1)S(1)} %copy-done.12), channel_id=1, source_target_pairs={{0,4},{2,6},{4,0},{6,2},{1,5},{3,7},{5,1},{7,3},{8,12},{10,14},{12... | collective-permute-start | bytes 442376 | tf_op jit(solution)/shard_map/ppermute | solution.py:30
  17.9 1.4 collective-permute-start.1
  19.4 1.5 collective-permute-start.9
  20.8 2.7 %collective-permute-start.8 = (bf16[24,3072]{1,0:T(8,128)(2,1)S(1)}, bf16[24,3072]{1,0:T(8,128)(2,1)S(1)}, u32[]{:S(2)}, u32[]{:S(2)}) collective-permute-start(bf16[24,3072]{1,0:T(8,128)(2,1)S(1)} %copy-done.11), channel_id=1, source_target_pairs={{0,16},{8,24},{16,0},{24,8},{1,17},{9,25},{17,1},{25,9},{2,18},{10... | collective-permute-start | bytes 442376 | tf_op jit(solution)/shard_map/ppermute | solution.py:30
  23.5 1.5 collective-permute-start.7
  25.0 18.1 %all-to-all-done.own = bf16[32,144,128]{2,1,0:T(8,128)(2,1)S(1)} async-done(((bf16[32,144,128]{2,1,0:T(8,128)(2,1)}), bf16[32,144,128]{2,1,0:T(8,128)(2,1)S(1)}, u32[]{:S(2)}, u32[]{:S(2)}) %all-to-all-start) | async-done | bytes 1179680 | tf_op jit(solution)/shard_map/all_to_all | solution.py:21
  43.3 2.8 %collective-permute-start.21 = (bf16[96,2048]{1,0:T(8,128)(2,1)S(1)}, bf16[96,2048]{1,0:T(8,128)(2,1)S(1)}, u32[]{:S(2)}, u32[]{:S(2)}) collective-permute-start(bf16[96,2048]{1,0:T(8,128)(2,1)S(1)} %slice.18), channel_id=1, source_target_pairs={{0,16},{8,24},{16,0},{24,8},{1,17},{9,25},{17,1},{25,9},{2,18},{10... | collective-permute-start | bytes 1179656 | tf_op jit(solution)/shard_map/ppermute | solution.py:30
  46.1 1.2 collective-permute-start.20
  47.4 1.6 collective-permute-start.25
  49.0 15.5 %collective-permute-done.22 = bf16[96,2048]{1,0:T(8,128)(2,1)S(1)} collective-permute-done((bf16[96,2048]{1,0:T(8,128)(2,1)S(1)}, bf16[96,2048]{1,0:T(8,128)(2,1)S(1)}, u32[]{:S(2)}, u32[]{:S(2)}) %collective-permute-start.22) | collective-permute-done | bytes 393248 | tf_op jit(solution)/shard_map/ppermute | solution.py:30
  64.5 3.0 %collective-permute-start.24 = (bf16[96,2048]{1,0:T(8,128)(2,1)S(1)}, bf16[96,2048]{1,0:T(8,128)(2,1)S(1)}, u32[]{:S(2)}, u32[]{:S(2)}) collective-permute-start(bf16[96,2048]{1,0:T(8,128)(2,1)S(1)} %slice.19), channel_id=1, source_target_pairs={{0,4},{2,6},{4,0},{6,2},{1,5},{3,7},{5,1},{7,3},{8,12},{10,14},{12... | collective-permute-start | bytes 1179656 | tf_op jit(solution)/shard_map/ppermute | solution.py:30
  67.5 1.1 collective-permute-start.23
  68.8 4.9 %collective-permute-done.24 = bf16[96,2048]{1,0:T(8,128)(2,1)S(1)} collective-permute-done((bf16[96,2048]{1,0:T(8,128)(2,1)S(1)}, bf16[96,2048]{1,0:T(8,128)(2,1)S(1)}, u32[]{:S(2)}, u32[]{:S(2)}) %collective-permute-start.24) | collective-permute-done | bytes 393248 | tf_op jit(solution)/shard_map/ppermute | solution.py:30
  73.8 5.5 %collective-permute-done.23 = bf16[96,2048]{1,0:T(8,128)(2,1)S(1)} collective-permute-done((bf16[96,2048]{1,0:T(8,128)(2,1)S(1)}, bf16[96,2048]{1,0:T(8,128)(2,1)S(1)}, u32[]{:S(2)}, u32[]{:S(2)}) %collective-permute-start.23) | collective-permute-done | bytes 393248 | tf_op jit(solution)/shard_map/ppermute | solution.py:30
  79.4 1.0 shard_map.137
  80.4 3.6 %shard_map.141 = (f32[288,2048]{1,0:T(8,128)S(1)}, bf16[288,2048]{1,0:T(8,128)(2,1)S(1)}, bf16[384,384]{1,0:T(8,128)(2,1)S(1)}) custom-call(bf16[384,2048]{1,0:T(8,128)(2,1)S(1)} %get-tuple-element.38.gate_up, bf16[192,2048]{1,0:T(8,128)(2,1)S(1)} %get-tuple-element.42.down, bf16[384,2048]{1,0:T(8,128)(2,1)S(1)} %pad_maximum_fusion.prev, ...), custom_call_target="tpu_custom_call" | custom-call | flops 1811939328 | tf_op jit(solution)/shard_map/pallas_call | solution.py:59
  84.8 2.8 %collective-permute-done.32.received = bf16[288,2048]{1,0:T(8,128)(2,1)S(1)} collective-permute-done((bf16[288,2048]{1,0:T(8,128)(2,1)S(1)}, bf16[288,2048]{1,0:T(8,128)(2,1)S(1)}, u32[]{:S(2)}, u32[]{:S(2)}) %collective-permute-start.32) | collective-permute-done | bytes 1179680 | tf_op jit(solution)/shard_map/ppermute | solution.py:25
  87.6 1.6 shard_map.144
  89.2 11.7 %all-to-all-start.1 = ((bf16[32,144,128]{2,1,0:T(8,128)(2,1)}), bf16[32,144,128]{2,1,0:T(8,128)(2,1)S(1)}, u32[]{:S(2)}, u32[]{:S(2)}) async-start(bf16[32,144,128]{2,1,0:T(8,128)(2,1)} %shard_map.144), calls=%async_computation.1 | async-start | bytes 2359296 | tf_op jit(solution)/shard_map/all_to_all | solution.py:21
  100.9 0.9 slice.16.refs_0_
  101.8 2.8 %collective-permute-start.4 = (bf16[96,1024]{1,0:T(8,128)(2,1)S(1)}, bf16[96,1024]{1,0:T(8,128)(2,1)S(1)}, u32[]{:S(2)}, u32[]{:S(2)}) collective-permute-start(bf16[96,1024]{1,0:T(8,128)(2,1)S(1)} %slice.16.refs_0_), channel_id=1, source_target_pairs={{0,24},{8,0},{16,8},{24,16},{1,25},{9,1},{17,9},{25,17},{2,26},{10... | collective-permute-start | bytes 589832 | tf_op jit(solution)/shard_map/ppermute | solution.py:30
  106.3 0.9 slice.17.refs_4_
  107.2 2.7 %collective-permute-start.10 = (bf16[96,1024]{1,0:T(8,128)(2,1)S(1)}, bf16[96,1024]{1,0:T(8,128)(2,1)S(1)}, u32[]{:S(2)}, u32[]{:S(2)}) collective-permute-start(bf16[96,1024]{1,0:T(8,128)(2,1)S(1)} %slice.17.refs_4_), channel_id=1, source_target_pairs={{0,6},{2,0},{4,2},{6,4},{1,7},{3,1},{5,3},{7,5},{8,14},{10,8},{12,... | collective-permute-start | bytes 589832 | tf_op jit(solution)/shard_map/ppermute | solution.py:30
  110.8 3.1 %collective-permute-done.4.refs_1_ = bf16[96,1024]{1,0:T(8,128)(2,1)S(1)} collective-permute-done((bf16[96,1024]{1,0:T(8,128)(2,1)S(1)}, bf16[96,1024]{1,0:T(8,128)(2,1)S(1)}, u32[]{:S(2)}, u32[]{:S(2)}) %collective-permute-start.4) | collective-permute-done | bytes 196640 | tf_op jit(solution)/shard_map/ppermute | solution.py:30
  113.9 1.4 collective-permute-start.12
  115.3 1.0 copy-done.8
  116.2 2.1 %shard_map.142 = (bf16[96,2048]{1,0:T(8,128)(2,1)S(1)}, bf16[96,2048]{1,0:T(8,128)(2,1)S(1)}, bf16[96,2048]{1,0:T(8,128)(2,1)}, bf16[96,2048]{1,0:T(8,128)(2,1)}) custom-call(bf16[384,384]{1,0:T(8,128)(2,1)S(1)} %copy-done.8, bf16[384,2048]{1,0:T(8,128)(2,1)S(1)} %get-tuple-element.38.gate_up), custom_call_target="tpu_custom_call" | custom-call | flops 603979776 | tf_op jit(solution)/shard_map/pallas_call | solution.py:59
  119.6 4.0 %collective-permute-done.6.refs_3_ = bf16[96,1024]{1,0:T(8,128)(2,1)S(1)} collective-permute-done((bf16[96,1024]{1,0:T(8,128)(2,1)S(1)}, bf16[96,1024]{1,0:T(8,128)(2,1)S(1)}, u32[]{:S(2)}, u32[]{:S(2)}) %collective-permute-start.6) | collective-permute-done | bytes 196640 | tf_op jit(solution)/shard_map/ppermute | solution.py:30
  123.6 3.3 %shard_map.138 = (bf16[384,128]{1,0:T(8,128)(2,1)S(1)}, bf16[384,128]{1,0:T(8,128)(2,1)S(1)}, bf16[384,192]{1,0:T(8,128)(2,1)S(1)}) custom-call(bf16[384,2048]{1,0:T(8,128)(2,1)S(1)} %get-tuple-element.38.gate_up, bf16[96,1024]{1,0:T(8,128)(2,1)S(1)} %slice.16.refs_0_, bf16[96,1024]{1,0:T(8,128)(2,1)S(1)} %collective-permute-done.4.refs_1_, ...), custom_call_target="tpu_custom_call" | custom-call | flops 603979776 | tf_op jit(solution)/shard_map/pallas_call | solution.py:59
  127.0 1.3 collective-permute-done.13.partner
  128.3 1.6 shard_map.139
  130.6 2.7 %collective-permute-start.27 = (bf16[96,2048]{1,0:T(8,128)(2,1)}, bf16[96,2048]{1,0:T(8,128)(2,1)S(1)}, u32[]{:S(2)}, u32[]{:S(2)}) collective-permute-start(bf16[96,2048]{1,0:T(8,128)(2,1)} %get-tuple-element.57), channel_id=1, source_target_pairs={{0,4},{2,6},{4,0},{6,2},{1,5},{3,7},{5,1},{7,3},{8,12},{10,14},{12... | collective-permute-start | bytes 1179656 | tf_op jit(solution)/shard_map/ppermute | solution.py:30
  133.9 9.5 %collective-permute-start.15 = (bf16[96,2304]{1,0:T(8,128)(2,1)}, bf16[96,2304]{1,0:T(8,128)(2,1)S(1)}, u32[]{:S(2)}, u32[]{:S(2)}) collective-permute-start(bf16[96,2304]{1,0:T(8,128)(2,1)} %get-tuple-element.47), channel_id=1, source_target_pairs={{0,16},{8,24},{16,0},{24,8},{1,17},{9,25},{17,1},{25,9},{2,18},{10... | collective-permute-start | bytes 1327112 | tf_op jit(solution)/shard_map/ppermute | solution.py:30
  144.2 7.1 %collective-permute-done.28.refs_3_ = bf16[96,2048]{1,0:T(8,128)(2,1)} collective-permute-done((bf16[96,2048]{1,0:T(8,128)(2,1)}, bf16[96,2048]{1,0:T(8,128)(2,1)}, u32[]{:S(2)}, u32[]{:S(2)}) %collective-permute-start.28) | collective-permute-done | bytes 393248 | tf_op jit(solution)/shard_map/ppermute | solution.py:30
  151.3 1.0 copy-done.1
  152.3 1.0 copy-done.3
  153.3 1.2 shard_map.143
  154.5 8.1 %collective-permute-start.31 = (bf16[24,2048]{1,0:T(8,128)(2,1)S(1)}, bf16[24,2048]{1,0:T(8,128)(2,1)S(1)}, u32[]{:S(2)}, u32[]{:S(2)}) collective-permute-start(bf16[24,2048]{1,0:T(8,128)(2,1)S(1)} %get-tuple-element.62), channel_id=1, source_target_pairs={{0,24},{8,0},{16,8},{24,16},{1,25},{9,1},{17,9},{25,17},{2,26},{10... | collective-permute-start | bytes 294920 | tf_op jit(solution)/shard_map/ppermute | solution.py:30
  162.6 1.3 collective-permute-start.30
  163.9 1.3 collective-permute-start.29
  165.3 1.5 shard_map.140
  166.8 2.6 %collective-permute-start.19 = (bf16[24,2048]{1,0:T(8,128)(2,1)S(1)}, bf16[24,2048]{1,0:T(8,128)(2,1)S(1)}, u32[]{:S(2)}, u32[]{:S(2)}) collective-permute-start(bf16[24,2048]{1,0:T(8,128)(2,1)S(1)} %get-tuple-element.52), channel_id=1, source_target_pairs={{0,6},{2,0},{4,2},{6,4},{1,7},{3,1},{5,3},{7,5},{8,14},{10,8},{12,... | collective-permute-start | bytes 294920 | tf_op jit(solution)/shard_map/ppermute | solution.py:30
  171.0 2.0 %collective-permute-done.19 = bf16[24,2048]{1,0:T(8,128)(2,1)S(1)} collective-permute-done((bf16[24,2048]{1,0:T(8,128)(2,1)S(1)}, bf16[24,2048]{1,0:T(8,128)(2,1)S(1)}, u32[]{:S(2)}, u32[]{:S(2)}) %collective-permute-start.19) | collective-permute-done | bytes 98336 | tf_op jit(solution)/shard_map/ppermute | solution.py:30
  173.0 2.6 %collective-permute-done.18 = bf16[24,2048]{1,0:T(8,128)(2,1)S(1)} collective-permute-done((bf16[24,2048]{1,0:T(8,128)(2,1)S(1)}, bf16[24,2048]{1,0:T(8,128)(2,1)S(1)}, u32[]{:S(2)}, u32[]{:S(2)}) %collective-permute-start.18) | collective-permute-done | bytes 98336 | tf_op jit(solution)/shard_map/ppermute | solution.py:30
  175.6 1.1 collective-permute-done.17
  (69 shorter events, 10.7 us)
Async XLA Ops:
  3.0 10.6 %copy-start.12 = (bf16[24,3072]{1,0:T(8,128)(2,1)S(1)}, bf16[24,3072]{1,0:T(8,128)(2,1)}, u32[]{:S(2)}) copy-start(bf16[24,3072]{1,0:T(8,128)(2,1)} %get-tuple-element.39) | copy-start | bytes 442372
  3.0 16.4 %copy-start.11 = (bf16[24,3072]{1,0:T(8,128)(2,1)S(1)}, bf16[24,3072]{1,0:T(8,128)(2,1)}, u32[]{:S(2)}) copy-start(bf16[24,3072]{1,0:T(8,128)(2,1)} %get-tuple-element.40) | copy-start | bytes 442372
  3.0 40.1 %all-to-all-start = ((bf16[32,144,128]{2,1,0:T(8,128)(2,1)}), bf16[32,144,128]{2,1,0:T(8,128)(2,1)S(1)}, u32[]{:S(2)}, u32[]{:S(2)}) async-start(bf16[32,144,128]{2,1,0:T(8,128)(2,1)} %get-tuple-element.37), calls=%async_computation | async-start | bytes 2359296 | tf_op jit(solution)/shard_map/all_to_all | solution.py:21
  13.6 9.9 %collective-permute-start.3 = (bf16[24,3072]{1,0:T(8,128)(2,1)S(1)}, bf16[24,3072]{1,0:T(8,128)(2,1)S(1)}, u32[]{:S(2)}, u32[]{:S(2)}) collective-permute-start(bf16[24,3072]{1,0:T(8,128)(2,1)S(1)} %copy-done.12), channel_id=1, source_target_pairs={{0,2},{2,4},{4,6},{6,0},{1,3},{3,5},{5,7},{7,1},{8,10},{10,12},{12... | collective-permute-start | bytes 442376 | tf_op jit(solution)/shard_map/ppermute | solution.py:30
  15.2 9.8 %collective-permute-start.2 = (bf16[24,3072]{1,0:T(8,128)(2,1)S(1)}, bf16[24,3072]{1,0:T(8,128)(2,1)S(1)}, u32[]{:S(2)}, u32[]{:S(2)}) collective-permute-start(bf16[24,3072]{1,0:T(8,128)(2,1)S(1)} %copy-done.12), channel_id=1, source_target_pairs={{0,4},{2,6},{4,0},{6,2},{1,5},{3,7},{5,1},{7,3},{8,12},{10,14},{12... | collective-permute-start | bytes 442376 | tf_op jit(solution)/shard_map/ppermute | solution.py:30
  17.9 25.2 %collective-permute-start.1 = (bf16[24,3072]{1,0:T(8,128)(2,1)S(1)}, bf16[24,3072]{1,0:T(8,128)(2,1)S(1)}, u32[]{:S(2)}, u32[]{:S(2)}) collective-permute-start(bf16[24,3072]{1,0:T(8,128)(2,1)S(1)} %copy-done.12), channel_id=1, source_target_pairs={{0,6},{2,0},{4,2},{6,4},{1,7},{3,1},{5,3},{7,5},{8,14},{10,8},{12,... | collective-permute-start | bytes 442376 | tf_op jit(solution)/shard_map/ppermute | solution.py:30
  19.4 24.0 %collective-permute-start.9 = (bf16[24,3072]{1,0:T(8,128)(2,1)S(1)}, bf16[24,3072]{1,0:T(8,128)(2,1)S(1)}, u32[]{:S(2)}, u32[]{:S(2)}) collective-permute-start(bf16[24,3072]{1,0:T(8,128)(2,1)S(1)} %copy-done.11), channel_id=1, source_target_pairs={{0,8},{8,16},{16,24},{24,0},{1,9},{9,17},{17,25},{25,1},{2,10},{10... | collective-permute-start | bytes 442376 | tf_op jit(solution)/shard_map/ppermute | solution.py:30
  20.8 25.3 %collective-permute-start.8 = (bf16[24,3072]{1,0:T(8,128)(2,1)S(1)}, bf16[24,3072]{1,0:T(8,128)(2,1)S(1)}, u32[]{:S(2)}, u32[]{:S(2)}) collective-permute-start(bf16[24,3072]{1,0:T(8,128)(2,1)S(1)} %copy-done.11), channel_id=1, source_target_pairs={{0,16},{8,24},{16,0},{24,8},{1,17},{9,25},{17,1},{25,9},{2,18},{10... | collective-permute-start | bytes 442376 | tf_op jit(solution)/shard_map/ppermute | solution.py:30
  23.5 23.8 %collective-permute-start.7 = (bf16[24,3072]{1,0:T(8,128)(2,1)S(1)}, bf16[24,3072]{1,0:T(8,128)(2,1)S(1)}, u32[]{:S(2)}, u32[]{:S(2)}) collective-permute-start(bf16[24,3072]{1,0:T(8,128)(2,1)S(1)} %copy-done.11), channel_id=1, source_target_pairs={{0,24},{8,0},{16,8},{24,16},{1,25},{9,1},{17,9},{25,17},{2,26},{10... | collective-permute-start | bytes 442376 | tf_op jit(solution)/shard_map/ppermute | solution.py:30
  43.1 36.3 %collective-permute-start = (bf16[32,144,128]{2,1,0:T(8,128)(2,1)S(1)}, bf16[32,144,128]{2,1,0:T(8,128)(2,1)S(1)}, u32[]{:S(2)}, u32[]{:S(2)}) collective-permute-start(bf16[32,144,128]{2,1,0:T(8,128)(2,1)S(1)} %all-to-all-done.own), channel_id=1, source_target_pairs={{0,1},{1,0},{2,3},{3,2},{4,5},{5,4},{6,7},{7,6},{8,9},{9,8},{10,11... | collective-permute-start | bytes 3538952 | tf_op jit(solution)/shard_map/ppermute | solution.py:25
  43.2 25.5 %copy-start.9 = (bf16[4,24,3072]{2,1,0:T(8,128)(2,1)}, bf16[4,24,3072]{2,1,0:T(8,128)(2,1)S(1)}, u32[]{:S(2)}) copy-start(bf16[4,24,3072]{2,1,0:T(8,128)(2,1)S(1)} %pad_maximum_fusion.2) | copy-start | bytes 1769476
  43.2 21.2 %collective-permute-start.22 = (bf16[96,2048]{1,0:T(8,128)(2,1)S(1)}, bf16[96,2048]{1,0:T(8,128)(2,1)S(1)}, u32[]{:S(2)}, u32[]{:S(2)}) collective-permute-start(bf16[96,2048]{1,0:T(8,128)(2,1)S(1)} %slice.18), channel_id=1, source_target_pairs={{0,8},{8,16},{16,24},{24,0},{1,9},{9,17},{17,25},{25,1},{2,10},{10... | collective-permute-start | bytes 1179656 | tf_op jit(solution)/shard_map/ppermute | solution.py:30
  43.3 24.2 %collective-permute-start.21 = (bf16[96,2048]{1,0:T(8,128)(2,1)S(1)}, bf16[96,2048]{1,0:T(8,128)(2,1)S(1)}, u32[]{:S(2)}, u32[]{:S(2)}) collective-permute-start(bf16[96,2048]{1,0:T(8,128)(2,1)S(1)} %slice.18), channel_id=1, source_target_pairs={{0,16},{8,24},{16,0},{24,8},{1,17},{9,25},{17,1},{25,9},{2,18},{10... | collective-permute-start | bytes 1179656 | tf_op jit(solution)/shard_map/ppermute | solution.py:30
  46.1 22.5 %collective-permute-start.20 = (bf16[96,2048]{1,0:T(8,128)(2,1)S(1)}, bf16[96,2048]{1,0:T(8,128)(2,1)S(1)}, u32[]{:S(2)}, u32[]{:S(2)}) collective-permute-start(bf16[96,2048]{1,0:T(8,128)(2,1)S(1)} %slice.18), channel_id=1, source_target_pairs={{0,24},{8,0},{16,8},{24,16},{1,25},{9,1},{17,9},{25,17},{2,26},{10... | collective-permute-start | bytes 1179656 | tf_op jit(solution)/shard_map/ppermute | solution.py:30
  47.4 21.3 %copy-start.10 = (bf16[4,24,3072]{2,1,0:T(8,128)(2,1)}, bf16[4,24,3072]{2,1,0:T(8,128)(2,1)S(1)}, u32[]{:S(2)}) copy-start(bf16[4,24,3072]{2,1,0:T(8,128)(2,1)S(1)} %pad_maximum_fusion.3) | copy-start | bytes 1769476
  47.4 21.4 %collective-permute-start.25 = (bf16[96,2048]{1,0:T(8,128)(2,1)S(1)}, bf16[96,2048]{1,0:T(8,128)(2,1)S(1)}, u32[]{:S(2)}, u32[]{:S(2)}) collective-permute-start(bf16[96,2048]{1,0:T(8,128)(2,1)S(1)} %slice.19), channel_id=1, source_target_pairs={{0,2},{2,4},{4,6},{6,0},{1,3},{3,5},{5,7},{7,1},{8,10},{10,12},{12... | collective-permute-start | bytes 1179656 | tf_op jit(solution)/shard_map/ppermute | solution.py:30
  64.5 9.3 %collective-permute-start.24 = (bf16[96,2048]{1,0:T(8,128)(2,1)S(1)}, bf16[96,2048]{1,0:T(8,128)(2,1)S(1)}, u32[]{:S(2)}, u32[]{:S(2)}) collective-permute-start(bf16[96,2048]{1,0:T(8,128)(2,1)S(1)} %slice.19), channel_id=1, source_target_pairs={{0,4},{2,6},{4,0},{6,2},{1,5},{3,7},{5,1},{7,3},{8,12},{10,14},{12... | collective-permute-start | bytes 1179656 | tf_op jit(solution)/shard_map/ppermute | solution.py:30
  67.5 11.7 %collective-permute-start.23 = (bf16[96,2048]{1,0:T(8,128)(2,1)S(1)}, bf16[96,2048]{1,0:T(8,128)(2,1)S(1)}, u32[]{:S(2)}, u32[]{:S(2)}) collective-permute-start(bf16[96,2048]{1,0:T(8,128)(2,1)S(1)} %slice.19), channel_id=1, source_target_pairs={{0,6},{2,0},{4,2},{6,4},{1,7},{3,1},{5,3},{7,5},{8,14},{10,8},{12,... | collective-permute-start | bytes 1179656 | tf_op jit(solution)/shard_map/ppermute | solution.py:30
  84.0 0.7 copy-start.7
  84.8 2.8 %collective-permute-start.32 = (bf16[288,2048]{1,0:T(8,128)(2,1)S(1)}, bf16[288,2048]{1,0:T(8,128)(2,1)S(1)}, u32[]{:S(2)}, u32[]{:S(2)}) collective-permute-start(bf16[288,2048]{1,0:T(8,128)(2,1)S(1)} %get-tuple-element.64), channel_id=1, source_target_pairs={{0,1},{1,0},{2,3},{3,2},{4,5},{5,4},{6,7},{7,6},{8,9},{9,8},{10,11... | collective-permute-start | bytes 3538952 | tf_op jit(solution)/shard_map/ppermute | solution.py:25
  89.2 88.2 %all-to-all-start.1 = ((bf16[32,144,128]{2,1,0:T(8,128)(2,1)}), bf16[32,144,128]{2,1,0:T(8,128)(2,1)S(1)}, u32[]{:S(2)}, u32[]{:S(2)}) async-start(bf16[32,144,128]{2,1,0:T(8,128)(2,1)} %shard_map.144), calls=%async_computation.1 | async-start | bytes 2359296 | tf_op jit(solution)/shard_map/all_to_all | solution.py:21
  101.8 12.1 %collective-permute-start.4 = (bf16[96,1024]{1,0:T(8,128)(2,1)S(1)}, bf16[96,1024]{1,0:T(8,128)(2,1)S(1)}, u32[]{:S(2)}, u32[]{:S(2)}) collective-permute-start(bf16[96,1024]{1,0:T(8,128)(2,1)S(1)} %slice.16.refs_0_), channel_id=1, source_target_pairs={{0,24},{8,0},{16,8},{24,16},{1,25},{9,1},{17,9},{25,17},{2,26},{10... | collective-permute-start | bytes 589832 | tf_op jit(solution)/shard_map/ppermute | solution.py:30
  104.6 14.4 %collective-permute-start.5 = (bf16[96,1024]{1,0:T(8,128)(2,1)S(1)}, bf16[96,1024]{1,0:T(8,128)(2,1)S(1)}, u32[]{:S(2)}, u32[]{:S(2)}) collective-permute-start(bf16[96,1024]{1,0:T(8,128)(2,1)S(1)} %slice.16.refs_0_), channel_id=1, source_target_pairs={{0,16},{8,24},{16,0},{24,8},{1,17},{9,25},{17,1},{25,9},{2,18},{10... | collective-permute-start | bytes 589832 | tf_op jit(solution)/shard_map/ppermute | solution.py:30
  105.4 18.1 %collective-permute-start.6 = (bf16[96,1024]{1,0:T(8,128)(2,1)S(1)}, bf16[96,1024]{1,0:T(8,128)(2,1)S(1)}, u32[]{:S(2)}, u32[]{:S(2)}) collective-permute-start(bf16[96,1024]{1,0:T(8,128)(2,1)S(1)} %slice.16.refs_0_), channel_id=1, source_target_pairs={{0,8},{8,16},{16,24},{24,0},{1,9},{9,17},{17,25},{25,1},{2,10},{10... | collective-permute-start | bytes 589832 | tf_op jit(solution)/shard_map/ppermute | solution.py:30
  107.2 16.4 %collective-permute-start.10 = (bf16[96,1024]{1,0:T(8,128)(2,1)S(1)}, bf16[96,1024]{1,0:T(8,128)(2,1)S(1)}, u32[]{:S(2)}, u32[]{:S(2)}) collective-permute-start(bf16[96,1024]{1,0:T(8,128)(2,1)S(1)} %slice.17.refs_4_), channel_id=1, source_target_pairs={{0,6},{2,0},{4,2},{6,4},{1,7},{3,1},{5,3},{7,5},{8,14},{10,8},{12,... | collective-permute-start | bytes 589832 | tf_op jit(solution)/shard_map/ppermute | solution.py:30
  110.0 13.6 %collective-permute-start.11 = (bf16[96,1024]{1,0:T(8,128)(2,1)S(1)}, bf16[96,1024]{1,0:T(8,128)(2,1)S(1)}, u32[]{:S(2)}, u32[]{:S(2)}) collective-permute-start(bf16[96,1024]{1,0:T(8,128)(2,1)S(1)} %slice.17.refs_4_), channel_id=1, source_target_pairs={{0,4},{2,6},{4,0},{6,2},{1,5},{3,7},{5,1},{7,3},{8,12},{10,14},{12... | collective-permute-start | bytes 589832 | tf_op jit(solution)/shard_map/ppermute | solution.py:30
  113.9 9.7 %collective-permute-start.12 = (bf16[96,1024]{1,0:T(8,128)(2,1)S(1)}, bf16[96,1024]{1,0:T(8,128)(2,1)S(1)}, u32[]{:S(2)}, u32[]{:S(2)}) collective-permute-start(bf16[96,1024]{1,0:T(8,128)(2,1)S(1)} %slice.17.refs_4_), channel_id=1, source_target_pairs={{0,2},{2,4},{4,6},{6,0},{1,3},{3,5},{5,7},{7,1},{8,10},{10,12},{12... | collective-permute-start | bytes 589832 | tf_op jit(solution)/shard_map/ppermute | solution.py:30
  115.3 1.0 copy-start.8
  118.3 0.7 copy-start
  119.0 24.4 %collective-permute-start.26 = (bf16[96,2048]{1,0:T(8,128)(2,1)S(1)}, bf16[96,2048]{1,0:T(8,128)(2,1)S(1)}, u32[]{:S(2)}, u32[]{:S(2)}) collective-permute-start(bf16[96,2048]{1,0:T(8,128)(2,1)S(1)} %get-tuple-element.56), channel_id=1, source_target_pairs={{0,2},{2,4},{4,6},{6,0},{1,3},{3,5},{5,7},{7,1},{8,10},{10,12},{12... | collective-permute-start | bytes 1179656 | tf_op jit(solution)/shard_map/ppermute | solution.py:30
  126.9 1.4 collective-permute-start.13
  129.8 34.1 %collective-permute-start.14 = (bf16[96,2304]{1,0:T(8,128)(2,1)}, bf16[96,2304]{1,0:T(8,128)(2,1)S(1)}, u32[]{:S(2)}, u32[]{:S(2)}) collective-permute-start(bf16[96,2304]{1,0:T(8,128)(2,1)} %get-tuple-element.46), channel_id=1, source_target_pairs={{0,8},{8,16},{16,24},{24,0},{1,9},{9,17},{17,25},{25,1},{2,10},{10... | collective-permute-start | bytes 1327112 | tf_op jit(solution)/shard_map/ppermute | solution.py:30
  130.6 13.5 %collective-permute-start.27 = (bf16[96,2048]{1,0:T(8,128)(2,1)}, bf16[96,2048]{1,0:T(8,128)(2,1)S(1)}, u32[]{:S(2)}, u32[]{:S(2)}) collective-permute-start(bf16[96,2048]{1,0:T(8,128)(2,1)} %get-tuple-element.57), channel_id=1, source_target_pairs={{0,4},{2,6},{4,0},{6,2},{1,5},{3,7},{5,1},{7,3},{8,12},{10,14},{12... | collective-permute-start | bytes 1179656 | tf_op jit(solution)/shard_map/ppermute | solution.py:30
  133.4 17.9 %collective-permute-start.28 = (bf16[96,2048]{1,0:T(8,128)(2,1)}, bf16[96,2048]{1,0:T(8,128)(2,1)}, u32[]{:S(2)}, u32[]{:S(2)}) collective-permute-start(bf16[96,2048]{1,0:T(8,128)(2,1)} %get-tuple-element.58), channel_id=1, source_target_pairs={{0,6},{2,0},{4,2},{6,4},{1,7},{3,1},{5,3},{7,5},{8,14},{10,8},{12,... | collective-permute-start | bytes 1179656 | tf_op jit(solution)/shard_map/ppermute | solution.py:30
  133.9 31.4 %collective-permute-start.15 = (bf16[96,2304]{1,0:T(8,128)(2,1)}, bf16[96,2304]{1,0:T(8,128)(2,1)S(1)}, u32[]{:S(2)}, u32[]{:S(2)}) collective-permute-start(bf16[96,2304]{1,0:T(8,128)(2,1)} %get-tuple-element.47), channel_id=1, source_target_pairs={{0,16},{8,24},{16,0},{24,8},{1,17},{9,25},{17,1},{25,9},{2,18},{10... | collective-permute-start | bytes 1327112 | tf_op jit(solution)/shard_map/ppermute | solution.py:30
  143.4 0.7 copy-start.2
  144.1 21.2 %collective-permute-start.16 = (bf16[96,2304]{1,0:T(8,128)(2,1)}, bf16[96,2304]{1,0:T(8,128)(2,1)S(1)}, u32[]{:S(2)}, u32[]{:S(2)}) collective-permute-start(bf16[96,2304]{1,0:T(8,128)(2,1)} %get-tuple-element.48), channel_id=1, source_target_pairs={{0,24},{8,0},{16,8},{24,16},{1,25},{9,1},{17,9},{25,17},{2,26},{10... | collective-permute-start | bytes 1327112 | tf_op jit(solution)/shard_map/ppermute | solution.py:30
  151.3 1.0 copy-start.1
  152.3 1.0 copy-start.3
  154.5 22.9 %copy-start.4 = (f32[64,352]{1,0:T(8,128)S(1)}, f32[64,352]{1,0:T(8,128)}, u32[]{:S(2)}) copy-start(f32[64,352]{1,0:T(8,128)} %gate.1) | copy-start | bytes 270340
  154.5 22.9 %copy-start.5 = (f32[64,352]{1,0:T(8,128)S(1)}, f32[64,352]{1,0:T(8,128)}, u32[]{:S(2)}) copy-start(f32[64,352]{1,0:T(8,128)} %up.1) | copy-start | bytes 270340
  154.5 22.9 %copy-start.6 = (f32[352,64]{0,1:T(8,128)S(1)}, f32[352,64]{0,1:T(8,128)}, u32[]{:S(2)}) copy-start(f32[352,64]{0,1:T(8,128)} %param.17) | copy-start | bytes 270340
  154.5 15.8 %collective-permute-start.31 = (bf16[24,2048]{1,0:T(8,128)(2,1)S(1)}, bf16[24,2048]{1,0:T(8,128)(2,1)S(1)}, u32[]{:S(2)}, u32[]{:S(2)}) collective-permute-start(bf16[24,2048]{1,0:T(8,128)(2,1)S(1)} %get-tuple-element.62), channel_id=1, source_target_pairs={{0,24},{8,0},{16,8},{24,16},{1,25},{9,1},{17,9},{25,17},{2,26},{10... | collective-permute-start | bytes 294920 | tf_op jit(solution)/shard_map/ppermute | solution.py:30
  162.6 7.7 %collective-permute-start.30 = (bf16[24,2048]{1,0:T(8,128)(2,1)S(1)}, bf16[24,2048]{1,0:T(8,128)(2,1)S(1)}, u32[]{:S(2)}, u32[]{:S(2)}) collective-permute-start(bf16[24,2048]{1,0:T(8,128)(2,1)S(1)} %get-tuple-element.61), channel_id=1, source_target_pairs={{0,16},{8,24},{16,0},{24,8},{1,17},{9,25},{17,1},{25,9},{2,18},{10... | collective-permute-start | bytes 294920 | tf_op jit(solution)/shard_map/ppermute | solution.py:30
  163.9 6.4 %collective-permute-start.29 = (bf16[24,2048]{1,0:T(8,128)(2,1)S(1)}, bf16[24,2048]{1,0:T(8,128)(2,1)S(1)}, u32[]{:S(2)}, u32[]{:S(2)}) collective-permute-start(bf16[24,2048]{1,0:T(8,128)(2,1)S(1)} %get-tuple-element.60), channel_id=1, source_target_pairs={{0,8},{8,16},{16,24},{24,0},{1,9},{9,17},{17,25},{25,1},{2,10},{10... | collective-permute-start | bytes 294920 | tf_op jit(solution)/shard_map/ppermute | solution.py:30
  166.8 6.2 %collective-permute-start.19 = (bf16[24,2048]{1,0:T(8,128)(2,1)S(1)}, bf16[24,2048]{1,0:T(8,128)(2,1)S(1)}, u32[]{:S(2)}, u32[]{:S(2)}) collective-permute-start(bf16[24,2048]{1,0:T(8,128)(2,1)S(1)} %get-tuple-element.52), channel_id=1, source_target_pairs={{0,6},{2,0},{4,2},{6,4},{1,7},{3,1},{5,3},{7,5},{8,14},{10,8},{12,... | collective-permute-start | bytes 294920 | tf_op jit(solution)/shard_map/ppermute | solution.py:30
  169.5 6.2 %collective-permute-start.18 = (bf16[24,2048]{1,0:T(8,128)(2,1)S(1)}, bf16[24,2048]{1,0:T(8,128)(2,1)S(1)}, u32[]{:S(2)}, u32[]{:S(2)}) collective-permute-start(bf16[24,2048]{1,0:T(8,128)(2,1)S(1)} %get-tuple-element.51), channel_id=1, source_target_pairs={{0,4},{2,6},{4,0},{6,2},{1,5},{3,7},{5,1},{7,3},{8,12},{10,14},{12... | collective-permute-start | bytes 294920 | tf_op jit(solution)/shard_map/ppermute | solution.py:30
  170.3 6.4 %collective-permute-start.17 = (bf16[24,2048]{1,0:T(8,128)(2,1)S(1)}, bf16[24,2048]{1,0:T(8,128)(2,1)S(1)}, u32[]{:S(2)}, u32[]{:S(2)}) collective-permute-start(bf16[24,2048]{1,0:T(8,128)(2,1)S(1)} %get-tuple-element.50), channel_id=1, source_target_pairs={{0,2},{2,4},{4,6},{6,0},{1,3},{3,5},{5,7},{7,1},{8,10},{10,12},{12... | collective-permute-start | bytes 294920 | tf_op jit(solution)/shard_map/ppermute | solution.py:30

commit v4 on v3

--- a/solution.py
+++ b/solution.py
@@ -67,10 +67,10 @@
     )(*inputs)
 
 
-def fetched(sources, target, sems, first=0):
+def fetched(sources, target, sems):
     rows = target.shape[0] // len(sources)
     copies = [
-        pltpu.make_async_copy(source, target.at[pl.ds(k * rows, rows)], sems.at[first + k])
+        pltpu.make_async_copy(source, target.at[pl.ds(k * rows, rows)], sems.at[k])
         for k, source in enumerate(sources)
     ]
     for copy in copies:
@@ -91,20 +91,17 @@
 
 
 def front_kernel(copies, part, pad, *refs):
-    sources, (first, second, out), refs = refs[:6], refs[6:9], refs[9:]
-    targets, sems = refs[:6], refs[6]
+    sources, (second, out), refs = refs[:5], refs[5:7], refs[7:]
+    targets, sems = refs[:5], refs[5]
     moves = [pltpu.make_async_copy(*pair, sems.at[k]) for k, pair in enumerate(zip(sources, targets))]
     for move in moves:
         move.start()
     for move in moves:
         move.wait()
-    x_next, x_prev, grad_out, gate, up, down_t = targets
-    width = x_prev.shape[1]
-    mid = width // 2
-    first[:, :width] = x_prev[...]
-    first[:, width:] = x_next[:, :mid]
+    x_next, grad_out, gate, up, down_t = targets
+    width = grad_out.shape[1]
     second[:, :width] = grad_out[...]
-    second[:, width:] = x_next[:, mid:]
+    second[:, width:] = x_next[...]
     shard, units = gate.shape
     both = jnp.concatenate((gate[...], up[...]), axis=0).astype(F32).T
     tall = jnp.concatenate((down_t[...], jnp.zeros_like(down_t))).astype(F32).T[:, :shard]
@@ -208,14 +205,10 @@
 
 
 def hidden_kernel(ny, nx, rows, pad, gate_up, *refs):
-    firsts, seconds = refs[:ny], refs[ny : ny + nx]
-    mine, theirs, hidden, left, right, sems = refs[ny + nx :]
-    half = left.shape[1]
-    moves = fetched(firsts, left, sems) + fetched(seconds, right, sems, ny)
-    for move in moves:
+    pieces, (mine, theirs, hidden, tokens, sems) = refs[:nx], refs[nx:]
+    for move in fetched(pieces, tokens, sems):
         move.wait()
-    pre = dot(left[...], gate_up[:, :half], ((1,), (1,)))
-    pre = pre + turned(dot(right[...], gate_up[:, half:], ((1,), (1,))), nx, ny, rows)
+    pre = turned(dot(tokens[...], gate_up[...], ((1,), (1,))), nx, ny, rows)
     value = jax.nn.silu(pre[:, : 2 * pad]) * pre[:, 2 * pad :]
     blank = jnp.zeros((value.shape[0], LANES - pad), F32)
     mine[...] = jnp.concatenate((value[:, :pad], blank), axis=1).astype(BF16)
@@ -267,33 +260,30 @@
     part = units // ny
     pad = -(-part // 32) * 32
     block = (nz * ny, pad + pad // 2, LANES)
-    mid = width // 2
     token_ops = 2 * group * 2 * pad * width
 
-    first, second, packed = whole(
+    second, packed = whole(
         functools.partial(front_kernel, nz, part, pad),
-        (like((rows, width + mid), BF16), like((rows, width + mid), BF16), like(block, BF16)),
-        (x_next, x_prev, grad_out, gate_w, up_w, down_w.T),
+        (like((rows, 2 * width), BF16), like(block, BF16)),
+        (x_next, grad_out, gate_w, up_w, down_w.T),
         (
-            *(pltpu.VMEM((rows, width), BF16) for _ in range(3)),
+            *(pltpu.VMEM((rows, width), BF16) for _ in range(2)),
             *(pltpu.VMEM((width // (nz * ny), units), BF16) for _ in range(3)),
-            pltpu.SemaphoreType.DMA((6,)),
+            pltpu.SemaphoreType.DMA((5,)),
         ),
         grant=60,
-        spaces=[pltpu.HBM] * 6,
+        spaces=[pltpu.HBM] * 5,
         result=None,
     )
 
     own = spread(packed, FS)
     other = swapped(own)
 
-    first = jnp.stack(around(first, "x")).reshape(nx * rows, width + mid)
-    second = jnp.stack(around(second, "y")).reshape(ny * rows, width + mid)
-    prevs = around(first[:, :width], "y")
+    first = jnp.stack(around(x_prev, "x")).reshape(nx * rows, width)
+    second = jnp.stack(around(second, "y")).reshape(ny * rows, 2 * width)
+    prevs = around(first, "y")
     cotangents = around(second[:, :width], "x")
-    nexts = around(first[:, width:], "y")
-    nexts = nexts + around(second[:, width:], "x")
-
+    nexts = around(second[:, width:], "x")
     gate_up, down = whole(
         functools.partial(unpack_kernel, pad),
         (like((4 * pad, width), BF16), like((2 * pad, width), BF16)),
@@ -335,13 +325,9 @@
         functools.partial(hidden_kernel, ny, nx, rows, pad),
         (like((group, LANES), BF16), like((group, LANES), BF16), like((group, 2 * pad), BF16)),
         (gate_up, *nexts),
-        (
-            pltpu.VMEM((group, mid), BF16),
-            pltpu.VMEM((group, mid), BF16),
-            pltpu.SemaphoreType.DMA((ny + nx,)),
-        ),
+        (pltpu.VMEM((group, width), BF16), pltpu.SemaphoreType.DMA((nx,))),
         flops=2 * token_ops,
-        spaces=[pltpu.VMEM] + [pltpu.HBM] * (ny + nx),
+        spaces=[pltpu.VMEM] + [pltpu.HBM] * nx,
     )
     partner = swapped(theirs)
     out_parts = whole(

time: 179 us -> 159 us (0.89)
  the two profiles are of different devices: /device:TPU:96 before, /device:TPU:64 now
where the time goes in v4:
time: 159 us; the launch traced here: 158 us
  starting transfers between devices  67.2 us (42%)
  waiting for transfers between devices  65.5 us (41%)
  Pallas kernels  17.8 us (11%)
  local copies, waits for them, and re-layouts  3.54 us (2%)
  other arithmetic  3.01 us (2%)
    ppermute x27, waiting for transfers between devices, moved(): lax.ppermute(array, axis, [(i, (i + step) % length) for i in range(length)])  58.1 us
    ppermute x27, starting transfers between devices, moved(): lax.ppermute(array, axis, [(i, (i + step) % length) for i in range(length)])  48.3 us
    all_to_all x2, starting transfers between devices, spread(): return lax.all_to_all(blocks, axis, 0, 0, tiled=True)  18.8 us
    pallas_call x10, Pallas kernels, whole(): pl.pallas_call(kernel, out_shape=out_shape, in_specs=[pl.BlockSpec(memory...  17.8 us
    ppermute x3, waiting for transfers between devices, swapped(): return lax.ppermute(array, 'c', [(0, 1), (1, 0)])  4.14 us
    unnamed x22, local copies, waits for them, and re-layouts  3.47 us
    all_to_all x2, waiting for transfers between devices, spread(): return lax.all_to_all(blocks, axis, 0, 0, tiled=True)  3.3 us
  transfers between devices with their start and end apart: 32, of which 16 were waited for; matrix products, arithmetic and copies ran while one was open for 2% of the time, Pallas kernels for 5%

profile of v4, /device:TPU:64, one launch (start us, length us, event | category | flops | bytes accessed | tf_op | source)
XLA Modules:
  0.0 158.0 jit_solution(14979617083600162907)
XLA Ops:
  0.6 2.3 %shard_map.136 = (bf16[24,4096]{1,0:T(8,128)(2,1)}, bf16[32,144,128]{2,1,0:T(8,128)(2,1)}) custom-call(bf16[24,2048]{1,0:T(8,128)(2,1)} %refs_0_.1, bf16[24,2048]{1,0:T(8,128)(2,1)} %refs_1_.1, bf16[64,352]{1,0:T(8,128)(2,1)} %refs_2_.1, bf16[64,352]{1,0:T(8,128)(2,1)} %refs_3_.1, bf16[64,352]{1,0:T(8,128)(2,1)} %bitcast.30), custom_call_target="tpu_custom_call" | custom-call | tf_op jit(solution)/shard_map/pallas_call | solution.py:59
  3.0 11.1 %all-to-all-start = ((bf16[32,144,128]{2,1,0:T(8,128)(2,1)}), bf16[32,144,128]{2,1,0:T(8,128)(2,1)S(1)}, u32[]{:S(2)}, u32[]{:S(2)}) async-start(bf16[32,144,128]{2,1,0:T(8,128)(2,1)} %get-tuple-element.36), calls=%async_computation | async-start | bytes 2359296 | tf_op jit(solution)/shard_map/all_to_all | solution.py:21
  14.1 1.6 collective-permute-start.16
  15.6 2.7 %collective-permute-start.15 = (bf16[24,2048]{1,0:T(8,128)(2,1)S(1)}, bf16[24,2048]{1,0:T(8,128)(2,1)S(1)}, u32[]{:S(2)}, u32[]{:S(2)}) collective-permute-start(bf16[24,2048]{1,0:T(8,128)(2,1)S(1)} %copy-done.10), channel_id=1, source_target_pairs={{0,4},{2,6},{4,0},{6,2},{1,5},{3,7},{5,1},{7,3},{8,12},{10,14},{12... | collective-permute-start | bytes 294920 | tf_op jit(solution)/shard_map/ppermute | solution.py:30
  18.4 1.4 collective-permute-start.14
  19.8 1.5 collective-permute-start.3
  21.3 2.7 %collective-permute-start.2 = (bf16[24,4096]{1,0:T(8,128)(2,1)S(1)}, bf16[24,4096]{1,0:T(8,128)(2,1)S(1)}, u32[]{:S(2)}, u32[]{:S(2)}) collective-permute-start(bf16[24,4096]{1,0:T(8,128)(2,1)S(1)} %copy-done.9), channel_id=1, source_target_pairs={{0,16},{8,24},{16,0},{24,8},{1,17},{9,25},{17,1},{25,9},{2,18},{10... | collective-permute-start | bytes 589832 | tf_op jit(solution)/shard_map/ppermute | solution.py:30
  23.9 1.5 collective-permute-start.1
  26.1 1.1 collective-permute-start.18
  27.3 9.6 %collective-permute-done.3 = bf16[24,4096]{1,0:T(8,128)(2,1)S(1)} collective-permute-done((bf16[24,4096]{1,0:T(8,128)(2,1)S(1)}, bf16[24,4096]{1,0:T(8,128)(2,1)S(1)}, u32[]{:S(2)}, u32[]{:S(2)}) %collective-permute-start.3) | collective-permute-done | bytes 196640 | tf_op jit(solution)/shard_map/ppermute | solution.py:30
  36.9 4.7 %collective-permute-done.2 = bf16[24,4096]{1,0:T(8,128)(2,1)S(1)} collective-permute-done((bf16[24,4096]{1,0:T(8,128)(2,1)S(1)}, bf16[24,4096]{1,0:T(8,128)(2,1)S(1)}, u32[]{:S(2)}, u32[]{:S(2)}) %collective-permute-start.2) | collective-permute-done | bytes 196640 | tf_op jit(solution)/shard_map/ppermute | solution.py:30
  41.6 3.3 %all-to-all-done.own = bf16[32,144,128]{2,1,0:T(8,128)(2,1)S(1)} async-done(((bf16[32,144,128]{2,1,0:T(8,128)(2,1)}), bf16[32,144,128]{2,1,0:T(8,128)(2,1)S(1)}, u32[]{:S(2)}, u32[]{:S(2)}) %all-to-all-start) | async-done | bytes 1179680 | tf_op jit(solution)/shard_map/all_to_all | solution.py:21
  45.1 1.6 collective-permute-start.22
  46.6 3.8 %collective-permute-done.19 = bf16[96,2048]{1,0:T(8,128)(2,1)S(1)} collective-permute-done((bf16[96,2048]{1,0:T(8,128)(2,1)S(1)}, bf16[96,2048]{1,0:T(8,128)(2,1)S(1)}, u32[]{:S(2)}, u32[]{:S(2)}) %collective-permute-start.19) | collective-permute-done | bytes 393248 | tf_op jit(solution)/shard_map/ppermute | solution.py:30
  50.4 8.4 %collective-permute-start.21 = (bf16[96,2048]{1,0:T(8,128)(2,1)S(1)}, bf16[96,2048]{1,0:T(8,128)(2,1)S(1)}, u32[]{:S(2)}, u32[]{:S(2)}) collective-permute-start(bf16[96,2048]{1,0:T(8,128)(2,1)S(1)} %get-tuple-element.66), channel_id=1, source_target_pairs={{0,4},{2,6},{4,0},{6,2},{1,5},{3,7},{5,1},{7,3},{8,12},{10,14},{12... | collective-permute-start | bytes 1179656 | tf_op jit(solution)/shard_map/ppermute | solution.py:30
  58.9 2.1 %collective-permute-start.20 = (bf16[96,2048]{1,0:T(8,128)(2,1)S(1)}, bf16[96,2048]{1,0:T(8,128)(2,1)S(1)}, u32[]{:S(2)}, u32[]{:S(2)}) collective-permute-start(bf16[96,2048]{1,0:T(8,128)(2,1)S(1)} %get-tuple-element.66), channel_id=1, source_target_pairs={{0,6},{2,0},{4,2},{6,4},{1,7},{3,1},{5,3},{7,5},{8,14},{10,8},{12,... | collective-permute-start | bytes 1179656 | tf_op jit(solution)/shard_map/ppermute | solution.py:30
  61.0 1.2 pad_maximum_fusion.prev
  62.3 5.0 %collective-permute-done.21 = bf16[96,2048]{1,0:T(8,128)(2,1)S(1)} collective-permute-done((bf16[96,2048]{1,0:T(8,128)(2,1)S(1)}, bf16[96,2048]{1,0:T(8,128)(2,1)S(1)}, u32[]{:S(2)}, u32[]{:S(2)}) %collective-permute-start.21) | collective-permute-done | bytes 393248 | tf_op jit(solution)/shard_map/ppermute | solution.py:30
  67.3 3.3 %collective-permute-done.20 = bf16[96,2048]{1,0:T(8,128)(2,1)S(1)} collective-permute-done((bf16[96,2048]{1,0:T(8,128)(2,1)S(1)}, bf16[96,2048]{1,0:T(8,128)(2,1)S(1)}, u32[]{:S(2)}, u32[]{:S(2)}) %collective-permute-start.20) | collective-permute-done | bytes 393248 | tf_op jit(solution)/shard_map/ppermute | solution.py:30
  70.8 1.0 shard_map.137
  71.8 3.6 %shard_map.141 = (f32[288,2048]{1,0:T(8,128)S(1)}, bf16[288,2048]{1,0:T(8,128)(2,1)S(1)}, bf16[384,384]{1,0:T(8,128)(2,1)S(1)}) custom-call(bf16[384,2048]{1,0:T(8,128)(2,1)S(1)} %get-tuple-element.37.gate_up, bf16[192,2048]{1,0:T(8,128)(2,1)S(1)} %get-tuple-element.40.down, bf16[384,2048]{1,0:T(8,128)(2,1)S(1)} %pad_maximum_fusion.prev, ...), custom_call_target="tpu_custom_call" | custom-call | flops 1811939328 | tf_op jit(solution)/shard_map/pallas_call | solution.py:59
  76.2 2.8 %collective-permute-done.29.received = bf16[288,2048]{1,0:T(8,128)(2,1)S(1)} collective-permute-done((bf16[288,2048]{1,0:T(8,128)(2,1)S(1)}, bf16[288,2048]{1,0:T(8,128)(2,1)S(1)}, u32[]{:S(2)}, u32[]{:S(2)}) %collective-permute-start.29) | collective-permute-done | bytes 1179680 | tf_op jit(solution)/shard_map/ppermute | solution.py:25
  79.0 1.6 %shard_map.144 = bf16[32,144,128]{2,1,0:T(8,128)(2,1)} custom-call(f32[288,2048]{1,0:T(8,128)S(1)} %get-tuple-element.61.kept, bf16[288,2048]{1,0:T(8,128)(2,1)S(1)} %collective-permute-done.29.received), custom_call_target="tpu_custom_call" | custom-call | tf_op jit(solution)/shard_map/pallas_call | solution.py:59
  80.6 7.7 %all-to-all-start.1 = ((bf16[32,144,128]{2,1,0:T(8,128)(2,1)}), bf16[32,144,128]{2,1,0:T(8,128)(2,1)S(1)}, u32[]{:S(2)}, u32[]{:S(2)}) async-start(bf16[32,144,128]{2,1,0:T(8,128)(2,1)} %shard_map.144), calls=%async_computation.1 | async-start | bytes 2359296 | tf_op jit(solution)/shard_map/all_to_all | solution.py:21
  88.4 2.7 %collective-permute-start.4 = (bf16[96,2048]{1,0:T(8,128)(2,1)S(1)}, bf16[96,2048]{1,0:T(8,128)(2,1)S(1)}, u32[]{:S(2)}, u32[]{:S(2)}) collective-permute-start(bf16[96,2048]{1,0:T(8,128)(2,1)S(1)} %get-tuple-element.67.refs_0_), channel_id=1, source_target_pairs={{0,6},{2,0},{4,2},{6,4},{1,7},{3,1},{5,3},{7,5},{8,14},{10,8},{12,... | collective-permute-start | bytes 1179656 | tf_op jit(solution)/shard_map/ppermute | solution.py:30
  93.0 2.1 %shard_map.142 = (bf16[96,2048]{1,0:T(8,128)(2,1)S(1)}, bf16[96,2048]{1,0:T(8,128)(2,1)S(1)}, bf16[96,2048]{1,0:T(8,128)(2,1)}, bf16[96,2048]{1,0:T(8,128)(2,1)}) custom-call(bf16[384,384]{1,0:T(8,128)(2,1)S(1)} %copy-done.8, bf16[384,2048]{1,0:T(8,128)(2,1)S(1)} %get-tuple-element.37.gate_up), custom_call_target="tpu_custom_call" | custom-call | flops 603979776 | tf_op jit(solution)/shard_map/pallas_call | solution.py:59
  95.0 2.5 %collective-permute-start.23 = (bf16[96,2048]{1,0:T(8,128)(2,1)S(1)}, bf16[96,2048]{1,0:T(8,128)(2,1)S(1)}, u32[]{:S(2)}, u32[]{:S(2)}) collective-permute-start(bf16[96,2048]{1,0:T(8,128)(2,1)S(1)} %get-tuple-element.54), channel_id=1, source_target_pairs={{0,2},{2,4},{4,6},{6,0},{1,3},{3,5},{5,7},{7,1},{8,10},{10,12},{12... | collective-permute-start | bytes 1179656 | tf_op jit(solution)/shard_map/ppermute | solution.py:30
  97.6 10.0 %collective-permute-done.4.refs_1_ = bf16[96,2048]{1,0:T(8,128)(2,1)S(1)} collective-permute-done((bf16[96,2048]{1,0:T(8,128)(2,1)S(1)}, bf16[96,2048]{1,0:T(8,128)(2,1)S(1)}, u32[]{:S(2)}, u32[]{:S(2)}) %collective-permute-start.4) | collective-permute-done | bytes 393248 | tf_op jit(solution)/shard_map/ppermute | solution.py:30
  107.6 3.8 %collective-permute-done.6.refs_3_ = bf16[96,2048]{1,0:T(8,128)(2,1)S(1)} collective-permute-done((bf16[96,2048]{1,0:T(8,128)(2,1)S(1)}, bf16[96,2048]{1,0:T(8,128)(2,1)S(1)}, u32[]{:S(2)}, u32[]{:S(2)}) %collective-permute-start.6) | collective-permute-done | bytes 393248 | tf_op jit(solution)/shard_map/ppermute | solution.py:30
  111.4 1.9 %shard_map.138 = (bf16[384,128]{1,0:T(8,128)(2,1)S(1)}, bf16[384,128]{1,0:T(8,128)(2,1)S(1)}, bf16[384,192]{1,0:T(8,128)(2,1)S(1)}) custom-call(bf16[384,2048]{1,0:T(8,128)(2,1)S(1)} %get-tuple-element.37.gate_up, bf16[96,2048]{1,0:T(8,128)(2,1)S(1)} %get-tuple-element.67.refs_0_, bf16[96,2048]{1,0:T(8,128)(2,1)S(1)} %collective-permute-done.4.refs_1_, ...), custom_call_target="tpu_custom_call" | custom-call | flops 603979776 | tf_op jit(solution)/shard_map/pallas_call | solution.py:59
  113.4 1.3 collective-permute-done.7.partner
  114.7 1.6 shard_map.139
  116.3 1.5 collective-permute-start.8
  117.7 1.2 collective-permute-start.24
  118.9 2.5 %collective-permute-start.25 = (bf16[96,2048]{1,0:T(8,128)(2,1)}, bf16[96,2048]{1,0:T(8,128)(2,1)}, u32[]{:S(2)}, u32[]{:S(2)}) collective-permute-start(bf16[96,2048]{1,0:T(8,128)(2,1)} %get-tuple-element.56), channel_id=1, source_target_pairs={{0,6},{2,0},{4,2},{6,4},{1,7},{3,1},{5,3},{7,5},{8,14},{10,8},{12,... | collective-permute-start | bytes 1179656 | tf_op jit(solution)/shard_map/ppermute | solution.py:30
  121.4 2.7 %collective-permute-start.9 = (bf16[96,2304]{1,0:T(8,128)(2,1)}, bf16[96,2304]{1,0:T(8,128)(2,1)S(1)}, u32[]{:S(2)}, u32[]{:S(2)}) collective-permute-start(bf16[96,2304]{1,0:T(8,128)(2,1)} %get-tuple-element.45), channel_id=1, source_target_pairs={{0,16},{8,24},{16,0},{24,8},{1,17},{9,25},{17,1},{25,9},{2,18},{10... | collective-permute-start | bytes 1327112 | tf_op jit(solution)/shard_map/ppermute | solution.py:30
  124.8 1.5 collective-permute-start.10
  126.3 4.2 %collective-permute-done.24.refs_2_ = bf16[96,2048]{1,0:T(8,128)(2,1)} collective-permute-done((bf16[96,2048]{1,0:T(8,128)(2,1)}, bf16[96,2048]{1,0:T(8,128)(2,1)}, u32[]{:S(2)}, u32[]{:S(2)}) %collective-permute-start.24) | collective-permute-done | bytes 393248 | tf_op jit(solution)/shard_map/ppermute | solution.py:30
  130.5 8.0 %collective-permute-done.25.refs_3_ = bf16[96,2048]{1,0:T(8,128)(2,1)} collective-permute-done((bf16[96,2048]{1,0:T(8,128)(2,1)}, bf16[96,2048]{1,0:T(8,128)(2,1)}, u32[]{:S(2)}, u32[]{:S(2)}) %collective-permute-start.25) | collective-permute-done | bytes 393248 | tf_op jit(solution)/shard_map/ppermute | solution.py:30
  138.4 1.0 copy-done.3
  139.4 1.3 shard_map.143
  140.8 1.8 %collective-permute-start.28 = (bf16[24,2048]{1,0:T(8,128)(2,1)S(1)}, bf16[24,2048]{1,0:T(8,128)(2,1)S(1)}, u32[]{:S(2)}, u32[]{:S(2)}) collective-permute-start(bf16[24,2048]{1,0:T(8,128)(2,1)S(1)} %get-tuple-element.60), channel_id=1, source_target_pairs={{0,24},{8,0},{16,8},{24,16},{1,25},{9,1},{17,9},{25,17},{2,26},{10... | collective-permute-start | bytes 294920 | tf_op jit(solution)/shard_map/ppermute | solution.py:30
  142.6 1.8 %collective-permute-start.27 = (bf16[24,2048]{1,0:T(8,128)(2,1)S(1)}, bf16[24,2048]{1,0:T(8,128)(2,1)S(1)}, u32[]{:S(2)}, u32[]{:S(2)}) collective-permute-start(bf16[24,2048]{1,0:T(8,128)(2,1)S(1)} %get-tuple-element.59), channel_id=1, source_target_pairs={{0,16},{8,24},{16,0},{24,8},{1,17},{9,25},{17,1},{25,9},{2,18},{10... | collective-permute-start | bytes 294920 | tf_op jit(solution)/shard_map/ppermute | solution.py:30
  145.0 1.5 shard_map.140
  146.6 2.6 %collective-permute-start.13 = (bf16[24,2048]{1,0:T(8,128)(2,1)S(1)}, bf16[24,2048]{1,0:T(8,128)(2,1)S(1)}, u32[]{:S(2)}, u32[]{:S(2)}) collective-permute-start(bf16[24,2048]{1,0:T(8,128)(2,1)S(1)} %get-tuple-element.50), channel_id=1, source_target_pairs={{0,6},{2,0},{4,2},{6,4},{1,7},{3,1},{5,3},{7,5},{8,14},{10,8},{12,... | collective-permute-start | bytes 294920 | tf_op jit(solution)/shard_map/ppermute | solution.py:30
  150.9 1.8 %collective-permute-done.13 = bf16[24,2048]{1,0:T(8,128)(2,1)S(1)} collective-permute-done((bf16[24,2048]{1,0:T(8,128)(2,1)S(1)}, bf16[24,2048]{1,0:T(8,128)(2,1)S(1)}, u32[]{:S(2)}, u32[]{:S(2)}) %collective-permute-start.13) | collective-permute-done | bytes 98336 | tf_op jit(solution)/shard_map/ppermute | solution.py:30
  152.7 2.6 %collective-permute-done.12 = bf16[24,2048]{1,0:T(8,128)(2,1)S(1)} collective-permute-done((bf16[24,2048]{1,0:T(8,128)(2,1)S(1)}, bf16[24,2048]{1,0:T(8,128)(2,1)S(1)}, u32[]{:S(2)}, u32[]{:S(2)}) %collective-permute-start.12) | collective-permute-done | bytes 98336 | tf_op jit(solution)/shard_map/ppermute | solution.py:30
  155.3 1.1 collective-permute-done.11
  (56 shorter events, 8.6 us)
Async XLA Ops:
  0.6 13.4 %copy-start.10 = (bf16[24,2048]{1,0:T(8,128)(2,1)S(1)}, bf16[24,2048]{1,0:T(8,128)(2,1)}, u32[]{:S(2)}) copy-start(bf16[24,2048]{1,0:T(8,128)(2,1)} %param.10) | copy-start | bytes 294916
  3.0 16.8 %copy-start.9 = (bf16[24,4096]{1,0:T(8,128)(2,1)S(1)}, bf16[24,4096]{1,0:T(8,128)(2,1)}, u32[]{:S(2)}) copy-start(bf16[24,4096]{1,0:T(8,128)(2,1)} %get-tuple-element.38) | copy-start | bytes 589828
  3.0 41.9 %all-to-all-start = ((bf16[32,144,128]{2,1,0:T(8,128)(2,1)}), bf16[32,144,128]{2,1,0:T(8,128)(2,1)S(1)}, u32[]{:S(2)}, u32[]{:S(2)}) async-start(bf16[32,144,128]{2,1,0:T(8,128)(2,1)} %get-tuple-element.36), calls=%async_computation | async-start | bytes 2359296 | tf_op jit(solution)/shard_map/all_to_all | solution.py:21
  14.1 9.9 %collective-permute-start.16 = (bf16[24,2048]{1,0:T(8,128)(2,1)S(1)}, bf16[24,2048]{1,0:T(8,128)(2,1)S(1)}, u32[]{:S(2)}, u32[]{:S(2)}) collective-permute-start(bf16[24,2048]{1,0:T(8,128)(2,1)S(1)} %copy-done.10), channel_id=1, source_target_pairs={{0,2},{2,4},{4,6},{6,0},{1,3},{3,5},{5,7},{7,1},{8,10},{10,12},{12... | collective-permute-start | bytes 294920 | tf_op jit(solution)/shard_map/ppermute | solution.py:30
  15.6 9.8 %collective-permute-start.15 = (bf16[24,2048]{1,0:T(8,128)(2,1)S(1)}, bf16[24,2048]{1,0:T(8,128)(2,1)S(1)}, u32[]{:S(2)}, u32[]{:S(2)}) collective-permute-start(bf16[24,2048]{1,0:T(8,128)(2,1)S(1)} %copy-done.10), channel_id=1, source_target_pairs={{0,4},{2,6},{4,0},{6,2},{1,5},{3,7},{5,1},{7,3},{8,12},{10,14},{12... | collective-permute-start | bytes 294920 | tf_op jit(solution)/shard_map/ppermute | solution.py:30
  18.4 7.0 %collective-permute-start.14 = (bf16[24,2048]{1,0:T(8,128)(2,1)S(1)}, bf16[24,2048]{1,0:T(8,128)(2,1)S(1)}, u32[]{:S(2)}, u32[]{:S(2)}) collective-permute-start(bf16[24,2048]{1,0:T(8,128)(2,1)S(1)} %copy-done.10), channel_id=1, source_target_pairs={{0,6},{2,0},{4,2},{6,4},{1,7},{3,1},{5,3},{7,5},{8,14},{10,8},{12,... | collective-permute-start | bytes 294920 | tf_op jit(solution)/shard_map/ppermute | solution.py:30
  19.8 17.1 %collective-permute-start.3 = (bf16[24,4096]{1,0:T(8,128)(2,1)S(1)}, bf16[24,4096]{1,0:T(8,128)(2,1)S(1)}, u32[]{:S(2)}, u32[]{:S(2)}) collective-permute-start(bf16[24,4096]{1,0:T(8,128)(2,1)S(1)} %copy-done.9), channel_id=1, source_target_pairs={{0,8},{8,16},{16,24},{24,0},{1,9},{9,17},{17,25},{25,1},{2,10},{10... | collective-permute-start | bytes 589832 | tf_op jit(solution)/shard_map/ppermute | solution.py:30
  21.3 20.3 %collective-permute-start.2 = (bf16[24,4096]{1,0:T(8,128)(2,1)S(1)}, bf16[24,4096]{1,0:T(8,128)(2,1)S(1)}, u32[]{:S(2)}, u32[]{:S(2)}) collective-permute-start(bf16[24,4096]{1,0:T(8,128)(2,1)S(1)} %copy-done.9), channel_id=1, source_target_pairs={{0,16},{8,24},{16,0},{24,8},{1,17},{9,25},{17,1},{25,9},{2,18},{10... | collective-permute-start | bytes 589832 | tf_op jit(solution)/shard_map/ppermute | solution.py:30
  23.9 20.9 %collective-permute-start.1 = (bf16[24,4096]{1,0:T(8,128)(2,1)S(1)}, bf16[24,4096]{1,0:T(8,128)(2,1)S(1)}, u32[]{:S(2)}, u32[]{:S(2)}) collective-permute-start(bf16[24,4096]{1,0:T(8,128)(2,1)S(1)} %copy-done.9), channel_id=1, source_target_pairs={{0,24},{8,0},{16,8},{24,16},{1,25},{9,1},{17,9},{25,17},{2,26},{10... | collective-permute-start | bytes 589832 | tf_op jit(solution)/shard_map/ppermute | solution.py:30
  25.5 25.0 %collective-permute-start.19 = (bf16[96,2048]{1,0:T(8,128)(2,1)S(1)}, bf16[96,2048]{1,0:T(8,128)(2,1)S(1)}, u32[]{:S(2)}, u32[]{:S(2)}) collective-permute-start(bf16[96,2048]{1,0:T(8,128)(2,1)S(1)} %bitcast.18), channel_id=1, source_target_pairs={{0,8},{8,16},{16,24},{24,0},{1,9},{9,17},{17,25},{25,1},{2,10},{10... | collective-permute-start | bytes 1179656 | tf_op jit(solution)/shard_map/ppermute | solution.py:30
  26.1 32.8 %collective-permute-start.18 = (bf16[96,2048]{1,0:T(8,128)(2,1)S(1)}, bf16[96,2048]{1,0:T(8,128)(2,1)}, u32[]{:S(2)}, u32[]{:S(2)}) collective-permute-start(bf16[96,2048]{1,0:T(8,128)(2,1)S(1)} %bitcast.19), channel_id=1, source_target_pairs={{0,16},{8,24},{16,0},{24,8},{1,17},{9,25},{17,1},{25,9},{2,18},{10... | collective-permute-start | bytes 1179656 | tf_op jit(solution)/shard_map/ppermute | solution.py:30
  36.9 24.1 %collective-permute-start.17 = (bf16[96,2048]{1,0:T(8,128)(2,1)S(1)}, bf16[96,2048]{1,0:T(8,128)(2,1)}, u32[]{:S(2)}, u32[]{:S(2)}) collective-permute-start(bf16[96,2048]{1,0:T(8,128)(2,1)S(1)} %bitcast.20), channel_id=1, source_target_pairs={{0,24},{8,0},{16,8},{24,16},{1,25},{9,1},{17,9},{25,17},{2,26},{10... | collective-permute-start | bytes 1179656 | tf_op jit(solution)/shard_map/ppermute | solution.py:30
  44.9 25.9 %collective-permute-start = (bf16[32,144,128]{2,1,0:T(8,128)(2,1)S(1)}, bf16[32,144,128]{2,1,0:T(8,128)(2,1)S(1)}, u32[]{:S(2)}, u32[]{:S(2)}) collective-permute-start(bf16[32,144,128]{2,1,0:T(8,128)(2,1)S(1)} %all-to-all-done.own), channel_id=1, source_target_pairs={{0,1},{1,0},{2,3},{3,2},{4,5},{5,4},{6,7},{7,6},{8,9},{9,8},{10,11... | collective-permute-start | bytes 3538952 | tf_op jit(solution)/shard_map/ppermute | solution.py:25
  45.1 17.2 %collective-permute-start.22 = (bf16[96,2048]{1,0:T(8,128)(2,1)S(1)}, bf16[96,2048]{1,0:T(8,128)(2,1)S(1)}, u32[]{:S(2)}, u32[]{:S(2)}) collective-permute-start(bf16[96,2048]{1,0:T(8,128)(2,1)S(1)} %get-tuple-element.66), channel_id=1, source_target_pairs={{0,2},{2,4},{4,6},{6,0},{1,3},{3,5},{5,7},{7,1},{8,10},{10,12},{12... | collective-permute-start | bytes 1179656 | tf_op jit(solution)/shard_map/ppermute | solution.py:30
  50.4 16.9 %collective-permute-start.21 = (bf16[96,2048]{1,0:T(8,128)(2,1)S(1)}, bf16[96,2048]{1,0:T(8,128)(2,1)S(1)}, u32[]{:S(2)}, u32[]{:S(2)}) collective-permute-start(bf16[96,2048]{1,0:T(8,128)(2,1)S(1)} %get-tuple-element.66), channel_id=1, source_target_pairs={{0,4},{2,6},{4,0},{6,2},{1,5},{3,7},{5,1},{7,3},{8,12},{10,14},{12... | collective-permute-start | bytes 1179656 | tf_op jit(solution)/shard_map/ppermute | solution.py:30
  58.9 11.7 %collective-permute-start.20 = (bf16[96,2048]{1,0:T(8,128)(2,1)S(1)}, bf16[96,2048]{1,0:T(8,128)(2,1)S(1)}, u32[]{:S(2)}, u32[]{:S(2)}) collective-permute-start(bf16[96,2048]{1,0:T(8,128)(2,1)S(1)} %get-tuple-element.66), channel_id=1, source_target_pairs={{0,6},{2,0},{4,2},{6,4},{1,7},{3,1},{5,3},{7,5},{8,14},{10,8},{12,... | collective-permute-start | bytes 1179656 | tf_op jit(solution)/shard_map/ppermute | solution.py:30
  71.8 3.6 %copy-start = (bf16[192,2048]{1,0:T(8,128)(2,1)}, bf16[192,2048]{1,0:T(8,128)(2,1)S(1)}, u32[]{:S(2)}) copy-start(bf16[192,2048]{1,0:T(8,128)(2,1)S(1)} %get-tuple-element.40.down) | copy-start | bytes 2359300
  75.4 0.7 copy-start.7
  76.2 2.8 %collective-permute-start.29 = (bf16[288,2048]{1,0:T(8,128)(2,1)S(1)}, bf16[288,2048]{1,0:T(8,128)(2,1)S(1)}, u32[]{:S(2)}, u32[]{:S(2)}) collective-permute-start(bf16[288,2048]{1,0:T(8,128)(2,1)S(1)} %get-tuple-element.62), channel_id=1, source_target_pairs={{0,1},{1,0},{2,3},{3,2},{4,5},{5,4},{6,7},{7,6},{8,9},{9,8},{10,11... | collective-permute-start | bytes 3538952 | tf_op jit(solution)/shard_map/ppermute | solution.py:25
  80.6 76.5 %all-to-all-start.1 = ((bf16[32,144,128]{2,1,0:T(8,128)(2,1)}), bf16[32,144,128]{2,1,0:T(8,128)(2,1)S(1)}, u32[]{:S(2)}, u32[]{:S(2)}) async-start(bf16[32,144,128]{2,1,0:T(8,128)(2,1)} %shard_map.144), calls=%async_computation.1 | async-start | bytes 2359296 | tf_op jit(solution)/shard_map/all_to_all | solution.py:21
  88.4 19.3 %collective-permute-start.4 = (bf16[96,2048]{1,0:T(8,128)(2,1)S(1)}, bf16[96,2048]{1,0:T(8,128)(2,1)S(1)}, u32[]{:S(2)}, u32[]{:S(2)}) collective-permute-start(bf16[96,2048]{1,0:T(8,128)(2,1)S(1)} %get-tuple-element.67.refs_0_), channel_id=1, source_target_pairs={{0,6},{2,0},{4,2},{6,4},{1,7},{3,1},{5,3},{7,5},{8,14},{10,8},{12,... | collective-permute-start | bytes 1179656 | tf_op jit(solution)/shard_map/ppermute | solution.py:30
  91.0 16.6 %collective-permute-start.5 = (bf16[96,2048]{1,0:T(8,128)(2,1)S(1)}, bf16[96,2048]{1,0:T(8,128)(2,1)S(1)}, u32[]{:S(2)}, u32[]{:S(2)}) collective-permute-start(bf16[96,2048]{1,0:T(8,128)(2,1)S(1)} %get-tuple-element.67.refs_0_), channel_id=1, source_target_pairs={{0,4},{2,6},{4,0},{6,2},{1,5},{3,7},{5,1},{7,3},{8,12},{10,14},{12... | collective-permute-start | bytes 1179656 | tf_op jit(solution)/shard_map/ppermute | solution.py:30
  91.9 19.5 %collective-permute-start.6 = (bf16[96,2048]{1,0:T(8,128)(2,1)S(1)}, bf16[96,2048]{1,0:T(8,128)(2,1)S(1)}, u32[]{:S(2)}, u32[]{:S(2)}) collective-permute-start(bf16[96,2048]{1,0:T(8,128)(2,1)S(1)} %get-tuple-element.67.refs_0_), channel_id=1, source_target_pairs={{0,2},{2,4},{4,6},{6,0},{1,3},{3,5},{5,7},{7,1},{8,10},{10,12},{12... | collective-permute-start | bytes 1179656 | tf_op jit(solution)/shard_map/ppermute | solution.py:30
  92.0 1.0 copy-start.8
  95.0 19.7 %copy-start.1 = (bf16[192,2048]{1,0:T(8,128)(2,1)S(1)}, bf16[192,2048]{1,0:T(8,128)(2,1)}, u32[]{:S(2)}) copy-start(bf16[192,2048]{1,0:T(8,128)(2,1)} %copy-done) | copy-start | bytes 2359300
  95.0 29.0 %collective-permute-start.23 = (bf16[96,2048]{1,0:T(8,128)(2,1)S(1)}, bf16[96,2048]{1,0:T(8,128)(2,1)S(1)}, u32[]{:S(2)}, u32[]{:S(2)}) collective-permute-start(bf16[96,2048]{1,0:T(8,128)(2,1)S(1)} %get-tuple-element.54), channel_id=1, source_target_pairs={{0,2},{2,4},{4,6},{6,0},{1,3},{3,5},{5,7},{7,1},{8,10},{10,12},{12... | collective-permute-start | bytes 1179656 | tf_op jit(solution)/shard_map/ppermute | solution.py:30
  113.3 1.4 collective-permute-start.7
  116.3 28.1 %collective-permute-start.8 = (bf16[96,2304]{1,0:T(8,128)(2,1)}, bf16[96,2304]{1,0:T(8,128)(2,1)S(1)}, u32[]{:S(2)}, u32[]{:S(2)}) collective-permute-start(bf16[96,2304]{1,0:T(8,128)(2,1)} %get-tuple-element.44), channel_id=1, source_target_pairs={{0,8},{8,16},{16,24},{24,0},{1,9},{9,17},{17,25},{25,1},{2,10},{10... | collective-permute-start | bytes 1327112 | tf_op jit(solution)/shard_map/ppermute | solution.py:30
  117.7 12.7 %collective-permute-start.24 = (bf16[96,2048]{1,0:T(8,128)(2,1)}, bf16[96,2048]{1,0:T(8,128)(2,1)}, u32[]{:S(2)}, u32[]{:S(2)}) collective-permute-start(bf16[96,2048]{1,0:T(8,128)(2,1)} %get-tuple-element.55), channel_id=1, source_target_pairs={{0,4},{2,6},{4,0},{6,2},{1,5},{3,7},{5,1},{7,3},{8,12},{10,14},{12... | collective-permute-start | bytes 1179656 | tf_op jit(solution)/shard_map/ppermute | solution.py:30
  118.9 19.5 %collective-permute-start.25 = (bf16[96,2048]{1,0:T(8,128)(2,1)}, bf16[96,2048]{1,0:T(8,128)(2,1)}, u32[]{:S(2)}, u32[]{:S(2)}) collective-permute-start(bf16[96,2048]{1,0:T(8,128)(2,1)} %get-tuple-element.56), channel_id=1, source_target_pairs={{0,6},{2,0},{4,2},{6,4},{1,7},{3,1},{5,3},{7,5},{8,14},{10,8},{12,... | collective-permute-start | bytes 1179656 | tf_op jit(solution)/shard_map/ppermute | solution.py:30
  121.4 23.6 %collective-permute-start.9 = (bf16[96,2304]{1,0:T(8,128)(2,1)}, bf16[96,2304]{1,0:T(8,128)(2,1)S(1)}, u32[]{:S(2)}, u32[]{:S(2)}) collective-permute-start(bf16[96,2304]{1,0:T(8,128)(2,1)} %get-tuple-element.45), channel_id=1, source_target_pairs={{0,16},{8,24},{16,0},{24,8},{1,17},{9,25},{17,1},{25,9},{2,18},{10... | collective-permute-start | bytes 1327112 | tf_op jit(solution)/shard_map/ppermute | solution.py:30
  124.1 0.7 copy-start.2
  124.8 20.2 %collective-permute-start.10 = (bf16[96,2304]{1,0:T(8,128)(2,1)}, bf16[96,2304]{1,0:T(8,128)(2,1)S(1)}, u32[]{:S(2)}, u32[]{:S(2)}) collective-permute-start(bf16[96,2304]{1,0:T(8,128)(2,1)} %get-tuple-element.46), channel_id=1, source_target_pairs={{0,24},{8,0},{16,8},{24,16},{1,25},{9,1},{17,9},{25,17},{2,26},{10... | collective-permute-start | bytes 1327112 | tf_op jit(solution)/shard_map/ppermute | solution.py:30
  138.4 1.0 copy-start.3
  140.7 16.3 %copy-start.4 = (f32[64,352]{1,0:T(8,128)S(1)}, f32[64,352]{1,0:T(8,128)}, u32[]{:S(2)}) copy-start(f32[64,352]{1,0:T(8,128)} %gate.1) | copy-start | bytes 270340
  140.8 16.3 %copy-start.5 = (f32[64,352]{1,0:T(8,128)S(1)}, f32[64,352]{1,0:T(8,128)}, u32[]{:S(2)}) copy-start(f32[64,352]{1,0:T(8,128)} %up.1) | copy-start | bytes 270340
  140.8 16.3 %copy-start.6 = (f32[352,64]{0,1:T(8,128)S(1)}, f32[352,64]{0,1:T(8,128)}, u32[]{:S(2)}) copy-start(f32[352,64]{0,1:T(8,128)} %param.17) | copy-start | bytes 270340
  140.8 9.3 %collective-permute-start.28 = (bf16[24,2048]{1,0:T(8,128)(2,1)S(1)}, bf16[24,2048]{1,0:T(8,128)(2,1)S(1)}, u32[]{:S(2)}, u32[]{:S(2)}) collective-permute-start(bf16[24,2048]{1,0:T(8,128)(2,1)S(1)} %get-tuple-element.60), channel_id=1, source_target_pairs={{0,24},{8,0},{16,8},{24,16},{1,25},{9,1},{17,9},{25,17},{2,26},{10... | collective-permute-start | bytes 294920 | tf_op jit(solution)/shard_map/ppermute | solution.py:30
  142.6 7.4 %collective-permute-start.27 = (bf16[24,2048]{1,0:T(8,128)(2,1)S(1)}, bf16[24,2048]{1,0:T(8,128)(2,1)S(1)}, u32[]{:S(2)}, u32[]{:S(2)}) collective-permute-start(bf16[24,2048]{1,0:T(8,128)(2,1)S(1)} %get-tuple-element.59), channel_id=1, source_target_pairs={{0,16},{8,24},{16,0},{24,8},{1,17},{9,25},{17,1},{25,9},{2,18},{10... | collective-permute-start | bytes 294920 | tf_op jit(solution)/shard_map/ppermute | solution.py:30
  144.4 5.8 %collective-permute-start.26 = (bf16[24,2048]{1,0:T(8,128)(2,1)S(1)}, bf16[24,2048]{1,0:T(8,128)(2,1)S(1)}, u32[]{:S(2)}, u32[]{:S(2)}) collective-permute-start(bf16[24,2048]{1,0:T(8,128)(2,1)S(1)} %get-tuple-element.58), channel_id=1, source_target_pairs={{0,8},{8,16},{16,24},{24,0},{1,9},{9,17},{17,25},{25,1},{2,10},{10... | collective-permute-start | bytes 294920 | tf_op jit(solution)/shard_map/ppermute | solution.py:30
  146.6 6.2 %collective-permute-start.13 = (bf16[24,2048]{1,0:T(8,128)(2,1)S(1)}, bf16[24,2048]{1,0:T(8,128)(2,1)S(1)}, u32[]{:S(2)}, u32[]{:S(2)}) collective-permute-start(bf16[24,2048]{1,0:T(8,128)(2,1)S(1)} %get-tuple-element.50), channel_id=1, source_target_pairs={{0,6},{2,0},{4,2},{6,4},{1,7},{3,1},{5,3},{7,5},{8,14},{10,8},{12,... | collective-permute-start | bytes 294920 | tf_op jit(solution)/shard_map/ppermute | solution.py:30
  149.2 6.2 %collective-permute-start.12 = (bf16[24,2048]{1,0:T(8,128)(2,1)S(1)}, bf16[24,2048]{1,0:T(8,128)(2,1)S(1)}, u32[]{:S(2)}, u32[]{:S(2)}) collective-permute-start(bf16[24,2048]{1,0:T(8,128)(2,1)S(1)} %get-tuple-element.49), channel_id=1, source_target_pairs={{0,4},{2,6},{4,0},{6,2},{1,5},{3,7},{5,1},{7,3},{8,12},{10,14},{12... | collective-permute-start | bytes 294920 | tf_op jit(solution)/shard_map/ppermute | solution.py:30
  150.1 6.3 %collective-permute-start.11 = (bf16[24,2048]{1,0:T(8,128)(2,1)S(1)}, bf16[24,2048]{1,0:T(8,128)(2,1)S(1)}, u32[]{:S(2)}, u32[]{:S(2)}) collective-permute-start(bf16[24,2048]{1,0:T(8,128)(2,1)S(1)} %get-tuple-element.48), channel_id=1, source_target_pairs={{0,2},{2,4},{4,6},{6,0},{1,3},{3,5},{5,7},{7,1},{8,10},{10,12},{12... | collective-permute-start | bytes 294920 | tf_op jit(solution)/shard_map/ppermute | solution.py:30

commit v5 on v4

--- a/solution.py
+++ b/solution.py
@@ -113,7 +113,7 @@
         ahead, behind = piece[:half], piece[half:]
         behind = jnp.concatenate((behind, jnp.zeros((pad - part, shard), F32)))
         low = jnp.concatenate((ahead, behind), axis=1)
-        block = jnp.concatenate((top, jnp.zeros((pad - part, LANES), F32), low)).astype(BF16)
+        block = jnp.concatenate((top, low)).astype(BF16)
         for z in range(copies):
             out[z * count + y] = block
 
@@ -128,16 +128,17 @@
     )
 
 
-def unpack_kernel(pad, own, other, gate_up, down):
+def unpack_kernel(part, pad, own, other, gate_up, down):
     half = pad // 2
+    blank = jnp.zeros((pad - part, LANES), F32)
     for base, packed in ((0, own), (pad, other)):
         for tile in range(packed.shape[0] // 2):
             at = pl.ds(tile * LANES, LANES)
             low, high = exchange_lanes(packed[2 * tile].astype(F32), packed[2 * tile + 1].astype(F32))
-            gate_up[pl.ds(base, pad), at] = low[:pad].astype(BF16)
-            gate_up[pl.ds(2 * pad + base, pad), at] = high[:pad].astype(BF16)
-            down[pl.ds(base, half), at] = low[pad:].astype(BF16)
-            down[pl.ds(base + half, half), at] = high[pad:].astype(BF16)
+            for row, value in ((base, low), (2 * pad + base, high)):
+                gate_up[pl.ds(row, pad), at] = jnp.concatenate((value[:part], blank)).astype(BF16)
+            down[pl.ds(base, half), at] = low[part:].astype(BF16)
+            down[pl.ds(base + half, half), at] = high[part:].astype(BF16)
 
 
 def backward_kernel(ny, nx, rows, pad, gate_up, down, prev, cotangent, kept, sent, grads):
@@ -174,13 +175,13 @@
         out[...] = total[k * rows : (k + 1) * rows].astype(BF16)
 
 
-def pair_kernel(pad, kept, received, out):
+def pair_kernel(part, pad, kept, received, out):
     half = pad // 2
     for tile in range(out.shape[0] // 2):
         at = pl.ds(tile * LANES, LANES)
         total = kept[:, at] + received[:, at].astype(F32)
-        left = jnp.concatenate((total[:pad], total[2 * pad : 2 * pad + half]))
-        right = jnp.concatenate((total[pad : 2 * pad], total[2 * pad + half :]))
+        left = jnp.concatenate((total[:part], total[2 * pad : 2 * pad + half]))
+        right = jnp.concatenate((total[pad : pad + part], total[2 * pad + half :]))
         even, odd = exchange_lanes(left, right)
         out[2 * tile] = even.astype(BF16)
         out[2 * tile + 1] = odd.astype(BF16)
@@ -195,7 +196,7 @@
         for z in range(1, arrived.shape[0] // ny):
             total = total + arrived[z * ny + y].astype(F32)
         tops.append(total[:part])
-        low = total[pad:]
+        low = total[part:]
         lows.append(low)
         lows.append(pltpu.roll(low, LANES // 2, 1)[: part - half])
     both = jnp.concatenate(tops).T
@@ -259,7 +260,7 @@
     units = gate_w.shape[1]
     part = units // ny
     pad = -(-part // 32) * 32
-    block = (nz * ny, pad + pad // 2, LANES)
+    block = (nz * ny, part + pad // 2, LANES)
     token_ops = 2 * group * 2 * pad * width
 
     second, packed = whole(
@@ -285,7 +286,7 @@
     cotangents = around(second[:, :width], "x")
     nexts = around(second[:, width:], "x")
     gate_up, down = whole(
-        functools.partial(unpack_kernel, pad),
+        functools.partial(unpack_kernel, part, pad),
         (like((4 * pad, width), BF16), like((2 * pad, width), BF16)),
         (own, other),
     )
@@ -305,7 +306,7 @@
         (grads, gate_up),
         flops=2 * token_ops,
     )
-    paired = whole(functools.partial(pair_kernel, pad), like(block, BF16), (kept, received))
+    paired = whole(functools.partial(pair_kernel, part, pad), like(block, BF16), (kept, received))
     arrived = spread(paired, FS)
     new_gate, new_up, new_down_t = whole(
         functools.partial(update_kernel, ny, part, pad, factor),

time: 159 us -> 158 us (level)
    ppermute x27, waiting for transfers between devices: 58.1 us -> 61.9 us  [moved(): lax.ppermute(array, axis, [(i, (i + step) % length) for i in range(length)])]
    all_to_all x2, waiting for transfers between devices: 3.3 us -> 0.01 us  [spread(): return lax.all_to_all(blocks, axis, 0, 0, tiled=True)]
where the time goes in v5:
time: 158 us; the launch traced here: 157 us
  starting transfers between devices  66.3 us (42%)
  waiting for transfers between devices  66 us (42%)
  Pallas kernels  17.7 us (11%)
  local copies, waits for them, and re-layouts  3.54 us (2%)
  other arithmetic  3.01 us (2%)
    ppermute x27, waiting for transfers between devices, moved(): lax.ppermute(array, axis, [(i, (i + step) % length) for i in range(length)])  61.9 us
    ppermute x27, starting transfers between devices, moved(): lax.ppermute(array, axis, [(i, (i + step) % length) for i in range(length)])  47.2 us
    all_to_all x2, starting transfers between devices, spread(): return lax.all_to_all(blocks, axis, 0, 0, tiled=True)  18.9 us
    pallas_call x10, Pallas kernels, whole(): pl.pallas_call(kernel, out_shape=out_shape, in_specs=[pl.BlockSpec(memory...  17.7 us
    ppermute x3, waiting for transfers between devices, swapped(): return lax.ppermute(array, 'c', [(0, 1), (1, 0)])  4.14 us
    unnamed x22, local copies, waits for them, and re-layouts  3.47 us
  transfers between devices with their start and end apart: 32, of which 16 were waited for; matrix products, arithmetic and copies ran while one was open for 2% of the time, Pallas kernels for 5%

profile of v5, /device:TPU:64, one launch (start us, length us, event | category | flops | bytes accessed | tf_op | source)
XLA Modules:
  0.0 157.4 jit_solution(14603722415019798363)
XLA Ops:
  0.6 2.3 %shard_map.136 = (bf16[24,4096]{1,0:T(8,128)(2,1)}, bf16[32,136,128]{2,1,0:T(8,128)(2,1)}) custom-call(bf16[24,2048]{1,0:T(8,128)(2,1)} %refs_0_.1, bf16[24,2048]{1,0:T(8,128)(2,1)} %refs_1_.1, bf16[64,352]{1,0:T(8,128)(2,1)} %refs_2_.1, bf16[64,352]{1,0:T(8,128)(2,1)} %refs_3_.1, bf16[64,352]{1,0:T(8,128)(2,1)} %bitcast.30), custom_call_target="tpu_custom_call" | custom-call | tf_op jit(solution)/shard_map/pallas_call | solution.py:59
  2.9 11.1 %all-to-all-start = ((bf16[32,136,128]{2,1,0:T(8,128)(2,1)}), bf16[32,136,128]{2,1,0:T(8,128)(2,1)S(1)}, u32[]{:S(2)}, u32[]{:S(2)}) async-start(bf16[32,136,128]{2,1,0:T(8,128)(2,1)} %get-tuple-element.36), calls=%async_computation | async-start | bytes 2228224 | tf_op jit(solution)/shard_map/all_to_all | solution.py:21
  14.0 1.6 collective-permute-start.16
  15.6 2.7 %collective-permute-start.15 = (bf16[24,2048]{1,0:T(8,128)(2,1)S(1)}, bf16[24,2048]{1,0:T(8,128)(2,1)S(1)}, u32[]{:S(2)}, u32[]{:S(2)}) collective-permute-start(bf16[24,2048]{1,0:T(8,128)(2,1)S(1)} %copy-done.10), channel_id=1, source_target_pairs={{0,4},{2,6},{4,0},{6,2},{1,5},{3,7},{5,1},{7,3},{8,12},{10,14},{12... | collective-permute-start | bytes 294920 | tf_op jit(solution)/shard_map/ppermute | solution.py:30
  18.3 1.4 collective-permute-start.14
  19.8 1.5 collective-permute-start.3
  21.2 2.7 %collective-permute-start.2 = (bf16[24,4096]{1,0:T(8,128)(2,1)S(1)}, bf16[24,4096]{1,0:T(8,128)(2,1)S(1)}, u32[]{:S(2)}, u32[]{:S(2)}) collective-permute-start(bf16[24,4096]{1,0:T(8,128)(2,1)S(1)} %copy-done.9), channel_id=1, source_target_pairs={{0,16},{8,24},{16,0},{24,8},{1,17},{9,25},{17,1},{25,9},{2,18},{10... | collective-permute-start | bytes 589832 | tf_op jit(solution)/shard_map/ppermute | solution.py:30
  23.9 1.5 collective-permute-start.1
  26.1 1.1 collective-permute-start.18
  27.2 11.3 %collective-permute-done.3 = bf16[24,4096]{1,0:T(8,128)(2,1)S(1)} collective-permute-done((bf16[24,4096]{1,0:T(8,128)(2,1)S(1)}, bf16[24,4096]{1,0:T(8,128)(2,1)S(1)}, u32[]{:S(2)}, u32[]{:S(2)}) %collective-permute-start.3) | collective-permute-done | bytes 196640 | tf_op jit(solution)/shard_map/ppermute | solution.py:30
  38.5 2.7 %collective-permute-done.2 = bf16[24,4096]{1,0:T(8,128)(2,1)S(1)} collective-permute-done((bf16[24,4096]{1,0:T(8,128)(2,1)S(1)}, bf16[24,4096]{1,0:T(8,128)(2,1)S(1)}, u32[]{:S(2)}, u32[]{:S(2)}) %collective-permute-start.2) | collective-permute-done | bytes 196640 | tf_op jit(solution)/shard_map/ppermute | solution.py:30
  41.2 2.9 %collective-permute-done.1 = bf16[24,4096]{1,0:T(8,128)(2,1)S(1)} collective-permute-done((bf16[24,4096]{1,0:T(8,128)(2,1)S(1)}, bf16[24,4096]{1,0:T(8,128)(2,1)S(1)}, u32[]{:S(2)}, u32[]{:S(2)}) %collective-permute-start.1) | collective-permute-done | bytes 196640 | tf_op jit(solution)/shard_map/ppermute | solution.py:30
  45.2 4.3 %collective-permute-done.19 = bf16[96,2048]{1,0:T(8,128)(2,1)S(1)} collective-permute-done((bf16[96,2048]{1,0:T(8,128)(2,1)S(1)}, bf16[96,2048]{1,0:T(8,128)(2,1)S(1)}, u32[]{:S(2)}, u32[]{:S(2)}) %collective-permute-start.19) | collective-permute-done | bytes 393248 | tf_op jit(solution)/shard_map/ppermute | solution.py:30
  49.5 8.7 %collective-permute-start.21 = (bf16[96,2048]{1,0:T(8,128)(2,1)S(1)}, bf16[96,2048]{1,0:T(8,128)(2,1)S(1)}, u32[]{:S(2)}, u32[]{:S(2)}) collective-permute-start(bf16[96,2048]{1,0:T(8,128)(2,1)S(1)} %get-tuple-element.66), channel_id=1, source_target_pairs={{0,4},{2,6},{4,0},{6,2},{1,5},{3,7},{5,1},{7,3},{8,12},{10,14},{12... | collective-permute-start | bytes 1179656 | tf_op jit(solution)/shard_map/ppermute | solution.py:30
  58.2 2.1 %collective-permute-start.20 = (bf16[96,2048]{1,0:T(8,128)(2,1)S(1)}, bf16[96,2048]{1,0:T(8,128)(2,1)S(1)}, u32[]{:S(2)}, u32[]{:S(2)}) collective-permute-start(bf16[96,2048]{1,0:T(8,128)(2,1)S(1)} %get-tuple-element.66), channel_id=1, source_target_pairs={{0,6},{2,0},{4,2},{6,4},{1,7},{3,1},{5,3},{7,5},{8,14},{10,8},{12,... | collective-permute-start | bytes 1179656 | tf_op jit(solution)/shard_map/ppermute | solution.py:30
  60.3 1.2 pad_maximum_fusion.prev
  61.5 4.3 %collective-permute-done.21 = bf16[96,2048]{1,0:T(8,128)(2,1)S(1)} collective-permute-done((bf16[96,2048]{1,0:T(8,128)(2,1)S(1)}, bf16[96,2048]{1,0:T(8,128)(2,1)S(1)}, u32[]{:S(2)}, u32[]{:S(2)}) %collective-permute-start.21) | collective-permute-done | bytes 393248 | tf_op jit(solution)/shard_map/ppermute | solution.py:30
  65.8 4.1 %collective-permute-done.20 = bf16[96,2048]{1,0:T(8,128)(2,1)S(1)} collective-permute-done((bf16[96,2048]{1,0:T(8,128)(2,1)S(1)}, bf16[96,2048]{1,0:T(8,128)(2,1)S(1)}, u32[]{:S(2)}, u32[]{:S(2)}) %collective-permute-start.20) | collective-permute-done | bytes 393248 | tf_op jit(solution)/shard_map/ppermute | solution.py:30
  70.2 0.9 shard_map.137
  71.1 3.6 %shard_map.141 = (f32[288,2048]{1,0:T(8,128)S(1)}, bf16[288,2048]{1,0:T(8,128)(2,1)S(1)}, bf16[384,384]{1,0:T(8,128)(2,1)S(1)}) custom-call(bf16[384,2048]{1,0:T(8,128)(2,1)S(1)} %get-tuple-element.37.gate_up, bf16[192,2048]{1,0:T(8,128)(2,1)S(1)} %get-tuple-element.40.down, bf16[384,2048]{1,0:T(8,128)(2,1)S(1)} %pad_maximum_fusion.prev, ...), custom_call_target="tpu_custom_call" | custom-call | flops 1811939328 | tf_op jit(solution)/shard_map/pallas_call | solution.py:59
  75.5 2.8 %collective-permute-done.29.received = bf16[288,2048]{1,0:T(8,128)(2,1)S(1)} collective-permute-done((bf16[288,2048]{1,0:T(8,128)(2,1)S(1)}, bf16[288,2048]{1,0:T(8,128)(2,1)S(1)}, u32[]{:S(2)}, u32[]{:S(2)}) %collective-permute-start.29) | collective-permute-done | bytes 1179680 | tf_op jit(solution)/shard_map/ppermute | solution.py:25
  78.3 1.5 shard_map.144
  79.9 7.9 %all-to-all-start.1 = ((bf16[32,136,128]{2,1,0:T(8,128)(2,1)}), bf16[32,136,128]{2,1,0:T(8,128)(2,1)S(1)}, u32[]{:S(2)}, u32[]{:S(2)}) async-start(bf16[32,136,128]{2,1,0:T(8,128)(2,1)} %shard_map.144), calls=%async_computation.1 | async-start | bytes 2228224 | tf_op jit(solution)/shard_map/all_to_all | solution.py:21
  87.7 2.9 %collective-permute-start.4 = (bf16[96,2048]{1,0:T(8,128)(2,1)S(1)}, bf16[96,2048]{1,0:T(8,128)(2,1)S(1)}, u32[]{:S(2)}, u32[]{:S(2)}) collective-permute-start(bf16[96,2048]{1,0:T(8,128)(2,1)S(1)} %get-tuple-element.67.refs_0_), channel_id=1, source_target_pairs={{0,6},{2,0},{4,2},{6,4},{1,7},{3,1},{5,3},{7,5},{8,14},{10,8},{12,... | collective-permute-start | bytes 1179656 | tf_op jit(solution)/shard_map/ppermute | solution.py:30
  90.7 0.9 collective-permute-start.6
  91.6 1.0 copy-done.8
  92.6 2.1 %shard_map.142 = (bf16[96,2048]{1,0:T(8,128)(2,1)S(1)}, bf16[96,2048]{1,0:T(8,128)(2,1)S(1)}, bf16[96,2048]{1,0:T(8,128)(2,1)}, bf16[96,2048]{1,0:T(8,128)(2,1)}) custom-call(bf16[384,384]{1,0:T(8,128)(2,1)S(1)} %copy-done.8, bf16[384,2048]{1,0:T(8,128)(2,1)S(1)} %get-tuple-element.37.gate_up), custom_call_target="tpu_custom_call" | custom-call | flops 603979776 | tf_op jit(solution)/shard_map/pallas_call | solution.py:59
  94.7 2.5 %collective-permute-start.23 = (bf16[96,2048]{1,0:T(8,128)(2,1)S(1)}, bf16[96,2048]{1,0:T(8,128)(2,1)S(1)}, u32[]{:S(2)}, u32[]{:S(2)}) collective-permute-start(bf16[96,2048]{1,0:T(8,128)(2,1)S(1)} %get-tuple-element.54), channel_id=1, source_target_pairs={{0,2},{2,4},{4,6},{6,0},{1,3},{3,5},{5,7},{7,1},{8,10},{10,12},{12... | collective-permute-start | bytes 1179656 | tf_op jit(solution)/shard_map/ppermute | solution.py:30
  97.2 10.0 %collective-permute-done.4.refs_1_ = bf16[96,2048]{1,0:T(8,128)(2,1)S(1)} collective-permute-done((bf16[96,2048]{1,0:T(8,128)(2,1)S(1)}, bf16[96,2048]{1,0:T(8,128)(2,1)S(1)}, u32[]{:S(2)}, u32[]{:S(2)}) %collective-permute-start.4) | collective-permute-done | bytes 393248 | tf_op jit(solution)/shard_map/ppermute | solution.py:30
  107.2 3.8 %collective-permute-done.6.refs_3_ = bf16[96,2048]{1,0:T(8,128)(2,1)S(1)} collective-permute-done((bf16[96,2048]{1,0:T(8,128)(2,1)S(1)}, bf16[96,2048]{1,0:T(8,128)(2,1)S(1)}, u32[]{:S(2)}, u32[]{:S(2)}) %collective-permute-start.6) | collective-permute-done | bytes 393248 | tf_op jit(solution)/shard_map/ppermute | solution.py:30
  111.0 1.9 %shard_map.138 = (bf16[384,128]{1,0:T(8,128)(2,1)S(1)}, bf16[384,128]{1,0:T(8,128)(2,1)S(1)}, bf16[384,192]{1,0:T(8,128)(2,1)S(1)}) custom-call(bf16[384,2048]{1,0:T(8,128)(2,1)S(1)} %get-tuple-element.37.gate_up, bf16[96,2048]{1,0:T(8,128)(2,1)S(1)} %get-tuple-element.67.refs_0_, bf16[96,2048]{1,0:T(8,128)(2,1)S(1)} %collective-permute-done.4.refs_1_, ...), custom_call_target="tpu_custom_call" | custom-call | flops 603979776 | tf_op jit(solution)/shard_map/pallas_call | solution.py:59
  113.1 1.3 collective-permute-done.7.partner
  114.3 1.6 shard_map.139
  115.9 1.5 collective-permute-start.8
  117.4 1.1 collective-permute-start.24
  118.5 1.7 %collective-permute-start.25 = (bf16[96,2048]{1,0:T(8,128)(2,1)}, bf16[96,2048]{1,0:T(8,128)(2,1)}, u32[]{:S(2)}, u32[]{:S(2)}) collective-permute-start(bf16[96,2048]{1,0:T(8,128)(2,1)} %get-tuple-element.56), channel_id=1, source_target_pairs={{0,6},{2,0},{4,2},{6,4},{1,7},{3,1},{5,3},{7,5},{8,14},{10,8},{12,... | collective-permute-start | bytes 1179656 | tf_op jit(solution)/shard_map/ppermute | solution.py:30
  120.2 2.7 %collective-permute-start.9 = (bf16[96,2304]{1,0:T(8,128)(2,1)}, bf16[96,2304]{1,0:T(8,128)(2,1)S(1)}, u32[]{:S(2)}, u32[]{:S(2)}) collective-permute-start(bf16[96,2304]{1,0:T(8,128)(2,1)} %get-tuple-element.45), channel_id=1, source_target_pairs={{0,16},{8,24},{16,0},{24,8},{1,17},{9,25},{17,1},{25,9},{2,18},{10... | collective-permute-start | bytes 1327112 | tf_op jit(solution)/shard_map/ppermute | solution.py:30
  123.7 1.5 collective-permute-start.10
  125.1 5.0 %collective-permute-done.24.refs_2_ = bf16[96,2048]{1,0:T(8,128)(2,1)} collective-permute-done((bf16[96,2048]{1,0:T(8,128)(2,1)}, bf16[96,2048]{1,0:T(8,128)(2,1)}, u32[]{:S(2)}, u32[]{:S(2)}) %collective-permute-start.24) | collective-permute-done | bytes 393248 | tf_op jit(solution)/shard_map/ppermute | solution.py:30
  130.1 7.9 %collective-permute-done.25.refs_3_ = bf16[96,2048]{1,0:T(8,128)(2,1)} collective-permute-done((bf16[96,2048]{1,0:T(8,128)(2,1)}, bf16[96,2048]{1,0:T(8,128)(2,1)}, u32[]{:S(2)}, u32[]{:S(2)}) %collective-permute-start.25) | collective-permute-done | bytes 393248 | tf_op jit(solution)/shard_map/ppermute | solution.py:30
  138.0 1.0 copy-done.3
  139.0 1.3 shard_map.143
  140.4 1.9 %collective-permute-start.28 = (bf16[24,2048]{1,0:T(8,128)(2,1)S(1)}, bf16[24,2048]{1,0:T(8,128)(2,1)S(1)}, u32[]{:S(2)}, u32[]{:S(2)}) collective-permute-start(bf16[24,2048]{1,0:T(8,128)(2,1)S(1)} %get-tuple-element.60), channel_id=1, source_target_pairs={{0,24},{8,0},{16,8},{24,16},{1,25},{9,1},{17,9},{25,17},{2,26},{10... | collective-permute-start | bytes 294920 | tf_op jit(solution)/shard_map/ppermute | solution.py:30
  142.2 1.8 %collective-permute-start.27 = (bf16[24,2048]{1,0:T(8,128)(2,1)S(1)}, bf16[24,2048]{1,0:T(8,128)(2,1)S(1)}, u32[]{:S(2)}, u32[]{:S(2)}) collective-permute-start(bf16[24,2048]{1,0:T(8,128)(2,1)S(1)} %get-tuple-element.59), channel_id=1, source_target_pairs={{0,16},{8,24},{16,0},{24,8},{1,17},{9,25},{17,1},{25,9},{2,18},{10... | collective-permute-start | bytes 294920 | tf_op jit(solution)/shard_map/ppermute | solution.py:30
  144.6 1.5 shard_map.140
  146.2 2.6 %collective-permute-start.13 = (bf16[24,2048]{1,0:T(8,128)(2,1)S(1)}, bf16[24,2048]{1,0:T(8,128)(2,1)S(1)}, u32[]{:S(2)}, u32[]{:S(2)}) collective-permute-start(bf16[24,2048]{1,0:T(8,128)(2,1)S(1)} %get-tuple-element.50), channel_id=1, source_target_pairs={{0,6},{2,0},{4,2},{6,4},{1,7},{3,1},{5,3},{7,5},{8,14},{10,8},{12,... | collective-permute-start | bytes 294920 | tf_op jit(solution)/shard_map/ppermute | solution.py:30
  150.5 1.8 %collective-permute-done.13 = bf16[24,2048]{1,0:T(8,128)(2,1)S(1)} collective-permute-done((bf16[24,2048]{1,0:T(8,128)(2,1)S(1)}, bf16[24,2048]{1,0:T(8,128)(2,1)S(1)}, u32[]{:S(2)}, u32[]{:S(2)}) %collective-permute-start.13) | collective-permute-done | bytes 98336 | tf_op jit(solution)/shard_map/ppermute | solution.py:30
  152.3 2.7 %collective-permute-done.12 = bf16[24,2048]{1,0:T(8,128)(2,1)S(1)} collective-permute-done((bf16[24,2048]{1,0:T(8,128)(2,1)S(1)}, bf16[24,2048]{1,0:T(8,128)(2,1)S(1)}, u32[]{:S(2)}, u32[]{:S(2)}) %collective-permute-start.12) | collective-permute-done | bytes 98336 | tf_op jit(solution)/shard_map/ppermute | solution.py:30
  (56 shorter events, 8.3 us)
Async XLA Ops:
  0.6 13.4 %copy-start.10 = (bf16[24,2048]{1,0:T(8,128)(2,1)S(1)}, bf16[24,2048]{1,0:T(8,128)(2,1)}, u32[]{:S(2)}) copy-start(bf16[24,2048]{1,0:T(8,128)(2,1)} %param.10) | copy-start | bytes 294916
  2.9 16.8 %copy-start.9 = (bf16[24,4096]{1,0:T(8,128)(2,1)S(1)}, bf16[24,4096]{1,0:T(8,128)(2,1)}, u32[]{:S(2)}) copy-start(bf16[24,4096]{1,0:T(8,128)(2,1)} %get-tuple-element.38) | copy-start | bytes 589828
  2.9 41.3 %all-to-all-start = ((bf16[32,136,128]{2,1,0:T(8,128)(2,1)}), bf16[32,136,128]{2,1,0:T(8,128)(2,1)S(1)}, u32[]{:S(2)}, u32[]{:S(2)}) async-start(bf16[32,136,128]{2,1,0:T(8,128)(2,1)} %get-tuple-element.36), calls=%async_computation | async-start | bytes 2228224 | tf_op jit(solution)/shard_map/all_to_all | solution.py:21
  14.0 9.9 %collective-permute-start.16 = (bf16[24,2048]{1,0:T(8,128)(2,1)S(1)}, bf16[24,2048]{1,0:T(8,128)(2,1)S(1)}, u32[]{:S(2)}, u32[]{:S(2)}) collective-permute-start(bf16[24,2048]{1,0:T(8,128)(2,1)S(1)} %copy-done.10), channel_id=1, source_target_pairs={{0,2},{2,4},{4,6},{6,0},{1,3},{3,5},{5,7},{7,1},{8,10},{10,12},{12... | collective-permute-start | bytes 294920 | tf_op jit(solution)/shard_map/ppermute | solution.py:30
  15.6 9.8 %collective-permute-start.15 = (bf16[24,2048]{1,0:T(8,128)(2,1)S(1)}, bf16[24,2048]{1,0:T(8,128)(2,1)S(1)}, u32[]{:S(2)}, u32[]{:S(2)}) collective-permute-start(bf16[24,2048]{1,0:T(8,128)(2,1)S(1)} %copy-done.10), channel_id=1, source_target_pairs={{0,4},{2,6},{4,0},{6,2},{1,5},{3,7},{5,1},{7,3},{8,12},{10,14},{12... | collective-permute-start | bytes 294920 | tf_op jit(solution)/shard_map/ppermute | solution.py:30
  18.3 7.0 %collective-permute-start.14 = (bf16[24,2048]{1,0:T(8,128)(2,1)S(1)}, bf16[24,2048]{1,0:T(8,128)(2,1)S(1)}, u32[]{:S(2)}, u32[]{:S(2)}) collective-permute-start(bf16[24,2048]{1,0:T(8,128)(2,1)S(1)} %copy-done.10), channel_id=1, source_target_pairs={{0,6},{2,0},{4,2},{6,4},{1,7},{3,1},{5,3},{7,5},{8,14},{10,8},{12,... | collective-permute-start | bytes 294920 | tf_op jit(solution)/shard_map/ppermute | solution.py:30
  19.8 18.8 %collective-permute-start.3 = (bf16[24,4096]{1,0:T(8,128)(2,1)S(1)}, bf16[24,4096]{1,0:T(8,128)(2,1)S(1)}, u32[]{:S(2)}, u32[]{:S(2)}) collective-permute-start(bf16[24,4096]{1,0:T(8,128)(2,1)S(1)} %copy-done.9), channel_id=1, source_target_pairs={{0,8},{8,16},{16,24},{24,0},{1,9},{9,17},{17,25},{25,1},{2,10},{10... | collective-permute-start | bytes 589832 | tf_op jit(solution)/shard_map/ppermute | solution.py:30
  21.2 20.0 %collective-permute-start.2 = (bf16[24,4096]{1,0:T(8,128)(2,1)S(1)}, bf16[24,4096]{1,0:T(8,128)(2,1)S(1)}, u32[]{:S(2)}, u32[]{:S(2)}) collective-permute-start(bf16[24,4096]{1,0:T(8,128)(2,1)S(1)} %copy-done.9), channel_id=1, source_target_pairs={{0,16},{8,24},{16,0},{24,8},{1,17},{9,25},{17,1},{25,9},{2,18},{10... | collective-permute-start | bytes 589832 | tf_op jit(solution)/shard_map/ppermute | solution.py:30
  23.9 20.3 %collective-permute-start.1 = (bf16[24,4096]{1,0:T(8,128)(2,1)S(1)}, bf16[24,4096]{1,0:T(8,128)(2,1)S(1)}, u32[]{:S(2)}, u32[]{:S(2)}) collective-permute-start(bf16[24,4096]{1,0:T(8,128)(2,1)S(1)} %copy-done.9), channel_id=1, source_target_pairs={{0,24},{8,0},{16,8},{24,16},{1,25},{9,1},{17,9},{25,17},{2,26},{10... | collective-permute-start | bytes 589832 | tf_op jit(solution)/shard_map/ppermute | solution.py:30
  25.4 24.1 %collective-permute-start.19 = (bf16[96,2048]{1,0:T(8,128)(2,1)S(1)}, bf16[96,2048]{1,0:T(8,128)(2,1)S(1)}, u32[]{:S(2)}, u32[]{:S(2)}) collective-permute-start(bf16[96,2048]{1,0:T(8,128)(2,1)S(1)} %bitcast.18), channel_id=1, source_target_pairs={{0,8},{8,16},{16,24},{24,0},{1,9},{9,17},{17,25},{25,1},{2,10},{10... | collective-permute-start | bytes 1179656 | tf_op jit(solution)/shard_map/ppermute | solution.py:30
  26.1 32.1 %collective-permute-start.18 = (bf16[96,2048]{1,0:T(8,128)(2,1)S(1)}, bf16[96,2048]{1,0:T(8,128)(2,1)}, u32[]{:S(2)}, u32[]{:S(2)}) collective-permute-start(bf16[96,2048]{1,0:T(8,128)(2,1)S(1)} %bitcast.19), channel_id=1, source_target_pairs={{0,16},{8,24},{16,0},{24,8},{1,17},{9,25},{17,1},{25,9},{2,18},{10... | collective-permute-start | bytes 1179656 | tf_op jit(solution)/shard_map/ppermute | solution.py:30
  38.5 21.8 %collective-permute-start.17 = (bf16[96,2048]{1,0:T(8,128)(2,1)S(1)}, bf16[96,2048]{1,0:T(8,128)(2,1)}, u32[]{:S(2)}, u32[]{:S(2)}) collective-permute-start(bf16[96,2048]{1,0:T(8,128)(2,1)S(1)} %bitcast.20), channel_id=1, source_target_pairs={{0,24},{8,0},{16,8},{24,16},{1,25},{9,1},{17,9},{25,17},{2,26},{10... | collective-permute-start | bytes 1179656 | tf_op jit(solution)/shard_map/ppermute | solution.py:30
  44.3 25.9 %collective-permute-start = (bf16[32,136,128]{2,1,0:T(8,128)(2,1)S(1)}, bf16[32,136,128]{2,1,0:T(8,128)(2,1)S(1)}, u32[]{:S(2)}, u32[]{:S(2)}) collective-permute-start(bf16[32,136,128]{2,1,0:T(8,128)(2,1)S(1)} %all-to-all-done.own), channel_id=1, source_target_pairs={{0,1},{1,0},{2,3},{3,2},{4,5},{5,4},{6,7},{7,6},{8,9},{9,8},{10,11... | collective-permute-start | bytes 3342344 | tf_op jit(solution)/shard_map/ppermute | solution.py:25
  44.5 17.1 %collective-permute-start.22 = (bf16[96,2048]{1,0:T(8,128)(2,1)S(1)}, bf16[96,2048]{1,0:T(8,128)(2,1)S(1)}, u32[]{:S(2)}, u32[]{:S(2)}) collective-permute-start(bf16[96,2048]{1,0:T(8,128)(2,1)S(1)} %get-tuple-element.66), channel_id=1, source_target_pairs={{0,2},{2,4},{4,6},{6,0},{1,3},{3,5},{5,7},{7,1},{8,10},{10,12},{12... | collective-permute-start | bytes 1179656 | tf_op jit(solution)/shard_map/ppermute | solution.py:30
  49.5 16.4 %collective-permute-start.21 = (bf16[96,2048]{1,0:T(8,128)(2,1)S(1)}, bf16[96,2048]{1,0:T(8,128)(2,1)S(1)}, u32[]{:S(2)}, u32[]{:S(2)}) collective-permute-start(bf16[96,2048]{1,0:T(8,128)(2,1)S(1)} %get-tuple-element.66), channel_id=1, source_target_pairs={{0,4},{2,6},{4,0},{6,2},{1,5},{3,7},{5,1},{7,3},{8,12},{10,14},{12... | collective-permute-start | bytes 1179656 | tf_op jit(solution)/shard_map/ppermute | solution.py:30
  58.2 11.8 %collective-permute-start.20 = (bf16[96,2048]{1,0:T(8,128)(2,1)S(1)}, bf16[96,2048]{1,0:T(8,128)(2,1)S(1)}, u32[]{:S(2)}, u32[]{:S(2)}) collective-permute-start(bf16[96,2048]{1,0:T(8,128)(2,1)S(1)} %get-tuple-element.66), channel_id=1, source_target_pairs={{0,6},{2,0},{4,2},{6,4},{1,7},{3,1},{5,3},{7,5},{8,14},{10,8},{12,... | collective-permute-start | bytes 1179656 | tf_op jit(solution)/shard_map/ppermute | solution.py:30
  71.1 3.6 %copy-start = (bf16[192,2048]{1,0:T(8,128)(2,1)}, bf16[192,2048]{1,0:T(8,128)(2,1)S(1)}, u32[]{:S(2)}) copy-start(bf16[192,2048]{1,0:T(8,128)(2,1)S(1)} %get-tuple-element.40.down) | copy-start | bytes 2359300
  74.8 0.7 copy-start.7
  75.5 2.8 %collective-permute-start.29 = (bf16[288,2048]{1,0:T(8,128)(2,1)S(1)}, bf16[288,2048]{1,0:T(8,128)(2,1)S(1)}, u32[]{:S(2)}, u32[]{:S(2)}) collective-permute-start(bf16[288,2048]{1,0:T(8,128)(2,1)S(1)} %get-tuple-element.62), channel_id=1, source_target_pairs={{0,1},{1,0},{2,3},{3,2},{4,5},{5,4},{6,7},{7,6},{8,9},{9,8},{10,11... | collective-permute-start | bytes 3538952 | tf_op jit(solution)/shard_map/ppermute | solution.py:25
  79.9 76.6 %all-to-all-start.1 = ((bf16[32,136,128]{2,1,0:T(8,128)(2,1)}), bf16[32,136,128]{2,1,0:T(8,128)(2,1)S(1)}, u32[]{:S(2)}, u32[]{:S(2)}) async-start(bf16[32,136,128]{2,1,0:T(8,128)(2,1)} %shard_map.144), calls=%async_computation.1 | async-start | bytes 2228224 | tf_op jit(solution)/shard_map/all_to_all | solution.py:21
  87.7 19.5 %collective-permute-start.4 = (bf16[96,2048]{1,0:T(8,128)(2,1)S(1)}, bf16[96,2048]{1,0:T(8,128)(2,1)S(1)}, u32[]{:S(2)}, u32[]{:S(2)}) collective-permute-start(bf16[96,2048]{1,0:T(8,128)(2,1)S(1)} %get-tuple-element.67.refs_0_), channel_id=1, source_target_pairs={{0,6},{2,0},{4,2},{6,4},{1,7},{3,1},{5,3},{7,5},{8,14},{10,8},{12,... | collective-permute-start | bytes 1179656 | tf_op jit(solution)/shard_map/ppermute | solution.py:30
  90.7 16.5 %collective-permute-start.5 = (bf16[96,2048]{1,0:T(8,128)(2,1)S(1)}, bf16[96,2048]{1,0:T(8,128)(2,1)S(1)}, u32[]{:S(2)}, u32[]{:S(2)}) collective-permute-start(bf16[96,2048]{1,0:T(8,128)(2,1)S(1)} %get-tuple-element.67.refs_0_), channel_id=1, source_target_pairs={{0,4},{2,6},{4,0},{6,2},{1,5},{3,7},{5,1},{7,3},{8,12},{10,14},{12... | collective-permute-start | bytes 1179656 | tf_op jit(solution)/shard_map/ppermute | solution.py:30
  90.7 20.3 %collective-permute-start.6 = (bf16[96,2048]{1,0:T(8,128)(2,1)S(1)}, bf16[96,2048]{1,0:T(8,128)(2,1)S(1)}, u32[]{:S(2)}, u32[]{:S(2)}) collective-permute-start(bf16[96,2048]{1,0:T(8,128)(2,1)S(1)} %get-tuple-element.67.refs_0_), channel_id=1, source_target_pairs={{0,2},{2,4},{4,6},{6,0},{1,3},{3,5},{5,7},{7,1},{8,10},{10,12},{12... | collective-permute-start | bytes 1179656 | tf_op jit(solution)/shard_map/ppermute | solution.py:30
  91.6 1.0 copy-start.8
  94.7 19.7 %copy-start.1 = (bf16[192,2048]{1,0:T(8,128)(2,1)S(1)}, bf16[192,2048]{1,0:T(8,128)(2,1)}, u32[]{:S(2)}) copy-start(bf16[192,2048]{1,0:T(8,128)(2,1)} %copy-done) | copy-start | bytes 2359300
  94.7 28.2 %collective-permute-start.23 = (bf16[96,2048]{1,0:T(8,128)(2,1)S(1)}, bf16[96,2048]{1,0:T(8,128)(2,1)S(1)}, u32[]{:S(2)}, u32[]{:S(2)}) collective-permute-start(bf16[96,2048]{1,0:T(8,128)(2,1)S(1)} %get-tuple-element.54), channel_id=1, source_target_pairs={{0,2},{2,4},{4,6},{6,0},{1,3},{3,5},{5,7},{7,1},{8,10},{10,12},{12... | collective-permute-start | bytes 1179656 | tf_op jit(solution)/shard_map/ppermute | solution.py:30
  113.0 1.4 collective-permute-start.7
  115.9 28.1 %collective-permute-start.8 = (bf16[96,2304]{1,0:T(8,128)(2,1)}, bf16[96,2304]{1,0:T(8,128)(2,1)S(1)}, u32[]{:S(2)}, u32[]{:S(2)}) collective-permute-start(bf16[96,2304]{1,0:T(8,128)(2,1)} %get-tuple-element.44), channel_id=1, source_target_pairs={{0,8},{8,16},{16,24},{24,0},{1,9},{9,17},{17,25},{25,1},{2,10},{10... | collective-permute-start | bytes 1327112 | tf_op jit(solution)/shard_map/ppermute | solution.py:30
  117.4 12.7 %collective-permute-start.24 = (bf16[96,2048]{1,0:T(8,128)(2,1)}, bf16[96,2048]{1,0:T(8,128)(2,1)}, u32[]{:S(2)}, u32[]{:S(2)}) collective-permute-start(bf16[96,2048]{1,0:T(8,128)(2,1)} %get-tuple-element.55), channel_id=1, source_target_pairs={{0,4},{2,6},{4,0},{6,2},{1,5},{3,7},{5,1},{7,3},{8,12},{10,14},{12... | collective-permute-start | bytes 1179656 | tf_op jit(solution)/shard_map/ppermute | solution.py:30
  118.5 19.5 %collective-permute-start.25 = (bf16[96,2048]{1,0:T(8,128)(2,1)}, bf16[96,2048]{1,0:T(8,128)(2,1)}, u32[]{:S(2)}, u32[]{:S(2)}) collective-permute-start(bf16[96,2048]{1,0:T(8,128)(2,1)} %get-tuple-element.56), channel_id=1, source_target_pairs={{0,6},{2,0},{4,2},{6,4},{1,7},{3,1},{5,3},{7,5},{8,14},{10,8},{12,... | collective-permute-start | bytes 1179656 | tf_op jit(solution)/shard_map/ppermute | solution.py:30
  120.2 24.4 %collective-permute-start.9 = (bf16[96,2304]{1,0:T(8,128)(2,1)}, bf16[96,2304]{1,0:T(8,128)(2,1)S(1)}, u32[]{:S(2)}, u32[]{:S(2)}) collective-permute-start(bf16[96,2304]{1,0:T(8,128)(2,1)} %get-tuple-element.45), channel_id=1, source_target_pairs={{0,16},{8,24},{16,0},{24,8},{1,17},{9,25},{17,1},{25,9},{2,18},{10... | collective-permute-start | bytes 1327112 | tf_op jit(solution)/shard_map/ppermute | solution.py:30
  122.9 0.8 copy-start.2
  123.7 21.0 %collective-permute-start.10 = (bf16[96,2304]{1,0:T(8,128)(2,1)}, bf16[96,2304]{1,0:T(8,128)(2,1)S(1)}, u32[]{:S(2)}, u32[]{:S(2)}) collective-permute-start(bf16[96,2304]{1,0:T(8,128)(2,1)} %get-tuple-element.46), channel_id=1, source_target_pairs={{0,24},{8,0},{16,8},{24,16},{1,25},{9,1},{17,9},{25,17},{2,26},{10... | collective-permute-start | bytes 1327112 | tf_op jit(solution)/shard_map/ppermute | solution.py:30
  138.0 1.0 copy-start.3
  140.3 16.1 %copy-start.4 = (f32[64,352]{1,0:T(8,128)S(1)}, f32[64,352]{1,0:T(8,128)}, u32[]{:S(2)}) copy-start(f32[64,352]{1,0:T(8,128)} %gate.1) | copy-start | bytes 270340
  140.4 16.1 %copy-start.5 = (f32[64,352]{1,0:T(8,128)S(1)}, f32[64,352]{1,0:T(8,128)}, u32[]{:S(2)}) copy-start(f32[64,352]{1,0:T(8,128)} %up.1) | copy-start | bytes 270340
  140.4 16.1 %copy-start.6 = (f32[352,64]{0,1:T(8,128)S(1)}, f32[352,64]{0,1:T(8,128)}, u32[]{:S(2)}) copy-start(f32[352,64]{0,1:T(8,128)} %param.17) | copy-start | bytes 270340
  140.4 8.5 %collective-permute-start.28 = (bf16[24,2048]{1,0:T(8,128)(2,1)S(1)}, bf16[24,2048]{1,0:T(8,128)(2,1)S(1)}, u32[]{:S(2)}, u32[]{:S(2)}) collective-permute-start(bf16[24,2048]{1,0:T(8,128)(2,1)S(1)} %get-tuple-element.60), channel_id=1, source_target_pairs={{0,24},{8,0},{16,8},{24,16},{1,25},{9,1},{17,9},{25,17},{2,26},{10... | collective-permute-start | bytes 294920 | tf_op jit(solution)/shard_map/ppermute | solution.py:30
  142.2 7.4 %collective-permute-start.27 = (bf16[24,2048]{1,0:T(8,128)(2,1)S(1)}, bf16[24,2048]{1,0:T(8,128)(2,1)S(1)}, u32[]{:S(2)}, u32[]{:S(2)}) collective-permute-start(bf16[24,2048]{1,0:T(8,128)(2,1)S(1)} %get-tuple-element.59), channel_id=1, source_target_pairs={{0,16},{8,24},{16,0},{24,8},{1,17},{9,25},{17,1},{25,9},{2,18},{10... | collective-permute-start | bytes 294920 | tf_op jit(solution)/shard_map/ppermute | solution.py:30
  144.0 5.8 %collective-permute-start.26 = (bf16[24,2048]{1,0:T(8,128)(2,1)S(1)}, bf16[24,2048]{1,0:T(8,128)(2,1)S(1)}, u32[]{:S(2)}, u32[]{:S(2)}) collective-permute-start(bf16[24,2048]{1,0:T(8,128)(2,1)S(1)} %get-tuple-element.58), channel_id=1, source_target_pairs={{0,8},{8,16},{16,24},{24,0},{1,9},{9,17},{17,25},{25,1},{2,10},{10... | collective-permute-start | bytes 294920 | tf_op jit(solution)/shard_map/ppermute | solution.py:30
  146.2 6.2 %collective-permute-start.13 = (bf16[24,2048]{1,0:T(8,128)(2,1)S(1)}, bf16[24,2048]{1,0:T(8,128)(2,1)S(1)}, u32[]{:S(2)}, u32[]{:S(2)}) collective-permute-start(bf16[24,2048]{1,0:T(8,128)(2,1)S(1)} %get-tuple-element.50), channel_id=1, source_target_pairs={{0,6},{2,0},{4,2},{6,4},{1,7},{3,1},{5,3},{7,5},{8,14},{10,8},{12,... | collective-permute-start | bytes 294920 | tf_op jit(solution)/shard_map/ppermute | solution.py:30
  148.8 6.2 %collective-permute-start.12 = (bf16[24,2048]{1,0:T(8,128)(2,1)S(1)}, bf16[24,2048]{1,0:T(8,128)(2,1)S(1)}, u32[]{:S(2)}, u32[]{:S(2)}) collective-permute-start(bf16[24,2048]{1,0:T(8,128)(2,1)S(1)} %get-tuple-element.49), channel_id=1, source_target_pairs={{0,4},{2,6},{4,0},{6,2},{1,5},{3,7},{5,1},{7,3},{8,12},{10,14},{12... | collective-permute-start | bytes 294920 | tf_op jit(solution)/shard_map/ppermute | solution.py:30
  148.9 6.9 %collective-permute-start.11 = (bf16[24,2048]{1,0:T(8,128)(2,1)S(1)}, bf16[24,2048]{1,0:T(8,128)(2,1)S(1)}, u32[]{:S(2)}, u32[]{:S(2)}) collective-permute-start(bf16[24,2048]{1,0:T(8,128)(2,1)S(1)} %get-tuple-element.48), channel_id=1, source_target_pairs={{0,2},{2,4},{4,6},{6,0},{1,3},{3,5},{5,7},{7,1},{8,10},{10,12},{12... | collective-permute-start | bytes 294920 | tf_op jit(solution)/shard_map/ppermute | solution.py:30

commit v6 on v5

--- a/solution.py
+++ b/solution.py
@@ -150,19 +150,19 @@
     grad_gate = grad_hidden * up_prev * sig * (1.0 + gate_prev * (1.0 - sig))
     grad_up = grad_hidden * silu
     hidden_prev = turned(silu * up_prev, ny, nx, rows)
-    grads[:, : 2 * pad] = turned(grad_gate, ny, nx, rows).astype(BF16)
-    grads[:, 2 * pad :] = turned(grad_up, ny, nx, rows).astype(BF16)
+    grads[:, : 2 * pad] = grad_gate.astype(BF16)
+    grads[:, 2 * pad :] = grad_up.astype(BF16)
     for k, (value, tokens) in enumerate(((grad_gate, prev), (grad_up, prev), (hidden_prev, cotangent))):
         term = dot(value.astype(BF16).T, tokens[...], ((1,), (0,)))
         kept[pl.ds(k * pad, pad)] = term[:pad]
         sent[pl.ds(k * pad, pad)] = term[pad:].astype(BF16)
 
 
-def input_kernel(grads, gate_up, *outs):
+def product_kernel(left, right, *outs):
     rows = outs[0].shape[0]
     for k, out in enumerate(outs):
         at = pl.ds(k * rows, rows)
-        out[...] = dot(grads[at, :], gate_up[...], ((1,), (0,))).astype(BF16)
+        out[...] = dot(left[at, :], right[...], ((1,), (0,))).astype(BF16)
 
 
 def sum_kernel(count, *refs):
@@ -205,11 +205,11 @@
     new_down_t[...] = down_t[...] + factor * jnp.concatenate(lows).T[:shard]
 
 
-def hidden_kernel(ny, nx, rows, pad, gate_up, *refs):
-    pieces, (mine, theirs, hidden, tokens, sems) = refs[:nx], refs[nx:]
+def hidden_kernel(pad, gate_up, *refs):
+    pieces, (mine, theirs, hidden, tokens, sems) = refs[:-5], refs[-5:]
     for move in fetched(pieces, tokens, sems):
         move.wait()
-    pre = turned(dot(tokens[...], gate_up[...], ((1,), (1,))), nx, ny, rows)
+    pre = dot(tokens[...], gate_up[...], ((1,), (1,)))
     value = jax.nn.silu(pre[:, : 2 * pad]) * pre[:, 2 * pad :]
     blank = jnp.zeros((value.shape[0], LANES - pad), F32)
     mine[...] = jnp.concatenate((value[:, :pad], blank), axis=1).astype(BF16)
@@ -217,37 +217,39 @@
     hidden[...] = value.astype(BF16)
 
 
-def output_kernel(hidden, down, mine, partner, *outs):
-    rows = outs[0].shape[0]
-    width = down.shape[1]
+def middle_kernel(nx, rows, mine, partner, *refs):
+    parts, outs = refs[:nx], refs[nx:]
+    ny, width = len(outs), parts[0].shape[1]
+    total = parts[0][...].astype(F32)
+    for part in parts[1:]:
+        total = total + part[...].astype(F32)
+    own, other = mine[...].astype(F32), partner[...].astype(F32)
     for k, out in enumerate(outs):
-        at = pl.ds(k * rows, rows)
-        out[:, :width] = dot(hidden[at, :], down[...], ((1,), (0,))).astype(BF16)
-        out[:, width : width + LANES] = mine[at, :]
-        out[:, width + LANES :] = partner[at, :]
-
-
-def arrival_kernel(nx, rows, part, place, *refs):
-    ny = len(refs) - nx - 3
-    parts, outs = refs[:ny], refs[ny : ny + nx]
-    saved, by_y, by_x = refs[ny + nx :]
-    width = outs[0].shape[1]
+        out[:, :width] = total[k * rows : (k + 1) * rows].astype(BF16)
+        for x in range(nx):
+            at, lane = (x * ny + k) * rows, width + 2 * LANES * x
+            out[:, lane : lane + LANES] = own[at : at + rows].astype(BF16)
+            out[:, lane + LANES : lane + 2 * LANES] = other[at : at + rows].astype(BF16)
+
+
+def arrival_kernel(nx, part, place, *refs):
+    parts, (output, saved, by_y, by_x) = refs[:-4], refs[-4:]
+    ny, (rows, width) = len(parts), output.shape
     total = parts[0][:, :width].astype(F32)
     for piece in parts[1:]:
         total = total + piece[:, :width].astype(F32)
-    for k, out in enumerate(outs):
-        out[...] = total[k * rows : (k + 1) * rows].astype(BF16)
+    output[...] = total.astype(BF16)
     x, y, core = place[0], place[1], place[2]
     for k in range(ny):
         by_y[k] = parts[k][:, width:].astype(F32)
     pieces = [by_y[lax.rem(y - s + ny, ny)] for s in range(ny)]
-    here = jnp.concatenate([piece[:, :part] for piece in pieces], axis=1)
-    there = jnp.concatenate([piece[:, LANES : LANES + part] for piece in pieces], axis=1)
-    low = jnp.where(core == 0, here, there)
-    high = jnp.where(core == 0, there, here)
     for k in range(nx):
-        by_x[k, :rows] = low[k * rows : (k + 1) * rows]
-        by_x[k, rows:] = high[k * rows : (k + 1) * rows]
+        lane = 2 * LANES * k
+        here = jnp.concatenate([piece[:, lane : lane + part] for piece in pieces], axis=1)
+        lane = lane + LANES
+        there = jnp.concatenate([piece[:, lane : lane + part] for piece in pieces], axis=1)
+        by_x[k, :rows] = jnp.where(core == 0, here, there)
+        by_x[k, rows:] = jnp.where(core == 0, there, here)
     ordered = [by_x[lax.rem(s - x + nx, nx)] for s in range(nx)]
     saved[...] = jnp.concatenate(ordered).astype(BF16)
 
@@ -301,8 +303,8 @@
     )
     received = swapped(sent)
     input_parts = whole(
-        input_kernel,
-        tuple(like((ny * rows, width), BF16) for _ in range(nx)),
+        product_kernel,
+        tuple(like((nx * rows, width), BF16) for _ in range(ny)),
         (grads, gate_up),
         flops=2 * token_ops,
     )
@@ -314,16 +316,16 @@
         (arrived, acc_gate, acc_up, acc_down.T),
     )
 
-    arrivals = for_owner(input_parts, "x")
-    by_x = whole(
-        functools.partial(sum_kernel, nx),
-        tuple(like((rows, width), BF16) for _ in range(ny)),
+    arrivals = for_owner(input_parts, "y")
+    by_y = whole(
+        functools.partial(sum_kernel, ny),
+        tuple(like((rows, width), BF16) for _ in range(nx)),
         arrivals,
     )
-    grad_input = added(for_owner(by_x, "y"))
+    grad_input = added(for_owner(by_y, "x"))
 
     mine, theirs, hidden = whole(
-        functools.partial(hidden_kernel, ny, nx, rows, pad),
+        functools.partial(hidden_kernel, pad),
         (like((group, LANES), BF16), like((group, LANES), BF16), like((group, 2 * pad), BF16)),
         (gate_up, *nexts),
         (pltpu.VMEM((group, width), BF16), pltpu.SemaphoreType.DMA((nx,))),
@@ -332,27 +334,29 @@
     )
     partner = swapped(theirs)
     out_parts = whole(
-        output_kernel,
-        tuple(like((nx * rows, width + 2 * LANES), BF16) for _ in range(ny)),
-        (hidden, down, mine, partner),
+        product_kernel,
+        tuple(like((ny * rows, width), BF16) for _ in range(nx)),
+        (hidden, down),
         flops=token_ops,
     )
-    arrivals = for_owner(out_parts, "y")
+    arrivals = for_owner(out_parts, "x")
+    by_x = whole(
+        functools.partial(middle_kernel, nx, rows),
+        tuple(like((rows, width + 2 * nx * LANES), BF16) for _ in range(ny)),
+        (mine, partner, *arrivals),
+    )
+    arrivals = for_owner(by_x, "y")
     place = jnp.stack([lax.axis_index(name) for name in ("x", "y", "c")]).astype(jnp.int32)
-    *by_y, saved = whole(
-        functools.partial(arrival_kernel, nx, rows, part),
-        (
-            *(like((rows, width), BF16) for _ in range(nx)),
-            like((nx * nc * rows, units), BF16),
-        ),
+    out_next, saved = whole(
+        functools.partial(arrival_kernel, nx, part),
+        (like((rows, width), BF16), like((nx * nc * rows, units), BF16)),
         (place, *arrivals),
         (
-            pltpu.VMEM((ny, nx * rows, 2 * LANES), F32),
+            pltpu.VMEM((ny, rows, 2 * nx * LANES), F32),
             pltpu.VMEM((nx, nc * rows, units), F32),
         ),
         spaces=[pltpu.SMEM] + [pltpu.VMEM] * ny,
     )
-    out_next = added(for_owner(by_y, "x"))
     return out_next, saved, grad_input, new_gate, new_up, new_down_t.T
 
 

time: 158 us -> 153 us (0.968)
  waiting for transfers between devices: 66 us -> 54.9 us
  starting transfers between devices: 66.3 us -> 68.4 us
  local copies, waits for them, and re-layouts: 3.54 us -> 5.29 us
    ppermute x27, waiting for transfers between devices: 61.9 us -> 52.1 us  [moved(): lax.ppermute(array, axis, [(i, (i + step) % length) for i in range(length)])]
    ppermute x27, starting transfers between devices: 47.2 us -> 49.4 us  [moved(): lax.ppermute(array, axis, [(i, (i + step) % length) for i in range(length)])]
    unnamed x22 -> x30, local copies, waits for them, and re-layouts: 3.47 us -> 5.22 us
    pallas_call x10 -> x11, Pallas kernels: 17.7 us -> 19.1 us  [whole(): pl.pallas_call(kernel, out_shape=out_shape, in_specs=[pl.BlockSpec(memory...]
  transfers between devices with their start and end apart: 32 -> 32, of which waited for: 16 -> 13; matrix products, arithmetic and copies ran while one was open for 2% -> 2% of each run, Pallas kernels for 5% -> 7%
where the time goes in v6:
time: 153 us; the launch traced here: 151 us
  starting transfers between devices  68.4 us (45%)
  waiting for transfers between devices  54.9 us (36%)
  Pallas kernels  19.1 us (12%)
  local copies, waits for them, and re-layouts  5.29 us (3%)
  other arithmetic  2.32 us (2%)
    ppermute x27, waiting for transfers between devices, moved(): lax.ppermute(array, axis, [(i, (i + step) % length) for i in range(length)])  52.1 us
    ppermute x27, starting transfers between devices, moved(): lax.ppermute(array, axis, [(i, (i + step) % length) for i in range(length)])  49.4 us
    pallas_call x11, Pallas kernels, whole(): pl.pallas_call(kernel, out_shape=out_shape, in_specs=[pl.BlockSpec(memory...  19.1 us
    all_to_all x2, starting transfers between devices, spread(): return lax.all_to_all(blocks, axis, 0, 0, tiled=True)  18.9 us
    unnamed x30, local copies, waits for them, and re-layouts  5.22 us
  transfers between devices with their start and end apart: 32, of which 13 were waited for; matrix products, arithmetic and copies ran while one was open for 2% of the time, Pallas kernels for 7%

profile of v6, /device:TPU:64, one launch (start us, length us, event | category | flops | bytes accessed | tf_op | source)
XLA Modules:
  0.0 150.9 jit_solution(18397680053854559708)
XLA Ops:
  0.6 2.3 %shard_map.136 = (bf16[24,4096]{1,0:T(8,128)(2,1)}, bf16[32,136,128]{2,1,0:T(8,128)(2,1)}) custom-call(bf16[24,2048]{1,0:T(8,128)(2,1)} %refs_0_.1, bf16[24,2048]{1,0:T(8,128)(2,1)} %refs_1_.1, bf16[64,352]{1,0:T(8,128)(2,1)} %refs_2_.1, bf16[64,352]{1,0:T(8,128)(2,1)} %refs_3_.1, bf16[64,352]{1,0:T(8,128)(2,1)} %bitcast.30), custom_call_target="tpu_custom_call" | custom-call | tf_op jit(solution)/shard_map/pallas_call | solution.py:59
  3.0 11.1 %all-to-all-start = ((bf16[32,136,128]{2,1,0:T(8,128)(2,1)}), bf16[32,136,128]{2,1,0:T(8,128)(2,1)S(1)}, u32[]{:S(2)}, u32[]{:S(2)}) async-start(bf16[32,136,128]{2,1,0:T(8,128)(2,1)} %get-tuple-element.37), calls=%async_computation | async-start | bytes 2228224 | tf_op jit(solution)/shard_map/all_to_all | solution.py:21
  14.0 1.6 %collective-permute-start.16 = (bf16[24,2048]{1,0:T(8,128)(2,1)S(1)}, bf16[24,2048]{1,0:T(8,128)(2,1)S(1)}, u32[]{:S(2)}, u32[]{:S(2)}) collective-permute-start(bf16[24,2048]{1,0:T(8,128)(2,1)S(1)} %copy-done.14), channel_id=1, source_target_pairs={{0,2},{2,4},{4,6},{6,0},{1,3},{3,5},{5,7},{7,1},{8,10},{10,12},{12... | collective-permute-start | bytes 294920 | tf_op jit(solution)/shard_map/ppermute | solution.py:30
  15.6 2.7 %collective-permute-start.15 = (bf16[24,2048]{1,0:T(8,128)(2,1)S(1)}, bf16[24,2048]{1,0:T(8,128)(2,1)S(1)}, u32[]{:S(2)}, u32[]{:S(2)}) collective-permute-start(bf16[24,2048]{1,0:T(8,128)(2,1)S(1)} %copy-done.14), channel_id=1, source_target_pairs={{0,4},{2,6},{4,0},{6,2},{1,5},{3,7},{5,1},{7,3},{8,12},{10,14},{12... | collective-permute-start | bytes 294920 | tf_op jit(solution)/shard_map/ppermute | solution.py:30
  18.3 1.4 collective-permute-start.14
  19.8 1.5 collective-permute-start.3
  21.2 2.7 %collective-permute-start.2 = (bf16[24,4096]{1,0:T(8,128)(2,1)S(1)}, bf16[24,4096]{1,0:T(8,128)(2,1)S(1)}, u32[]{:S(2)}, u32[]{:S(2)}) collective-permute-start(bf16[24,4096]{1,0:T(8,128)(2,1)S(1)} %copy-done.13), channel_id=1, source_target_pairs={{0,16},{8,24},{16,0},{24,8},{1,17},{9,25},{17,1},{25,9},{2,18},{10... | collective-permute-start | bytes 589832 | tf_op jit(solution)/shard_map/ppermute | solution.py:30
  23.9 1.5 collective-permute-start.1
  26.1 1.1 collective-permute-start.18
  27.2 11.3 %collective-permute-done.3 = bf16[24,4096]{1,0:T(8,128)(2,1)S(1)} collective-permute-done((bf16[24,4096]{1,0:T(8,128)(2,1)S(1)}, bf16[24,4096]{1,0:T(8,128)(2,1)S(1)}, u32[]{:S(2)}, u32[]{:S(2)}) %collective-permute-start.3) | collective-permute-done | bytes 196640 | tf_op jit(solution)/shard_map/ppermute | solution.py:30
  38.5 2.7 %collective-permute-done.2 = bf16[24,4096]{1,0:T(8,128)(2,1)S(1)} collective-permute-done((bf16[24,4096]{1,0:T(8,128)(2,1)S(1)}, bf16[24,4096]{1,0:T(8,128)(2,1)S(1)}, u32[]{:S(2)}, u32[]{:S(2)}) %collective-permute-start.2) | collective-permute-done | bytes 196640 | tf_op jit(solution)/shard_map/ppermute | solution.py:30
  41.2 2.9 %collective-permute-done.1 = bf16[24,4096]{1,0:T(8,128)(2,1)S(1)} collective-permute-done((bf16[24,4096]{1,0:T(8,128)(2,1)S(1)}, bf16[24,4096]{1,0:T(8,128)(2,1)S(1)}, u32[]{:S(2)}, u32[]{:S(2)}) %collective-permute-start.1) | collective-permute-done | bytes 196640 | tf_op jit(solution)/shard_map/ppermute | solution.py:30
  45.2 4.3 %collective-permute-done.19 = bf16[96,2048]{1,0:T(8,128)(2,1)S(1)} collective-permute-done((bf16[96,2048]{1,0:T(8,128)(2,1)S(1)}, bf16[96,2048]{1,0:T(8,128)(2,1)S(1)}, u32[]{:S(2)}, u32[]{:S(2)}) %collective-permute-start.19) | collective-permute-done | bytes 393248 | tf_op jit(solution)/shard_map/ppermute | solution.py:30
  49.5 8.7 %collective-permute-start.21 = (bf16[96,2048]{1,0:T(8,128)(2,1)S(1)}, bf16[96,2048]{1,0:T(8,128)(2,1)S(1)}, u32[]{:S(2)}, u32[]{:S(2)}) collective-permute-start(bf16[96,2048]{1,0:T(8,128)(2,1)S(1)} %get-tuple-element.68), channel_id=1, source_target_pairs={{0,4},{2,6},{4,0},{6,2},{1,5},{3,7},{5,1},{7,3},{8,12},{10,14},{12... | collective-permute-start | bytes 1179656 | tf_op jit(solution)/shard_map/ppermute | solution.py:30
  58.2 2.1 %collective-permute-start.20 = (bf16[96,2048]{1,0:T(8,128)(2,1)S(1)}, bf16[96,2048]{1,0:T(8,128)(2,1)S(1)}, u32[]{:S(2)}, u32[]{:S(2)}) collective-permute-start(bf16[96,2048]{1,0:T(8,128)(2,1)S(1)} %get-tuple-element.68), channel_id=1, source_target_pairs={{0,6},{2,0},{4,2},{6,4},{1,7},{3,1},{5,3},{7,5},{8,14},{10,8},{12,... | collective-permute-start | bytes 1179656 | tf_op jit(solution)/shard_map/ppermute | solution.py:30
  60.3 1.2 pad_maximum_fusion.prev
  61.5 4.3 %collective-permute-done.21 = bf16[96,2048]{1,0:T(8,128)(2,1)S(1)} collective-permute-done((bf16[96,2048]{1,0:T(8,128)(2,1)S(1)}, bf16[96,2048]{1,0:T(8,128)(2,1)S(1)}, u32[]{:S(2)}, u32[]{:S(2)}) %collective-permute-start.21) | collective-permute-done | bytes 393248 | tf_op jit(solution)/shard_map/ppermute | solution.py:30
  65.9 4.1 %collective-permute-done.20 = bf16[96,2048]{1,0:T(8,128)(2,1)S(1)} collective-permute-done((bf16[96,2048]{1,0:T(8,128)(2,1)S(1)}, bf16[96,2048]{1,0:T(8,128)(2,1)S(1)}, u32[]{:S(2)}, u32[]{:S(2)}) %collective-permute-start.20) | collective-permute-done | bytes 393248 | tf_op jit(solution)/shard_map/ppermute | solution.py:30
  70.2 0.9 shard_map.137
  71.1 3.6 %shard_map.142 = (f32[288,2048]{1,0:T(8,128)S(1)}, bf16[288,2048]{1,0:T(8,128)(2,1)S(1)}, bf16[384,384]{1,0:T(8,128)(2,1)S(1)}) custom-call(bf16[384,2048]{1,0:T(8,128)(2,1)S(1)} %get-tuple-element.38.gate_up.right, bf16[192,2048]{1,0:T(8,128)(2,1)S(1)} %get-tuple-element.43.right.down, bf16[384,2048]{1,0:T(8,128)(2,1)S(1)} %pad_maximum_fusion.prev, ...), custom_call_target="tpu_custom_call" | custom-call | flops 1811939328 | tf_op jit(solution)/shard_map/pallas_call | solution.py:59
  75.5 2.8 %collective-permute-done.29.received = bf16[288,2048]{1,0:T(8,128)(2,1)S(1)} collective-permute-done((bf16[288,2048]{1,0:T(8,128)(2,1)S(1)}, bf16[288,2048]{1,0:T(8,128)(2,1)S(1)}, u32[]{:S(2)}, u32[]{:S(2)}) %collective-permute-start.29) | collective-permute-done | bytes 1179680 | tf_op jit(solution)/shard_map/ppermute | solution.py:25
  78.4 1.5 %shard_map.145 = bf16[32,136,128]{2,1,0:T(8,128)(2,1)} custom-call(f32[288,2048]{1,0:T(8,128)S(1)} %get-tuple-element.63.kept, bf16[288,2048]{1,0:T(8,128)(2,1)S(1)} %collective-permute-done.29.received), custom_call_target="tpu_custom_call" | custom-call | tf_op jit(solution)/shard_map/pallas_call | solution.py:59
  79.9 7.9 %all-to-all-start.1 = ((bf16[32,136,128]{2,1,0:T(8,128)(2,1)}), bf16[32,136,128]{2,1,0:T(8,128)(2,1)S(1)}, u32[]{:S(2)}, u32[]{:S(2)}) async-start(bf16[32,136,128]{2,1,0:T(8,128)(2,1)} %shard_map.145), calls=%async_computation.1 | async-start | bytes 2228224 | tf_op jit(solution)/shard_map/all_to_all | solution.py:21
  87.8 2.9 %collective-permute-start.4 = (bf16[96,2048]{1,0:T(8,128)(2,1)S(1)}, bf16[96,2048]{1,0:T(8,128)(2,1)S(1)}, u32[]{:S(2)}, u32[]{:S(2)}) collective-permute-start(bf16[96,2048]{1,0:T(8,128)(2,1)S(1)} %get-tuple-element.69.refs_0_), channel_id=1, source_target_pairs={{0,6},{2,0},{4,2},{6,4},{1,7},{3,1},{5,3},{7,5},{8,14},{10,8},{12,... | collective-permute-start | bytes 1179656 | tf_op jit(solution)/shard_map/ppermute | solution.py:30
  90.7 0.9 collective-permute-start.6
  91.7 1.0 copy-done.12
  92.6 2.1 %shard_map.143 = (bf16[96,2048]{1,0:T(8,128)(2,1)S(1)}, bf16[96,2048]{1,0:T(8,128)(2,1)S(1)}, bf16[96,2048]{1,0:T(8,128)(2,1)S(1)}, bf16[96,2048]{1,0:T(8,128)(2,1)}) custom-call(bf16[384,384]{1,0:T(8,128)(2,1)S(1)} %copy-done.12, bf16[384,2048]{1,0:T(8,128)(2,1)S(1)} %get-tuple-element.38.gate_up.right), custom_call_target="tpu_custom_call" | custom-call | flops 603979776 | tf_op jit(solution)/shard_map/pallas_call | solution.py:59
  94.7 1.5 collective-permute-start.23
  96.1 2.7 %collective-permute-start.24 = (bf16[96,2048]{1,0:T(8,128)(2,1)S(1)}, bf16[96,2048]{1,0:T(8,128)(2,1)S(1)}, u32[]{:S(2)}, u32[]{:S(2)}) collective-permute-start(bf16[96,2048]{1,0:T(8,128)(2,1)S(1)} %get-tuple-element.57), channel_id=1, source_target_pairs={{0,16},{8,24},{16,0},{24,8},{1,17},{9,25},{17,1},{25,9},{2,18},{10... | collective-permute-start | bytes 1179656 | tf_op jit(solution)/shard_map/ppermute | solution.py:30
  98.8 8.4 %collective-permute-done.4.refs_1_ = bf16[96,2048]{1,0:T(8,128)(2,1)S(1)} collective-permute-done((bf16[96,2048]{1,0:T(8,128)(2,1)S(1)}, bf16[96,2048]{1,0:T(8,128)(2,1)S(1)}, u32[]{:S(2)}, u32[]{:S(2)}) %collective-permute-start.4) | collective-permute-done | bytes 393248 | tf_op jit(solution)/shard_map/ppermute | solution.py:30
  107.2 2.7 %collective-permute-start.25 = (bf16[96,2048]{1,0:T(8,128)(2,1)}, bf16[96,2048]{1,0:T(8,128)(2,1)}, u32[]{:S(2)}, u32[]{:S(2)}) collective-permute-start(bf16[96,2048]{1,0:T(8,128)(2,1)} %get-tuple-element.58), channel_id=1, source_target_pairs={{0,24},{8,0},{16,8},{24,16},{1,25},{9,1},{17,9},{25,17},{2,26},{10... | collective-permute-start | bytes 1179656 | tf_op jit(solution)/shard_map/ppermute | solution.py:30
  110.7 2.6 %shard_map.138 = (bf16[384,128]{1,0:T(8,128)(2,1)S(1)}, bf16[384,128]{1,0:T(8,128)(2,1)}, bf16[384,192]{1,0:T(8,128)(2,1)S(1)}) custom-call(bf16[384,2048]{1,0:T(8,128)(2,1)S(1)} %get-tuple-element.38.gate_up.right, bf16[96,2048]{1,0:T(8,128)(2,1)S(1)} %get-tuple-element.69.refs_0_, bf16[96,2048]{1,0:T(8,128)(2,1)S(1)} %collective-permute-done.4.refs_1_, ...), custom_call_target="tpu_custom_call" | custom-call | flops 603979776 | tf_op jit(solution)/shard_map/pallas_call | solution.py:59
  113.3 1.4 shard_map.139
  114.7 4.4 %collective-permute-start.9 = (bf16[96,2048]{1,0:T(8,128)(2,1)}, bf16[96,2048]{1,0:T(8,128)(2,1)S(1)}, u32[]{:S(2)}, u32[]{:S(2)}) collective-permute-start(bf16[96,2048]{1,0:T(8,128)(2,1)} %get-tuple-element.46), channel_id=1, source_target_pairs={{0,4},{2,6},{4,0},{6,2},{1,5},{3,7},{5,1},{7,3},{8,12},{10,14},{12... | collective-permute-start | bytes 1179656 | tf_op jit(solution)/shard_map/ppermute | solution.py:30
  119.8 3.3 %collective-permute-done.24.refs_2_ = bf16[96,2048]{1,0:T(8,128)(2,1)S(1)} collective-permute-done((bf16[96,2048]{1,0:T(8,128)(2,1)S(1)}, bf16[96,2048]{1,0:T(8,128)(2,1)S(1)}, u32[]{:S(2)}, u32[]{:S(2)}) %collective-permute-start.24) | collective-permute-done | bytes 393248 | tf_op jit(solution)/shard_map/ppermute | solution.py:30
  123.9 1.0 copy-done.1
  124.9 1.0 copy-done.3
  125.9 1.2 shard_map.144
  127.2 2.6 %collective-permute-start.28 = (bf16[24,2048]{1,0:T(8,128)(2,1)S(1)}, bf16[24,2048]{1,0:T(8,128)(2,1)S(1)}, u32[]{:S(2)}, u32[]{:S(2)}) collective-permute-start(bf16[24,2048]{1,0:T(8,128)(2,1)S(1)} %get-tuple-element.62), channel_id=1, source_target_pairs={{0,6},{2,0},{4,2},{6,4},{1,7},{3,1},{5,3},{7,5},{8,14},{10,8},{12,... | collective-permute-start | bytes 294920 | tf_op jit(solution)/shard_map/ppermute | solution.py:30
  129.8 1.3 collective-permute-start.27
  131.1 6.2 %collective-permute-done.8.refs_1_ = bf16[96,2048]{1,0:T(8,128)(2,1)S(1)} collective-permute-done((bf16[96,2048]{1,0:T(8,128)(2,1)}, bf16[96,2048]{1,0:T(8,128)(2,1)S(1)}, u32[]{:S(2)}, u32[]{:S(2)}) %collective-permute-start.8) | collective-permute-done | bytes 393248 | tf_op jit(solution)/shard_map/ppermute | solution.py:30
  137.5 1.1 shard_map.140
  138.6 1.5 %collective-permute-start.11 = (bf16[24,3072]{1,0:T(8,128)(2,1)S(1)}, bf16[24,3072]{1,0:T(8,128)(2,1)S(1)}, u32[]{:S(2)}, u32[]{:S(2)}) collective-permute-start(bf16[24,3072]{1,0:T(8,128)(2,1)S(1)} %get-tuple-element.49), channel_id=1, source_target_pairs={{0,8},{8,16},{16,24},{24,0},{1,9},{9,17},{17,25},{25,1},{2,10},{10... | collective-permute-start | bytes 442376 | tf_op jit(solution)/shard_map/ppermute | solution.py:30
  140.1 2.7 %collective-permute-start.12 = (bf16[24,3072]{1,0:T(8,128)(2,1)S(1)}, bf16[24,3072]{1,0:T(8,128)(2,1)S(1)}, u32[]{:S(2)}, u32[]{:S(2)}) collective-permute-start(bf16[24,3072]{1,0:T(8,128)(2,1)S(1)} %get-tuple-element.50), channel_id=1, source_target_pairs={{0,16},{8,24},{16,0},{24,8},{1,17},{9,25},{17,1},{25,9},{2,18},{10... | collective-permute-start | bytes 442376 | tf_op jit(solution)/shard_map/ppermute | solution.py:30
  142.8 1.5 collective-permute-start.13
  144.9 1.6 %collective-permute-done.11.refs_1_ = bf16[24,3072]{1,0:T(8,128)(2,1)S(1)} collective-permute-done((bf16[24,3072]{1,0:T(8,128)(2,1)S(1)}, bf16[24,3072]{1,0:T(8,128)(2,1)S(1)}, u32[]{:S(2)}, u32[]{:S(2)}) %collective-permute-start.11) | collective-permute-done | bytes 147488 | tf_op jit(solution)/shard_map/ppermute | solution.py:30
  146.6 2.0 %collective-permute-done.12.refs_2_ = bf16[24,3072]{1,0:T(8,128)(2,1)S(1)} collective-permute-done((bf16[24,3072]{1,0:T(8,128)(2,1)S(1)}, bf16[24,3072]{1,0:T(8,128)(2,1)S(1)}, u32[]{:S(2)}, u32[]{:S(2)}) %collective-permute-start.12) | collective-permute-done | bytes 147488 | tf_op jit(solution)/shard_map/ppermute | solution.py:30
  148.5 1.5 shard_map.141
  (64 shorter events, 6.6 us)
Async XLA Ops:
  0.6 13.4 %copy-start.14 = (bf16[24,2048]{1,0:T(8,128)(2,1)S(1)}, bf16[24,2048]{1,0:T(8,128)(2,1)}, u32[]{:S(2)}) copy-start(bf16[24,2048]{1,0:T(8,128)(2,1)} %param.10) | copy-start | bytes 294916
  2.9 16.8 %copy-start.13 = (bf16[24,4096]{1,0:T(8,128)(2,1)S(1)}, bf16[24,4096]{1,0:T(8,128)(2,1)}, u32[]{:S(2)}) copy-start(bf16[24,4096]{1,0:T(8,128)(2,1)} %get-tuple-element.39) | copy-start | bytes 589828
  3.0 41.3 %all-to-all-start = ((bf16[32,136,128]{2,1,0:T(8,128)(2,1)}), bf16[32,136,128]{2,1,0:T(8,128)(2,1)S(1)}, u32[]{:S(2)}, u32[]{:S(2)}) async-start(bf16[32,136,128]{2,1,0:T(8,128)(2,1)} %get-tuple-element.37), calls=%async_computation | async-start | bytes 2228224 | tf_op jit(solution)/shard_map/all_to_all | solution.py:21
  14.0 9.9 %collective-permute-start.16 = (bf16[24,2048]{1,0:T(8,128)(2,1)S(1)}, bf16[24,2048]{1,0:T(8,128)(2,1)S(1)}, u32[]{:S(2)}, u32[]{:S(2)}) collective-permute-start(bf16[24,2048]{1,0:T(8,128)(2,1)S(1)} %copy-done.14), channel_id=1, source_target_pairs={{0,2},{2,4},{4,6},{6,0},{1,3},{3,5},{5,7},{7,1},{8,10},{10,12},{12... | collective-permute-start | bytes 294920 | tf_op jit(solution)/shard_map/ppermute | solution.py:30
  15.6 9.8 %collective-permute-start.15 = (bf16[24,2048]{1,0:T(8,128)(2,1)S(1)}, bf16[24,2048]{1,0:T(8,128)(2,1)S(1)}, u32[]{:S(2)}, u32[]{:S(2)}) collective-permute-start(bf16[24,2048]{1,0:T(8,128)(2,1)S(1)} %copy-done.14), channel_id=1, source_target_pairs={{0,4},{2,6},{4,0},{6,2},{1,5},{3,7},{5,1},{7,3},{8,12},{10,14},{12... | collective-permute-start | bytes 294920 | tf_op jit(solution)/shard_map/ppermute | solution.py:30
  18.3 7.0 %collective-permute-start.14 = (bf16[24,2048]{1,0:T(8,128)(2,1)S(1)}, bf16[24,2048]{1,0:T(8,128)(2,1)S(1)}, u32[]{:S(2)}, u32[]{:S(2)}) collective-permute-start(bf16[24,2048]{1,0:T(8,128)(2,1)S(1)} %copy-done.14), channel_id=1, source_target_pairs={{0,6},{2,0},{4,2},{6,4},{1,7},{3,1},{5,3},{7,5},{8,14},{10,8},{12,... | collective-permute-start | bytes 294920 | tf_op jit(solution)/shard_map/ppermute | solution.py:30
  19.8 18.8 %collective-permute-start.3 = (bf16[24,4096]{1,0:T(8,128)(2,1)S(1)}, bf16[24,4096]{1,0:T(8,128)(2,1)S(1)}, u32[]{:S(2)}, u32[]{:S(2)}) collective-permute-start(bf16[24,4096]{1,0:T(8,128)(2,1)S(1)} %copy-done.13), channel_id=1, source_target_pairs={{0,8},{8,16},{16,24},{24,0},{1,9},{9,17},{17,25},{25,1},{2,10},{10... | collective-permute-start | bytes 589832 | tf_op jit(solution)/shard_map/ppermute | solution.py:30
  21.2 20.0 %collective-permute-start.2 = (bf16[24,4096]{1,0:T(8,128)(2,1)S(1)}, bf16[24,4096]{1,0:T(8,128)(2,1)S(1)}, u32[]{:S(2)}, u32[]{:S(2)}) collective-permute-start(bf16[24,4096]{1,0:T(8,128)(2,1)S(1)} %copy-done.13), channel_id=1, source_target_pairs={{0,16},{8,24},{16,0},{24,8},{1,17},{9,25},{17,1},{25,9},{2,18},{10... | collective-permute-start | bytes 589832 | tf_op jit(solution)/shard_map/ppermute | solution.py:30
  23.9 20.3 %collective-permute-start.1 = (bf16[24,4096]{1,0:T(8,128)(2,1)S(1)}, bf16[24,4096]{1,0:T(8,128)(2,1)S(1)}, u32[]{:S(2)}, u32[]{:S(2)}) collective-permute-start(bf16[24,4096]{1,0:T(8,128)(2,1)S(1)} %copy-done.13), channel_id=1, source_target_pairs={{0,24},{8,0},{16,8},{24,16},{1,25},{9,1},{17,9},{25,17},{2,26},{10... | collective-permute-start | bytes 589832 | tf_op jit(solution)/shard_map/ppermute | solution.py:30
  25.4 24.1 %collective-permute-start.19 = (bf16[96,2048]{1,0:T(8,128)(2,1)S(1)}, bf16[96,2048]{1,0:T(8,128)(2,1)S(1)}, u32[]{:S(2)}, u32[]{:S(2)}) collective-permute-start(bf16[96,2048]{1,0:T(8,128)(2,1)S(1)} %bitcast.18), channel_id=1, source_target_pairs={{0,8},{8,16},{16,24},{24,0},{1,9},{9,17},{17,25},{25,1},{2,10},{10... | collective-permute-start | bytes 1179656 | tf_op jit(solution)/shard_map/ppermute | solution.py:30
  26.1 32.1 %collective-permute-start.18 = (bf16[96,2048]{1,0:T(8,128)(2,1)S(1)}, bf16[96,2048]{1,0:T(8,128)(2,1)}, u32[]{:S(2)}, u32[]{:S(2)}) collective-permute-start(bf16[96,2048]{1,0:T(8,128)(2,1)S(1)} %bitcast.19), channel_id=1, source_target_pairs={{0,16},{8,24},{16,0},{24,8},{1,17},{9,25},{17,1},{25,9},{2,18},{10... | collective-permute-start | bytes 1179656 | tf_op jit(solution)/shard_map/ppermute | solution.py:30
  38.5 21.8 %collective-permute-start.17 = (bf16[96,2048]{1,0:T(8,128)(2,1)S(1)}, bf16[96,2048]{1,0:T(8,128)(2,1)}, u32[]{:S(2)}, u32[]{:S(2)}) collective-permute-start(bf16[96,2048]{1,0:T(8,128)(2,1)S(1)} %bitcast.20), channel_id=1, source_target_pairs={{0,24},{8,0},{16,8},{24,16},{1,25},{9,1},{17,9},{25,17},{2,26},{10... | collective-permute-start | bytes 1179656 | tf_op jit(solution)/shard_map/ppermute | solution.py:30
  44.3 25.9 %collective-permute-start = (bf16[32,136,128]{2,1,0:T(8,128)(2,1)S(1)}, bf16[32,136,128]{2,1,0:T(8,128)(2,1)S(1)}, u32[]{:S(2)}, u32[]{:S(2)}) collective-permute-start(bf16[32,136,128]{2,1,0:T(8,128)(2,1)S(1)} %all-to-all-done.own), channel_id=1, source_target_pairs={{0,1},{1,0},{2,3},{3,2},{4,5},{5,4},{6,7},{7,6},{8,9},{9,8},{10,11... | collective-permute-start | bytes 3342344 | tf_op jit(solution)/shard_map/ppermute | solution.py:25
  44.5 17.1 %collective-permute-start.22 = (bf16[96,2048]{1,0:T(8,128)(2,1)S(1)}, bf16[96,2048]{1,0:T(8,128)(2,1)S(1)}, u32[]{:S(2)}, u32[]{:S(2)}) collective-permute-start(bf16[96,2048]{1,0:T(8,128)(2,1)S(1)} %get-tuple-element.68), channel_id=1, source_target_pairs={{0,2},{2,4},{4,6},{6,0},{1,3},{3,5},{5,7},{7,1},{8,10},{10,12},{12... | collective-permute-start | bytes 1179656 | tf_op jit(solution)/shard_map/ppermute | solution.py:30
  49.5 16.4 %collective-permute-start.21 = (bf16[96,2048]{1,0:T(8,128)(2,1)S(1)}, bf16[96,2048]{1,0:T(8,128)(2,1)S(1)}, u32[]{:S(2)}, u32[]{:S(2)}) collective-permute-start(bf16[96,2048]{1,0:T(8,128)(2,1)S(1)} %get-tuple-element.68), channel_id=1, source_target_pairs={{0,4},{2,6},{4,0},{6,2},{1,5},{3,7},{5,1},{7,3},{8,12},{10,14},{12... | collective-permute-start | bytes 1179656 | tf_op jit(solution)/shard_map/ppermute | solution.py:30
  58.2 11.8 %collective-permute-start.20 = (bf16[96,2048]{1,0:T(8,128)(2,1)S(1)}, bf16[96,2048]{1,0:T(8,128)(2,1)S(1)}, u32[]{:S(2)}, u32[]{:S(2)}) collective-permute-start(bf16[96,2048]{1,0:T(8,128)(2,1)S(1)} %get-tuple-element.68), channel_id=1, source_target_pairs={{0,6},{2,0},{4,2},{6,4},{1,7},{3,1},{5,3},{7,5},{8,14},{10,8},{12,... | collective-permute-start | bytes 1179656 | tf_op jit(solution)/shard_map/ppermute | solution.py:30
  71.1 3.6 %copy-start.9 = (bf16[192,2048]{1,0:T(8,128)(2,1)}, bf16[192,2048]{1,0:T(8,128)(2,1)S(1)}, u32[]{:S(2)}) copy-start(bf16[192,2048]{1,0:T(8,128)(2,1)S(1)} %get-tuple-element.43.right.down) | copy-start | bytes 2359300
  74.8 0.7 copy-start.11
  75.5 2.8 %collective-permute-start.29 = (bf16[288,2048]{1,0:T(8,128)(2,1)S(1)}, bf16[288,2048]{1,0:T(8,128)(2,1)S(1)}, u32[]{:S(2)}, u32[]{:S(2)}) collective-permute-start(bf16[288,2048]{1,0:T(8,128)(2,1)S(1)} %get-tuple-element.64), channel_id=1, source_target_pairs={{0,1},{1,0},{2,3},{3,2},{4,5},{5,4},{6,7},{7,6},{8,9},{9,8},{10,11... | collective-permute-start | bytes 3538952 | tf_op jit(solution)/shard_map/ppermute | solution.py:25
  79.9 70.1 %all-to-all-start.1 = ((bf16[32,136,128]{2,1,0:T(8,128)(2,1)}), bf16[32,136,128]{2,1,0:T(8,128)(2,1)S(1)}, u32[]{:S(2)}, u32[]{:S(2)}) async-start(bf16[32,136,128]{2,1,0:T(8,128)(2,1)} %shard_map.145), calls=%async_computation.1 | async-start | bytes 2228224 | tf_op jit(solution)/shard_map/all_to_all | solution.py:21
  87.8 19.5 %collective-permute-start.4 = (bf16[96,2048]{1,0:T(8,128)(2,1)S(1)}, bf16[96,2048]{1,0:T(8,128)(2,1)S(1)}, u32[]{:S(2)}, u32[]{:S(2)}) collective-permute-start(bf16[96,2048]{1,0:T(8,128)(2,1)S(1)} %get-tuple-element.69.refs_0_), channel_id=1, source_target_pairs={{0,6},{2,0},{4,2},{6,4},{1,7},{3,1},{5,3},{7,5},{8,14},{10,8},{12,... | collective-permute-start | bytes 1179656 | tf_op jit(solution)/shard_map/ppermute | solution.py:30
  90.7 19.2 %collective-permute-start.5 = (bf16[96,2048]{1,0:T(8,128)(2,1)S(1)}, bf16[96,2048]{1,0:T(8,128)(2,1)S(1)}, u32[]{:S(2)}, u32[]{:S(2)}) collective-permute-start(bf16[96,2048]{1,0:T(8,128)(2,1)S(1)} %get-tuple-element.69.refs_0_), channel_id=1, source_target_pairs={{0,4},{2,6},{4,0},{6,2},{1,5},{3,7},{5,1},{7,3},{8,12},{10,14},{12... | collective-permute-start | bytes 1179656 | tf_op jit(solution)/shard_map/ppermute | solution.py:30
  90.7 19.9 %collective-permute-start.6 = (bf16[96,2048]{1,0:T(8,128)(2,1)S(1)}, bf16[96,2048]{1,0:T(8,128)(2,1)S(1)}, u32[]{:S(2)}, u32[]{:S(2)}) collective-permute-start(bf16[96,2048]{1,0:T(8,128)(2,1)S(1)} %get-tuple-element.69.refs_0_), channel_id=1, source_target_pairs={{0,2},{2,4},{4,6},{6,0},{1,3},{3,5},{5,7},{7,1},{8,10},{10,12},{12... | collective-permute-start | bytes 1179656 | tf_op jit(solution)/shard_map/ppermute | solution.py:30
  91.7 1.0 copy-start.12
  94.7 24.4 %collective-permute-start.23 = (bf16[96,2048]{1,0:T(8,128)(2,1)S(1)}, bf16[96,2048]{1,0:T(8,128)(2,1)S(1)}, u32[]{:S(2)}, u32[]{:S(2)}) collective-permute-start(bf16[96,2048]{1,0:T(8,128)(2,1)S(1)} %get-tuple-element.56), channel_id=1, source_target_pairs={{0,8},{8,16},{16,24},{24,0},{1,9},{9,17},{17,25},{25,1},{2,10},{10... | collective-permute-start | bytes 1179656 | tf_op jit(solution)/shard_map/ppermute | solution.py:30
  96.1 27.0 %collective-permute-start.24 = (bf16[96,2048]{1,0:T(8,128)(2,1)S(1)}, bf16[96,2048]{1,0:T(8,128)(2,1)S(1)}, u32[]{:S(2)}, u32[]{:S(2)}) collective-permute-start(bf16[96,2048]{1,0:T(8,128)(2,1)S(1)} %get-tuple-element.57), channel_id=1, source_target_pairs={{0,16},{8,24},{16,0},{24,8},{1,17},{9,25},{17,1},{25,9},{2,18},{10... | collective-permute-start | bytes 1179656 | tf_op jit(solution)/shard_map/ppermute | solution.py:30
  107.2 6.0 %copy-start.10 = (bf16[192,2048]{1,0:T(8,128)(2,1)S(1)}, bf16[192,2048]{1,0:T(8,128)(2,1)}, u32[]{:S(2)}) copy-start(bf16[192,2048]{1,0:T(8,128)(2,1)} %copy-done.9) | copy-start | bytes 2359300
  107.2 16.7 %collective-permute-start.25 = (bf16[96,2048]{1,0:T(8,128)(2,1)}, bf16[96,2048]{1,0:T(8,128)(2,1)}, u32[]{:S(2)}, u32[]{:S(2)}) collective-permute-start(bf16[96,2048]{1,0:T(8,128)(2,1)} %get-tuple-element.58), channel_id=1, source_target_pairs={{0,24},{8,0},{16,8},{24,16},{1,25},{9,1},{17,9},{25,17},{2,26},{10... | collective-permute-start | bytes 1179656 | tf_op jit(solution)/shard_map/ppermute | solution.py:30
  113.2 9.9 %copy-start.4 = (bf16[384,128]{1,0:T(8,128)(2,1)}, bf16[384,128]{1,0:T(8,128)(2,1)S(1)}, u32[]{:S(2)}) copy-start(bf16[384,128]{1,0:T(8,128)(2,1)S(1)} %get-tuple-element.40.mine) | copy-start | bytes 294916
  114.7 22.7 %collective-permute-start.8 = (bf16[96,2048]{1,0:T(8,128)(2,1)}, bf16[96,2048]{1,0:T(8,128)(2,1)S(1)}, u32[]{:S(2)}, u32[]{:S(2)}) collective-permute-start(bf16[96,2048]{1,0:T(8,128)(2,1)} %get-tuple-element.45), channel_id=1, source_target_pairs={{0,2},{2,4},{4,6},{6,0},{1,3},{3,5},{5,7},{7,1},{8,10},{10,12},{12... | collective-permute-start | bytes 1179656 | tf_op jit(solution)/shard_map/ppermute | solution.py:30
  114.7 22.8 %collective-permute-start.9 = (bf16[96,2048]{1,0:T(8,128)(2,1)}, bf16[96,2048]{1,0:T(8,128)(2,1)S(1)}, u32[]{:S(2)}, u32[]{:S(2)}) collective-permute-start(bf16[96,2048]{1,0:T(8,128)(2,1)} %get-tuple-element.46), channel_id=1, source_target_pairs={{0,4},{2,6},{4,0},{6,2},{1,5},{3,7},{5,1},{7,3},{8,12},{10,14},{12... | collective-permute-start | bytes 1179656 | tf_op jit(solution)/shard_map/ppermute | solution.py:30
  119.1 0.7 copy-start
  119.8 17.6 %collective-permute-start.10 = (bf16[96,2048]{1,0:T(8,128)(2,1)}, bf16[96,2048]{1,0:T(8,128)(2,1)S(1)}, u32[]{:S(2)}, u32[]{:S(2)}) collective-permute-start(bf16[96,2048]{1,0:T(8,128)(2,1)} %get-tuple-element.47), channel_id=1, source_target_pairs={{0,6},{2,0},{4,2},{6,4},{1,7},{3,1},{5,3},{7,5},{8,14},{10,8},{12,... | collective-permute-start | bytes 1179656 | tf_op jit(solution)/shard_map/ppermute | solution.py:30
  123.2 0.8 copy-start.2
  123.9 5.9 %collective-permute-start.7 = (bf16[384,128]{1,0:T(8,128)(2,1)}, bf16[384,128]{1,0:T(8,128)(2,1)}, u32[]{:S(2)}, u32[]{:S(2)}) collective-permute-start(bf16[384,128]{1,0:T(8,128)(2,1)} %get-tuple-element.41), channel_id=1, source_target_pairs={{0,1},{1,0},{2,3},{3,2},{4,5},{5,4},{6,7},{7,6},{8,9},{9,8},{10,11... | collective-permute-start | bytes 294920 | tf_op jit(solution)/shard_map/ppermute | solution.py:25
  123.9 1.0 copy-start.1
  124.9 1.0 copy-start.3
  125.9 11.5 %copy-start.5 = (bf16[384,128]{1,0:T(8,128)(2,1)S(1)}, bf16[384,128]{1,0:T(8,128)(2,1)}, u32[]{:S(2)}) copy-start(bf16[384,128]{1,0:T(8,128)(2,1)} %copy-done.4) | copy-start | bytes 294916
  127.1 22.9 %copy-start.6 = (f32[64,352]{1,0:T(8,128)S(1)}, f32[64,352]{1,0:T(8,128)}, u32[]{:S(2)}) copy-start(f32[64,352]{1,0:T(8,128)} %gate.1) | copy-start | bytes 270340
  127.2 22.8 %copy-start.7 = (f32[64,352]{1,0:T(8,128)S(1)}, f32[64,352]{1,0:T(8,128)}, u32[]{:S(2)}) copy-start(f32[64,352]{1,0:T(8,128)} %up.1) | copy-start | bytes 270340
  127.2 22.8 %copy-start.8 = (f32[352,64]{0,1:T(8,128)S(1)}, f32[352,64]{0,1:T(8,128)}, u32[]{:S(2)}) copy-start(f32[352,64]{0,1:T(8,128)} %param.17) | copy-start | bytes 270340
  127.2 15.6 %collective-permute-start.28 = (bf16[24,2048]{1,0:T(8,128)(2,1)S(1)}, bf16[24,2048]{1,0:T(8,128)(2,1)S(1)}, u32[]{:S(2)}, u32[]{:S(2)}) collective-permute-start(bf16[24,2048]{1,0:T(8,128)(2,1)S(1)} %get-tuple-element.62), channel_id=1, source_target_pairs={{0,6},{2,0},{4,2},{6,4},{1,7},{3,1},{5,3},{7,5},{8,14},{10,8},{12,... | collective-permute-start | bytes 294920 | tf_op jit(solution)/shard_map/ppermute | solution.py:30
  129.8 14.4 %collective-permute-start.27 = (bf16[24,2048]{1,0:T(8,128)(2,1)S(1)}, bf16[24,2048]{1,0:T(8,128)(2,1)S(1)}, u32[]{:S(2)}, u32[]{:S(2)}) collective-permute-start(bf16[24,2048]{1,0:T(8,128)(2,1)S(1)} %get-tuple-element.61), channel_id=1, source_target_pairs={{0,4},{2,6},{4,0},{6,2},{1,5},{3,7},{5,1},{7,3},{8,12},{10,14},{12... | collective-permute-start | bytes 294920 | tf_op jit(solution)/shard_map/ppermute | solution.py:30
  137.4 6.9 %collective-permute-start.26 = (bf16[24,2048]{1,0:T(8,128)(2,1)S(1)}, bf16[24,2048]{1,0:T(8,128)(2,1)S(1)}, u32[]{:S(2)}, u32[]{:S(2)}) collective-permute-start(bf16[24,2048]{1,0:T(8,128)(2,1)S(1)} %get-tuple-element.60), channel_id=1, source_target_pairs={{0,2},{2,4},{4,6},{6,0},{1,3},{3,5},{5,7},{7,1},{8,10},{10,12},{12... | collective-permute-start | bytes 294920 | tf_op jit(solution)/shard_map/ppermute | solution.py:30
  138.6 8.0 %collective-permute-start.11 = (bf16[24,3072]{1,0:T(8,128)(2,1)S(1)}, bf16[24,3072]{1,0:T(8,128)(2,1)S(1)}, u32[]{:S(2)}, u32[]{:S(2)}) collective-permute-start(bf16[24,3072]{1,0:T(8,128)(2,1)S(1)} %get-tuple-element.49), channel_id=1, source_target_pairs={{0,8},{8,16},{16,24},{24,0},{1,9},{9,17},{17,25},{25,1},{2,10},{10... | collective-permute-start | bytes 442376 | tf_op jit(solution)/shard_map/ppermute | solution.py:30
  140.1 8.4 %collective-permute-start.12 = (bf16[24,3072]{1,0:T(8,128)(2,1)S(1)}, bf16[24,3072]{1,0:T(8,128)(2,1)S(1)}, u32[]{:S(2)}, u32[]{:S(2)}) collective-permute-start(bf16[24,3072]{1,0:T(8,128)(2,1)S(1)} %get-tuple-element.50), channel_id=1, source_target_pairs={{0,16},{8,24},{16,0},{24,8},{1,17},{9,25},{17,1},{25,9},{2,18},{10... | collective-permute-start | bytes 442376 | tf_op jit(solution)/shard_map/ppermute | solution.py:30
  142.8 5.8 %collective-permute-start.13 = (bf16[24,3072]{1,0:T(8,128)(2,1)S(1)}, bf16[24,3072]{1,0:T(8,128)(2,1)S(1)}, u32[]{:S(2)}, u32[]{:S(2)}) collective-permute-start(bf16[24,3072]{1,0:T(8,128)(2,1)S(1)} %get-tuple-element.51), channel_id=1, source_target_pairs={{0,24},{8,0},{16,8},{24,16},{1,25},{9,1},{17,9},{25,17},{2,26},{10... | collective-permute-start | bytes 442376 | tf_op jit(solution)/shard_map/ppermute | solution.py:30
